TPU v7x, 128 devices: a whole 4x4x4 slice. The times are simulated.
128 devices in a mesh: sp: 64 (over z, y, x), tp: 2 (over core).
Axes of the slice: x: 4, y: 4, z: 4, core: 2. Of those that a mesh axis runs over, the one named last changes fastest.
Arguments:
- queries: bfloat16 [16384, 512], P('sp', 'tp'), may hold values from -20 to 20
- key_rows: bfloat16 [16384, 512], P('sp', 'tp'), may hold values from -20 to 20
- value_rows: bfloat16 [16384, 512], P('sp', 'tp'), may hold values from -6 to 6
- residual: bfloat16 [16384, 2048], P(('sp', 'tp')), may hold values from -6 to 6
- out_weight: bfloat16 [512, 2048], replicated, may hold values from -0.75 to 0.75
- norm_gain: float32 [2048], replicated, may hold values from 0.1 to 1.9
- routes: int32 [16384, 8], P(('sp', 'tp')), may hold values from 0 to 63, all different within a row; in each aligned block of 128 rows (0 to 127, 128 to 255, ...) at most 20 rows name the same one
- route_weight: float32 [16384, 8], P(('sp', 'tp')), may hold values from 0.1 to 0.6
- expert_gate: bfloat16 [64, 2048, 512], P('sp', None, 'tp'), may hold values from -0.125 to 0.125
- expert_up: bfloat16 [64, 2048, 512], P('sp', None, 'tp'), may hold values from -0.125 to 0.125
- expert_down: bfloat16 [64, 512, 2048], P('sp', 'tp'), may hold values from -0.25 to 0.25
- shared_gate: bfloat16 [2048, 512], replicated, may hold values from -0.125 to 0.125
- shared_up: bfloat16 [2048, 512], replicated, may hold values from -0.125 to 0.125
- shared_down: bfloat16 [512, 2048], replicated, may hold values from -0.25 to 0.25
Outputs:
- output: bfloat16 [16384, 2048], P(('sp', 'tp'))
Inputs may be any that keep to these rules, and one draw needn't show every extreme that they name: `routes`: each row names 8 different experts. In each aligned block of 128 rows (the rows of one device) no expert is named more than 20 times, a bound that some block reaches.
All inputs are finite; a program needn't handle non-finite values.
Results may differ from a plain program's by a relative error of at most 0.012.
Values may be sent and summed in bfloat16 or wider, within the bound.
No kernel may reach another device: no remote copies, remote signals or barrier semaphores. Data moves between devices by JAX's collectives and lax.ppermute only.
A program may use at most 192 MiB of HBM per device.

v0:
```python
import jax
import jax.numpy as jnp
from jax import lax
from jax.sharding import PartitionSpec as P

HEAD_DIM = 64
TOPK = 8


norm_eps = 1e-06


def side_by_side(arrays, axis, dim, along):
    ends, at = ([], 0)
    for a in arrays[:-1]:
        at += a.shape[along]
        ends.append(at)
    both = jnp.concatenate(arrays, axis=along)
    return tuple(jnp.split(lax.all_gather(both, axis, axis=dim, tiled=True), ends, axis=along))


def block_terms(query_heads, key_piece, value_piece, first_block, own_block):
    query_count, local_heads, head_width = query_heads.shape
    groups = key_piece.shape[0] // query_count
    key_heads = key_piece.reshape(groups, query_count, local_heads, head_width)
    value_heads = value_piece.reshape(groups, query_count, local_heads, head_width)
    scores = jnp.einsum(
        "thd,gshd->hgts", query_heads, key_heads, preferred_element_type=jnp.float32
    ) * head_width ** (-0.5)
    query_pos = own_block * query_count + jnp.arange(query_count, dtype=jnp.int32)
    key_pos = (first_block + jnp.arange(groups, dtype=jnp.int32))[
        :, None
    ] * query_count + jnp.arange(query_count, dtype=jnp.int32)[None, :]
    live = key_pos[None, :, None, :] < query_pos[None, None, :, None]
    cost = jnp.where(live, jax.nn.softplus(scores), 0.0)
    inside = lax.cumsum(cost, axis=3, reverse=True) - cost
    weight = jnp.where(live, jnp.exp(jax.nn.log_sigmoid(scores) - inside), 0.0).astype(jnp.bfloat16)
    partial_value = jnp.einsum(
        "hgts,gshd->gthd", weight, value_heads, preferred_element_type=jnp.float32
    )
    total = jnp.sum(cost, axis=3).transpose(1, 0, 2)
    return (partial_value.reshape(groups, query_count, local_heads * head_width), total)


def expert_product(rows, gate_half, up_half, down_half):
    gate = jnp.einsum("seid,edf->seif", rows, gate_half, preferred_element_type=jnp.float32)
    upward = jnp.einsum("seid,edf->seif", rows, up_half, preferred_element_type=jnp.float32)
    hidden = (jax.nn.silu(gate) * upward).astype(jnp.bfloat16)
    return jnp.einsum("seif,efd->seid", hidden, down_half, preferred_element_type=jnp.float32)


def local(
    queries,
    key_rows,
    value_rows,
    residual,
    out_weight,
    norm_gain,
    routes,
    route_weight,
    expert_gate,
    expert_up,
    expert_down,
    shared_gate,
    shared_up,
    shared_down,
):
    query_count = queries.shape[0]
    local_width = queries.shape[1]
    local_heads = local_width // HEAD_DIM
    blocks = lax.axis_size("sp")
    own_block = lax.axis_index("sp")
    query_heads = queries.reshape(query_count, local_heads, HEAD_DIM)
    empty = (
        jnp.zeros((blocks, query_count, local_width), jnp.float32),
        jnp.zeros((blocks, local_heads, query_count), jnp.float32),
    )
    key_piece, value_piece = side_by_side((key_rows, value_rows), "sp", 0, 1)
    shards = key_piece.shape[0] // query_count
    group = 4

    def turn(index, tables):
        first_block = index * group
        key_group = lax.dynamic_slice_in_dim(
            key_piece, index * group * query_count, group * query_count, 0
        )
        value_group = lax.dynamic_slice_in_dim(
            value_piece, index * group * query_count, group * query_count, 0
        )

        def compute():
            return block_terms(query_heads, key_group, value_group, first_block, own_block)

        def skipped():
            return (
                jnp.zeros((group, query_count, local_width), jnp.float32),
                jnp.zeros((group, local_heads, query_count), jnp.float32),
            )

        partial_value, total = lax.cond(first_block <= own_block, compute, skipped)
        return (
            lax.dynamic_update_slice_in_dim(tables[0], partial_value, first_block, 0),
            lax.dynamic_update_slice_in_dim(tables[1], total, first_block, 0),
        )

    partials, totals = lax.fori_loop(0, shards // group, turn, empty)
    later = lax.cumsum(totals, axis=0, reverse=True) - totals
    attended = jnp.einsum(
        "bht,bthd->thd",
        jnp.exp(-later),
        partials.reshape(blocks, query_count, local_heads, HEAD_DIM),
        precision=lax.Precision.HIGHEST,
    )
    attended = attended.reshape(query_count, local_width).astype(jnp.bfloat16)
    token_rows = residual.shape[0]
    token_heads = lax.all_to_all(attended, "tp", split_axis=0, concat_axis=1, tiled=True)
    projected = jnp.dot(token_heads, out_weight, preferred_element_type=jnp.float32)
    mixed_wide = (residual.astype(jnp.float32) + projected).astype(jnp.bfloat16).astype(jnp.float32)
    inverse = lax.rsqrt(jnp.mean(mixed_wide * mixed_wide, axis=1, keepdims=True) + norm_eps)
    normed = (mixed_wide * inverse * norm_gain).astype(jnp.bfloat16)
    width = normed.shape[1]
    local_experts = expert_gate.shape[0]
    experts_all = blocks * local_experts
    capacity = max(2, token_rows * TOPK * 5 // (4 * experts_all))
    flat_routes = routes.reshape(-1)
    picks = (flat_routes[:, None] == jnp.arange(experts_all, dtype=jnp.int32)[None, :]).astype(
        jnp.int32
    )
    earlier = jnp.cumsum(picks, axis=0) - picks
    position = flat_routes * capacity + jnp.sum(earlier * picks, axis=1)
    filler = (
        jnp.zeros((experts_all * capacity,), jnp.int32)
        .at[position]
        .set(jnp.arange(flat_routes.shape[0], dtype=jnp.int32) + 1)
    )
    occupied = filler > 0
    source_token = jnp.maximum(filler - 1, 0) // TOPK
    outgoing = jnp.where(
        occupied[:, None], normed[source_token], jnp.zeros((), jnp.bfloat16)
    ).reshape(experts_all, capacity, width)
    both = lax.all_gather(
        lax.all_to_all(outgoing, "sp", split_axis=0, concat_axis=0, tiled=True),
        "tp",
        axis=0,
        tiled=True,
    )
    shaped = both.reshape(-1, local_experts, both.shape[1], both.shape[2])
    pieces = expert_product(shaped, expert_gate, expert_up, expert_down).reshape(both.shape)
    summed = lax.psum_scatter(pieces.astype(jnp.bfloat16), "tp", scatter_dimension=0, tiled=True)
    results = lax.all_to_all(summed, "sp", split_axis=0, concat_axis=0, tiled=True).reshape(
        experts_all * capacity, width
    )
    picked = results[position].reshape(token_rows, TOPK, width)
    routed = jnp.sum(picked.astype(jnp.float32) * route_weight[:, :, None], axis=1)
    shared_gate_out = jnp.dot(normed, shared_gate, preferred_element_type=jnp.float32)
    shared_up_out = jnp.dot(normed, shared_up, preferred_element_type=jnp.float32)
    shared_act = (jax.nn.silu(shared_gate_out) * shared_up_out).astype(jnp.bfloat16)
    shared_out = jnp.dot(shared_act, shared_down, preferred_element_type=jnp.float32)
    return (mixed_wide + routed + shared_out).astype(jnp.bfloat16)


def solution(mesh):
    return jax.shard_map(
        local,
        mesh=mesh,
        in_specs=(
            P("sp", "tp"),
            P("sp", "tp"),
            P("sp", "tp"),
            P(("sp", "tp"), None),
            P(),
            P(),
            P(("sp", "tp"), None),
            P(("sp", "tp"), None),
            P("sp", None, "tp"),
            P("sp", None, "tp"),
            P("sp", "tp", None),
            P(),
            P(),
            P(),
        ),
        out_specs=P(("sp", "tp"), None),
        check_vma=False,
    )
```

profile of v0, /device:TPU:0, one launch (start us, length us, event | category | flops | bytes accessed | tf_op | source)
XLA Modules:
  0.0 1779.6 jit_solution(9955450502240374601)
XLA Ops:
  6.5 1.1 copy.47
  11.5 18.0 %reduce-window.28 = s32[64,8,128]{2,1,0:T(8,128)S(1)} reduce-window(s32[64,8,128]{2,1,0:T(8,128)S(1)} %fusion.43, s32[]{:T(128)} %constant.144.clone.1), window={size=1x1x128 pad=0_0x0_0x127_0}, to_apply=%region_8.9 | reduce-window | flops 8323072 | bytes 524292 | tf_op jit(solution)/shard_map/reduce-window.2
  31.1 4.3 scatter_custom_fusion
  36.8 114.8 %all-gather.3.cloned.1.call-done = bf16[16384,512]{0,1:T(8,128)(2,1)} async-done(((bf16[256,512]{0,1:T(8,128)(2,1)}), bf16[16384,512]{0,1:T(8,128)(2,1)}) %all-gather.3.cloned.1.call-update) | async-done | bytes 16777232 | tf_op jit(solution)/shard_map/all_gather | solution.py:19
  151.5 11.4 fusion.50
  163.0 7.8 broadcast_in_dim.53
  170.8 125.3 %while.17 = (s32[]{:T(128)}, f32[64,256,256]{1,2,0:T(8,128)}, f32[64,4,256]{2,1,0:T(4,128)S(1)}, s32[]{:T(128)}, bf16[16384,256]{0,1:T(8,128)(2,1)}, /*index=5*/...) while((s32[]{:T(128)}, f32[64,256,256]{1,2,0:T(8,128)}, ...), condition=%wide.region_6.7_spmd, body=%wide.region_0.6_spmd.sunk | while | flops 433333504 | bytes 72526192 | solution.py:106
  171.0 70.4 %conditional.2 = (f32[4,256,256]{1,2,0:T(8,128)S(1)}, f32[4,4,256]{2,0,1:T(4,128)S(1)}) conditional(s32[]{:T(128)} %convert_element_type.96, () %tuple.64, (s32[]{:T(128)}, s32[]{:T(128)}, s32[]{:T(128)}, bf16[16384,256]{0,1:T(8,128)(2,1)}, bf16[256,4,64]{0,2,1:T(8,128)(2,1)S(1)}, /*index=5*/bf16[16384,256]{0,1:T(8,128)(2,1)}) %tuple.65), branch_computations={%region_1.0_spmd, %region_2.5_spmd} | conditional | flops 433333504 | bytes 70396048 | solution.py:100
  171.0 1.3 constant_dynamic-slice_fusion
  172.3 1.2 reshape.174
  173.8 7.5 fusion.18
  181.2 41.6 %fusion.10 = f32[4,4,256,2,128]{2,3,4,1,0:T(2,128)} fusion(f32[4,4,256,2,128]{2,4,3,1,0:T(8,128)} %bitcast.139), kind=kOutput, calls=%fused_computation.19 | output fusion | flops 133169152 | bytes 8388608 | tf_op jit(solution)/shard_map/reduce-window.10
  223.7 4.0 broadcast_add_fusion
  228.3 1.6 copy-done.1
  229.9 7.7 fusion.4
  237.6 1.2 reshape.177
  238.8 2.2 fusion.12
  241.4 1.1 constant_dynamic-update-slice_fusion.2
  250.0 9.5 conditional.2
  259.5 1.1 constant_dynamic-update-slice_fusion.2
  260.6 8.5 conditional.2
  269.2 1.1 constant_dynamic-update-slice_fusion.2
  270.5 1.1 constant_dynamic-update-slice_fusion.2
  273.1 1.1 constant_dynamic-update-slice_fusion.2
  274.5 1.1 constant_dynamic-update-slice_fusion.2
  277.1 1.1 constant_dynamic-update-slice_fusion.2
  282.5 1.1 constant_dynamic-update-slice_fusion.2
  285.2 1.1 constant_dynamic-update-slice_fusion.2
  286.5 1.1 constant_dynamic-update-slice_fusion.2
  296.7 7.8 multiply_reduce_fusion
  304.5 3.8 all_to_all.26
  310.1 6.2 gather_fusion
  316.3 8.9 gather.9
  325.2 3.3 broadcast_select_fusion
  328.5 1232.3 %all_to_all.27 = bf16[64,20,2048]{2,1,0:T(8,128)(2,1)S(1)} all-to-all(bf16[64,20,2048]{2,1,0:T(8,128)(2,1)S(1)} %broadcast_select_fusion), channel_id=1, replica_groups=mesh['sp'=64,'tp'=2] {'sp'}, dimensions={0} | all-to-all | bytes 10485760 | tf_op jit(solution)/shard_map/all_to_all | solution.py:142
  1560.8 5.2 copy.58
  1566.1 22.3 %all-gather.5.cloned.1.call-done = bf16[128,20,2048]{2,0,1:T(8,128)(2,1)} async-done(((bf16[64,20,2048]{2,0,1:T(8,128)(2,1)}), bf16[128,20,2048]{2,0,1:T(8,128)(2,1)}) %all-gather.5.cloned.1.call-update) | async-done | bytes 10485776 | tf_op jit(solution)/shard_map/all_gather | solution.py:141
  1588.4 8.6 fusion.31
  1597.0 16.9 convolution_convert_fusion
  1614.0 22.2 %reduce-scatter.2.cloned.1.call-done = bf16[64,20,2048]{2,0,1:T(8,128)(2,1)} async-done(((bf16[128,20,2048]{2,0,1:T(8,128)(2,1)}), bf16[64,20,2048]{2,0,1:T(8,128)(2,1)}) %reduce-scatter.2.cloned.1.call-update) | async-done | bytes 5242896 | tf_op jit(solution)/shard_map/reduce_scatter | solution.py:149
  1636.2 8.1 copy.59
  1644.3 11.0 all-to-all-start.2
  1655.4 2.0 fusion.51
  1657.5 82.4 %all-to-all-done.2 = bf16[64,20,2048]{2,1,0:T(8,128)(2,1)} async-done(((bf16[64,20,2048]{2,1,0:T(8,128)(2,1)}), bf16[64,20,2048]{2,1,0:T(8,128)(2,1)}, u32[]{:S(2)}, u32[]{:S(2)}) %all-to-all-start.2) | async-done | bytes 5242912 | tf_op jit(solution)/shard_map/all_to_all | solution.py:150
  1739.9 9.0 reshape.194
  1748.9 12.0 gather_fusion.1
  1760.9 7.5 fusion.19
  1768.4 4.4 fusion.26
  (130 shorter events, 21.6 us)
Async XLA Ops:
  6.5 301.8 %copy-start = (bf16[512,2048]{1,0:T(8,128)(2,1)S(1)}, bf16[512,2048]{1,0:T(8,128)(2,1)}, u32[]{:S(2)}) copy-start(bf16[512,2048]{1,0:T(8,128)(2,1)} %param.22) | copy-start | bytes 6291460
  6.5 145.0 %all-gather.3.cloned.1.call-start = ((), (), s32[]{:S(2)}) async-start(), calls=%async_computation.4 | async-start | bytes 17039360 | tf_op jit(solution)/shard_map/all_gather | solution.py:19
  9.5 1579.0 %all-gather.5.cloned.1.call-start = ((), (), s32[]{:S(2)}) async-start(), calls=%async_computation.5 | async-start | bytes 15728640 | tf_op jit(solution)/shard_map/all_gather | solution.py:141
  31.1 131.9 %copy-start.6 = (s32[1024,1]{0,1:T(1,128)}, s32[1024,1]{0,1:T(1,128)S(1)}, u32[]{:S(2)}) copy-start(s32[1024,1]{0,1:T(1,128)S(1)} %compare_select_fusion.2) | copy-start | bytes 12292
  227.7 2.2 copy-start.1
  296.7 11.7 copy-start.3
  304.5 5.5 copy-start.8
  304.5 5.6 copy-start.4
  308.9 1.0 copy-start.2
  316.3 8.9 copy-start.5
  1566.1 70.1 %reduce-scatter.2.cloned.1.call-start = ((), (), s32[]{:S(2)}) async-start(), calls=%async_computation.6 | async-start | bytes 15728640 | tf_op jit(solution)/shard_map/reduce_scatter | solution.py:149
  1644.3 11.0 copy-start.9
  1644.3 11.1 copy-start.7
  1644.3 95.6 %all-to-all-start.2 = ((bf16[64,20,2048]{2,1,0:T(8,128)(2,1)}), bf16[64,20,2048]{2,1,0:T(8,128)(2,1)}, u32[]{:S(2)}, u32[]{:S(2)}) async-start(bf16[64,20,2048]{2,1,0:T(8,128)(2,1)} %copy.59), calls=%async_computation.3 | async-start | bytes 12582912 | tf_op jit(solution)/shard_map/all_to_all | solution.py:150
Sparse Core Ops, SparseCore 0:
  10.0 141.4 all-gather.2
  1566.2 22.1 all-gather.4
  1614.1 22.0 reduce-scatter.1
where the time goes:
time: 1790 us; the launch traced here: 1780 us
  blocking collectives  1240 us (69%)
  waiting for transfers between devices  242 us (14%)
  local copies, waits for them, and re-layouts  105 us (6%)
  other arithmetic  93.2 us (5%)
  matrix products  42.2 us (2%)
  loops' own time  36.9 us (2%)
    all_to_all x1, blocking collectives, local(): lax.all_to_all(outgoing, 'sp', split_axis=0, concat_axis=0, tiled=True)  1230 us
    all_gather x1, waiting for transfers between devices, side_by_side(): lax.all_gather(both, axis, axis=dim, tiled=True)  115 us
    all_to_all x1, waiting for transfers between devices, local(): lax.all_to_all(summed, 'sp', split_axis=0, concat_axis=0, tiled=True)  82.4 us
    another operation x5, other arithmetic  59.9 us
  transfers between devices with their start and end apart: 4, of which 4 were waited for; matrix products, arithmetic and copies ran while one was open for 2% of the time, Pallas kernels for 0%

commit v1 on v0

v1 whole, which is shorter than its diff:
```python
import jax
import jax.numpy as jnp
from jax import lax
from jax.experimental import pallas as pl
from jax.experimental.pallas import tpu as pltpu
from jax.sharding import PartitionSpec as P

HEAD_DIM = 64
LANES = 128
TOPK = 8
LOG2E = 1.4426950408889634
norm_eps = 1e-06


def attention_kernel(meta_ref, query_ref, kv_ref, out_ref, tri_ref, acc_ref):
    own, plane = meta_ref[0], meta_ref[1]
    side = tri_ref.shape[0]
    row = lax.broadcasted_iota(jnp.int32, (side, side), 0)
    col = lax.broadcasted_iota(jnp.int32, (side, side), 1)
    tri_ref[...] = (row > col).astype(jnp.bfloat16)

    def key_block(block):
        quarter, place = block // 16, block % 16
        slot = jnp.where((quarter + plane) % 2 == 1, 15 - place, place)
        return kv_ref[slot, quarter]

    def tile(query, block, diagonal):
        kv = key_block(block)
        score = lax.dot_general(
            query, kv, (((1,), (1,)), ((), ())), preferred_element_type=jnp.float32
        ) * (HEAD_DIM**-0.5 * LOG2E)
        cost = jnp.maximum(score, 0.0) + jnp.log2(1.0 + jnp.exp2(-jnp.abs(score)))
        slack = score - cost
        if diagonal is not None:
            live = col + block * side < row + diagonal * side
            cost = jnp.where(live, cost, 0.0)
        high = cost.astype(jnp.bfloat16)
        low = (cost - high.astype(jnp.float32)).astype(jnp.bfloat16)
        tri = tri_ref[...]
        inside = jnp.dot(high, tri, preferred_element_type=jnp.float32) + jnp.dot(
            low, tri, preferred_element_type=jnp.float32
        )
        weight = jnp.exp2(slack - inside)
        if diagonal is not None:
            weight = jnp.where(live, weight, 0.0)
        part = jnp.dot(weight.astype(jnp.bfloat16), kv, preferred_element_type=jnp.float32)
        decay = jnp.exp2(-(inside[:, 0:1] + cost[:, 0:1]))
        return part, decay

    @pl.loop(0, 4)
    def _(quarter):
        block = quarter * 16 + jnp.where(quarter % 2 == 1, 15 - own, own)
        query = query_ref[quarter]
        acc_ref[...] = jnp.zeros_like(acc_ref)

        @pl.loop(0, block // 2)
        def _(pair):
            part0, decay0 = tile(query, pair * 2, None)
            part1, decay1 = tile(query, pair * 2 + 1, None)
            acc_ref[...] = (acc_ref[...] * decay0 + part0) * decay1 + part1

        last = block // 2 * 2
        part0, decay0 = tile(query, last, block)
        part1, decay1 = tile(query, last + 1, block)
        out_ref[quarter] = ((acc_ref[...] * decay0 + part0) * decay1 + part1).astype(jnp.bfloat16)


def attention(meta, query, kv):
    side = query.shape[1]
    pairs = 132 * side * side
    return pl.pallas_call(
        attention_kernel,
        out_shape=jax.ShapeDtypeStruct((4, side, LANES), jnp.bfloat16),
        in_specs=[pl.BlockSpec(memory_space=pltpu.SMEM)] + [pl.BlockSpec(memory_space=pltpu.VMEM)] * 2,
        out_specs=pl.BlockSpec(memory_space=pltpu.VMEM),
        scratch_shapes=[pltpu.VMEM((side, side), jnp.bfloat16), pltpu.VMEM((side, LANES), jnp.float32)],
        compiler_params=pltpu.CompilerParams(vmem_limit_bytes=24 * 2**20),
        cost_estimate=pl.CostEstimate(
            flops=pairs * 2 * 768, bytes_accessed=6 * 2**20, transcendentals=pairs * 3
        ),
        name="attend",
    )(meta, query, kv)


def local(
    queries,
    key_rows,
    value_rows,
    residual,
    out_weight,
    norm_gain,
    routes,
    route_weight,
    expert_gate,
    expert_up,
    expert_down,
    shared_gate,
    shared_up,
    shared_down,
):
    side = queries.shape[0]
    position = lax.axis_index("sp")
    plane = position // 16
    spot = position % 16
    own = jnp.where(plane % 2 == 1, 15 - spot, spot)
    meta = jnp.stack([own, plane]).astype(jnp.int32)
    columns = [[i, 31 - i, 32 + i, 63 - i] for i in range(16)]
    planes = [[16 * z + j for j in range(16)] for z in range(4)]

    def heads(rows):
        return rows.reshape(side, 4, HEAD_DIM).transpose(1, 0, 2)

    query_heads = heads(queries)
    packed = jnp.concatenate(
        [query_heads, jnp.zeros_like(query_heads), heads(key_rows), heads(value_rows)], axis=2
    )
    packed = lax.all_to_all(packed, "sp", 0, 0, axis_index_groups=columns, tiled=True)
    kv = lax.all_gather(packed[:, :, LANES:], "sp", axis_index_groups=planes, axis=0)
    peer = [(0, 1), (1, 0)]
    kv, expert_gate_, expert_up_, expert_down_ = lax.optimization_barrier(
        (kv, expert_gate, expert_up, expert_down)
    )
    gate_other = lax.ppermute(expert_gate_, "tp", peer)
    up_other = lax.ppermute(expert_up_, "tp", peer)
    down_other = lax.ppermute(expert_down_, "tp", peer)
    attended = attention(meta, packed[:, :, :LANES], kv)[:, :, HEAD_DIM:]
    tokens = residual.shape[0]
    eights = [[2 * s + c for s in g for c in range(2)] for g in columns]
    attended = attended.reshape(8, tokens, HEAD_DIM)
    attended = lax.all_to_all(attended, ("sp", "tp"), 0, 0, axis_index_groups=eights, tiled=True)
    attended = attended.reshape(4, 2, tokens, HEAD_DIM).transpose(2, 1, 0, 3).reshape(tokens, 512)

    projected = jnp.dot(attended, out_weight, preferred_element_type=jnp.float32)
    mixed = (residual.astype(jnp.float32) + projected).astype(jnp.bfloat16).astype(jnp.float32)
    inverse = lax.rsqrt(jnp.mean(mixed * mixed, axis=1, keepdims=True) + norm_eps)
    normed = (mixed * inverse * norm_gain).astype(jnp.bfloat16)
    width = normed.shape[1]
    experts = lax.axis_size("sp")
    capacity = 20
    named = routes[:, :, None] == jnp.arange(experts, dtype=jnp.int32)
    pick = jnp.any(named, axis=1)
    share = jnp.sum(jnp.where(named, route_weight[:, :, None], 0.0), axis=1)
    below = jnp.tril(jnp.ones((tokens, tokens), jnp.bfloat16), -1)
    rank = jnp.dot(below, pick.astype(jnp.bfloat16), preferred_element_type=jnp.float32)
    rank = jnp.where(pick, rank, -1.0).T
    slot = rank[:, None, :] == jnp.arange(capacity, dtype=jnp.float32)[None, :, None]
    send = slot.astype(jnp.bfloat16).reshape(experts * capacity, tokens)
    outgoing = jnp.dot(send, normed, preferred_element_type=jnp.bfloat16)
    incoming = lax.all_to_all(
        outgoing.reshape(experts, capacity, width), "sp", 0, 0, tiled=True
    ).reshape(experts * capacity, width)

    def half(gate_half, up_half, down_half):
        gate = jnp.dot(incoming, gate_half[0], preferred_element_type=jnp.float32)
        upward = jnp.dot(incoming, up_half[0], preferred_element_type=jnp.float32)
        hidden = (jax.nn.silu(gate) * upward).astype(jnp.bfloat16)
        return jnp.dot(hidden, down_half[0], preferred_element_type=jnp.float32)

    result = half(expert_gate, expert_up, expert_down) + half(gate_other, up_other, down_other)
    returned = lax.all_to_all(
        result.astype(jnp.bfloat16).reshape(experts, capacity, width), "sp", 0, 0, tiled=True
    ).reshape(experts * capacity, width)
    weighted = jnp.where(slot, share.T[:, None, :], 0.0).reshape(experts * capacity, tokens)
    high = weighted.astype(jnp.bfloat16)
    low = (weighted - high.astype(jnp.float32)).astype(jnp.bfloat16)
    both = jnp.concatenate([high, low], axis=1)
    routed = lax.dot_general(
        both, returned, (((0,), (0,)), ((), ())), preferred_element_type=jnp.float32
    )
    routed = routed[:tokens] + routed[tokens:]
    shared_gate_out = jnp.dot(normed, shared_gate, preferred_element_type=jnp.float32)
    shared_up_out = jnp.dot(normed, shared_up, preferred_element_type=jnp.float32)
    shared_act = (jax.nn.silu(shared_gate_out) * shared_up_out).astype(jnp.bfloat16)
    shared_out = jnp.dot(shared_act, shared_down, preferred_element_type=jnp.float32)
    return (mixed + routed + shared_out).astype(jnp.bfloat16)


def solution(mesh):
    return jax.shard_map(
        local,
        mesh=mesh,
        in_specs=(
            P("sp", "tp"),
            P("sp", "tp"),
            P("sp", "tp"),
            P(("sp", "tp"), None),
            P(),
            P(),
            P(("sp", "tp"), None),
            P(("sp", "tp"), None),
            P("sp", None, "tp"),
            P("sp", None, "tp"),
            P("sp", "tp", None),
            P(),
            P(),
            P(),
        ),
        out_specs=P(("sp", "tp"), None),
        check_vma=False,
    )
```

time: 1790 us -> 444 us (0.25)
  blocking collectives: 1240 us -> 22.9 us
  other arithmetic: 93.2 us -> 2.44 us
  Pallas kernels: 0 us -> 68.2 us
  local copies, waits for them, and re-layouts: 105 us -> 41 us
  loops' own time: 36.9 us -> 0 us
  waiting for transfers between devices: 242 us -> 214 us
    all_to_all x2 -> x1, blocking collectives: 1240 us -> 22.9 us  [local(): lax.all_to_all(packed, 'sp', 0, 0, axis_index_groups=columns, tiled=True)]
    all_gather x2 -> x1, waiting for transfers between devices: 137 us -> 46.1 us  [local(): lax.all_gather(packed[:, :, LANES:], 'sp', axis_index_groups=planes, axis=0)]
    all_to_all x1 -> x3, waiting for transfers between devices: 82.4 us -> 168 us  [the longest x1 80.3 us: local(): lax.all_to_all(outgoing.reshape(experts, capacity, width), 'sp', 0, 0, ti...]
    pallas_call x0 -> x1, Pallas kernels: none -> 68.2 us  [attention(): pl.pallas_call(attention_kernel, out_shape=jax.ShapeDtypeStruct((4, side,...]
    another operation x7 -> x1, other arithmetic: 64.4 us -> 0.08 us  [local(): meta = jnp.stack([own, plane]).astype(jnp.int32)]
    another operation x17 -> x0, loops' own time: 36.9 us -> none  [the longest x16 20.4 us: turn(): partial_value, total = lax.cond(first_block <= own_block, compute, skipped)]
    gather x3 -> x0, local copies, waits for them, and re-layouts: 27.1 us -> none  [the longest x2 15.1 us: local(): normed[source_token]]
    reduce_scatter x1 -> x0, waiting for transfers between devices: 22.2 us -> none  [local(): lax.psum_scatter(pieces.astype(jnp.bfloat16), 'tp', scatter_dimension=0,...]
  transfers between devices with their start and end apart: 4 -> 7, of which waited for: 4 -> 4; matrix products, arithmetic and copies ran while one was open for 2% -> 8% of each run, Pallas kernels for 0% -> 0%
where the time goes in v1:
time: 444 us; the launch traced here: 438 us
  waiting for transfers between devices  214 us (48%)
  Pallas kernels  68.2 us (15%)
  matrix products  48.7 us (11%)
  local copies, waits for them, and re-layouts  41 us (9%)
  starting transfers between devices  27.3 us (6%)
  blocking collectives  22.9 us (5%)
  between operations  13.7 us (3%)
    all_to_all x1, waiting for transfers between devices, local(): lax.all_to_all(outgoing.reshape(experts, capacity, width), 'sp', 0, 0, ti...  80.3 us
    all_to_all x1, waiting for transfers between devices, local(): lax.all_to_all(result.astype(jnp.bfloat16).reshape(experts, capacity, wid...  77.5 us
    pallas_call x1, Pallas kernels, attention(): pl.pallas_call(attention_kernel, out_shape=jax.ShapeDtypeStruct((4, side,...  68.2 us
    all_gather x1, waiting for transfers between devices, local(): lax.all_gather(packed[:, :, LANES:], 'sp', axis_index_groups=planes, axis=0)  46.1 us
    dot_general x2, matrix products, half(): return jnp.dot(hidden, down_half[0], preferred_element_type=jnp.float32)  26.6 us
    all_to_all x1, blocking collectives, local(): lax.all_to_all(packed, 'sp', 0, 0, axis_index_groups=columns, tiled=True)  22.9 us
    all_to_all x1, starting transfers between devices, local(): lax.all_to_all(result.astype(jnp.bfloat16).reshape(experts, capacity, wid...  14.2 us
    all_to_all x1, waiting for transfers between devices, local(): lax.all_to_all(attended, ('sp', 'tp'), 0, 0, axis_index_groups=eights, ti...  9.89 us
  transfers between devices with their start and end apart: 7, of which 4 were waited for; matrix products, arithmetic and copies ran while one was open for 8% of the time, Pallas kernels for 0%

profile of v1, /device:TPU:0, one launch (start us, length us, event | category | flops | bytes accessed | tf_op | source)
XLA Modules:
  0.0 438.1 jit_solution(7317147392711615054)
XLA Ops:
  6.5 1.1 copy.51
  7.7 0.2 copy.52
  7.9 1.0 copy.53
  8.9 0.2 copy.54
  9.1 1.0 copy.55
  10.1 0.2 copy.56
  10.3 0.1 pad.3.clone
  10.4 0.2 pad_maximum_fusion
  10.6 22.9 %all_to_all.20 = bf16[4,256,256]{2,1,0:T(8,128)(2,1)S(1)} all-to-all(bf16[4,256,256]{2,1,0:T(8,128)(2,1)S(1)} %pad_maximum_fusion), channel_id=1, replica_groups={{0,62,64,126},{2,60,66,124},{4,58,68,122},{6,56,70,120},{8,54,72,118},{..., dimensions={0} | all-to-all | bytes 1048576 | tf_op jit(solution)/shard_map/all_to_all | solution.py:117
  33.5 0.8 fusion.54
  34.4 0.1 pad_add_fusion.meta_ref
  34.5 0.2 convolution_select_fusion
  34.7 46.1 %all-gather.3.cloned.1.call-done = bf16[64,256,128]{2,1,0:T(8,128)(2,1)} async-done(((bf16[4,256,128]{2,1,0:T(8,128)(2,1)}), bf16[64,256,128]{2,1,0:T(8,128)(2,1)}) %all-gather.3.cloned.1.call-update) | async-done | bytes 4194320 | tf_op jit(solution)/shard_map/all_gather | solution.py:118
  80.8 2.2 copy-done.2
  83.0 68.2 %attend.1 = bf16[4,256,128]{2,1,0:T(8,128)(2,1)S(1)} custom-call(s32[2]{0:T(128)S(1)} %pad_add_fusion.meta_ref, bf16[4,256,128]{2,1,0:T(8,128)(2,1)S(1)} %get-tuple-element.14.query_ref, bf16[16,4,256,128]{3,2,1,0:T(8,128)(2,1)S(1)} %bitcast.54), custom_call_target="tpu_custom_call" | custom-call | flops 13287555072 | bytes 6291456 | tf_op jit(solution)/shard_map/attend/pallas_call | solution.py:71
  151.2 0.1 slice.22
  151.3 0.8 copy.57
  152.1 6.6 %all-to-all-start.1 = ((bf16[8,128,64]{1,2,0:T(8,128)(2,1)}), bf16[8,128,64]{1,2,0:T(8,128)(2,1)S(1)}, u32[]{:S(2)}, u32[]{:S(2)}) async-start(bf16[8,128,64]{1,2,0:T(8,128)(2,1)} %copy.57), calls=%async_computation.1 | async-start | bytes 262144 | tf_op jit(solution)/shard_map/all_to_all | solution.py:130
  158.8 0.1 iota_compare_fusion
  158.9 9.9 %all-to-all-done.1 = bf16[8,128,64]{1,2,0:T(8,128)(2,1)S(1)} async-done(((bf16[8,128,64]{1,2,0:T(8,128)(2,1)}), bf16[8,128,64]{1,2,0:T(8,128)(2,1)S(1)}, u32[]{:S(2)}, u32[]{:S(2)}) %all-to-all-start.1) | async-done | bytes 131104 | tf_op jit(solution)/shard_map/all_to_all | solution.py:130
  168.8 1.6 multiply_reduce_fusion
  170.4 1.6 fusion.29
  172.0 5.6 %copy.60 = bf16[64,20,2048]{2,1,0:T(8,128)(2,1)} copy(bf16[64,20,2048]{2,0,1:T(8,128)(2,1)S(1)} %fusion.29) | data formatting | bytes 10485760 | tf_op jit(solution)/shard_map/dot_general | solution.py:148
  177.6 5.8 %all-to-all-start.2 = ((bf16[64,20,2048]{2,1,0:T(8,128)(2,1)}), bf16[64,20,2048]{2,1,0:T(8,128)(2,1)}, u32[]{:S(2)}, u32[]{:S(2)}) async-start(bf16[64,20,2048]{2,1,0:T(8,128)(2,1)} %copy.60), calls=%async_computation.2 | async-start | bytes 12582912 | tf_op jit(solution)/shard_map/all_to_all | solution.py:149
  183.4 0.1 collective-permute-start
  183.5 0.5 collective-permute-start.1
  184.0 0.1 collective-permute-start.2
  184.1 80.3 %all-to-all-done.2 = bf16[64,20,2048]{2,1,0:T(8,128)(2,1)} async-done(((bf16[64,20,2048]{2,1,0:T(8,128)(2,1)}), bf16[64,20,2048]{2,1,0:T(8,128)(2,1)}, u32[]{:S(2)}, u32[]{:S(2)}) %all-to-all-start.2) | async-done | bytes 5242912 | tf_op jit(solution)/shard_map/all_to_all | solution.py:149
  264.4 9.0 %reshape.60 = bf16[1280,2048]{1,0:T(8,128)(2,1)} reshape(bf16[64,20,2048]{2,1,0:T(8,128)(2,1)} %all-to-all-done.2) | data formatting | bytes 10485760 | tf_op jit(solution)/shard_map/reshape | solution.py:151
  273.4 5.2 %fusion.22 = f32[1280,256]{1,0:T(8,128)} fusion(bf16[1280,2048]{1,0:T(8,128)(2,1)} %reshape.60, bf16[1,2048,256]{2,1,0:T(8,128)(2,1)S(1)} %copy-done.8), kind=kOutput, calls=%fused_computation.27 | convolution fusion | flops 1342177280 | bytes 7602176 | tf_op jit(solution)/shard_map/dot_general | solution.py:154
  278.6 2.8 fusion.17
  281.4 12.8 %fusion.4 = f32[1280,2048]{1,0:T(8,128)} fusion(bf16[1280,2048]{1,0:T(8,128)(2,1)} %reshape.60, f32[1280,256]{1,0:T(8,128)} %fusion.22, bf16[1,256,2048]{2,1,0:T(8,128)(2,1)} %param.24, bf16[1,2048,256]{2,1,0:T(8,128)(2,1)} %param.23), kind=kOutput, calls=%fused_computation.8 | convolution fusion | flops 2686320640 | bytes 19136512 | tf_op jit(solution)/shard_map/dot_general | solution.py:157
  294.2 13.8 %add_convert_fusion = bf16[1280,2048]{1,0:T(8,128)(2,1)} fusion(f32[1280,2048]{1,0:T(8,128)} %fusion.4, bf16[1,256,2048]{2,1,0:T(8,128)(2,1)} %collective-permute-done.2, f32[1280,256]{1,0:T(8,128)S(1)} %fusion.17, bf16[1280,2048]{1,0:T(8,128)(2,1)} %reshape.60, bf16[1,2048,256]{2,1,0:T(8,128)(2,1)} %collective-permute-done.1), kind=kOutput, calls=%fused_computation | convolution fusion | flops 2691563520 | bytes 24379392 | tf_op jit(solution)/shard_map/dot_general | solution.py:157
  308.0 8.9 %reshape.61 = bf16[64,20,2048]{2,1,0:T(8,128)(2,1)} reshape(bf16[1280,2048]{1,0:T(8,128)(2,1)} %add_convert_fusion) | data formatting | bytes 10485760 | tf_op jit(solution)/shard_map/reshape | solution.py:161
  316.9 14.2 %all-to-all-start.3 = ((bf16[64,20,2048]{2,1,0:T(8,128)(2,1)}), bf16[64,20,2048]{2,1,0:T(8,128)(2,1)}, u32[]{:S(2)}, u32[]{:S(2)}) async-start(bf16[64,20,2048]{2,1,0:T(8,128)(2,1)} %reshape.61), calls=%async_computation.3 | async-start | bytes 12582912 | tf_op jit(solution)/shard_map/all_to_all | solution.py:160
  331.1 0.1 eq.49
  331.2 0.1 eq.50
  331.3 0.6 copy-done.7
  331.8 0.1 broadcast_in_dim.54
  331.9 0.1 broadcast_in_dim.55
  332.0 0.1 eq.52
  332.1 1.0 fusion.41
  333.1 1.0 subtract_convert_fusion
  334.0 0.5 fusion.53
  334.5 77.5 %all-to-all-done.3 = bf16[64,20,2048]{2,1,0:T(8,128)(2,1)} async-done(((bf16[64,20,2048]{2,1,0:T(8,128)(2,1)}), bf16[64,20,2048]{2,1,0:T(8,128)(2,1)}, u32[]{:S(2)}, u32[]{:S(2)}) %all-to-all-start.3) | async-done | bytes 5242912 | tf_op jit(solution)/shard_map/all_to_all | solution.py:160
  412.0 9.0 %reshape.62 = bf16[1280,2048]{1,0:T(8,128)(2,1)} reshape(bf16[64,20,2048]{2,1,0:T(8,128)(2,1)} %all-to-all-done.3) | data formatting | bytes 10485760 | tf_op jit(solution)/shard_map/reshape | solution.py:162
  421.0 5.7 %fusion.24 = f32[256,2048]{1,0:T(8,128)} fusion(bf16[1280,2048]{1,0:T(8,128)(2,1)} %reshape.62, bf16[1280,128]{1,0:T(8,128)(2,1)} %subtract_convert_fusion, bf16[1280,128]{1,0:T(8,128)(2,1)} %fusion.41), kind=kOutput, calls=%fused_computation.32 | convolution fusion | flops 1343488000 | bytes 7995392 | tf_op jit(solution)/shard_map/dot_general | solution.py:167
  426.7 4.5 %fusion.3 = bf16[128,2048]{1,0:T(8,128)(2,1)} fusion(bf16[512,2048]{1,0:T(8,128)(2,1)} %param.27, bf16[2048,512]{1,0:T(8,128)(2,1)} %param.26, f32[128,2048]{1,0:T(8,128)S(1)} %get-tuple-element.16, f32[256,2048]{1,0:T(8,128)} %fusion.24, f32[128,512]{1,0:T(8,128)S(1)} %fusion.53, f32[2048]{0:T(1024)S(1)} %copy-done.5, f32[128]{0:T(128)S(1)} %add_rsqrt_fusion), kind=kOutput, calls=%fused_computation.7 | convolution fusion | flops 539099136 | bytes 9183744 | tf_op jit(solution)/shard_map/dot_general | solution.py:174
  (28 shorter events, 0.2 us)
Async XLA Ops:
  6.5 162.3 %copy-start = (bf16[512,2048]{1,0:T(8,128)(2,1)S(1)}, bf16[512,2048]{1,0:T(8,128)(2,1)}, u32[]{:S(2)}) copy-start(bf16[512,2048]{1,0:T(8,128)(2,1)} %param.18) | copy-start | bytes 6291460
  6.5 74.3 %all-gather.3.cloned.1.call-start = ((), (), s32[]{:S(2)}) async-start(), calls=%async_computation.4 | async-start | bytes 4456448 | tf_op jit(solution)/shard_map/all_gather | solution.py:118
  10.1 24.4 %copy-start.6 = (s32[128,8]{0,1:T(8,128)S(1)}, s32[128,8]{0,1:T(8,128)}, u32[]{:S(2)}) copy-start(s32[128,8]{0,1:T(8,128)} %param.20) | copy-start | bytes 12292
  80.8 2.2 copy-start.2
  152.1 16.7 %all-to-all-start.1 = ((bf16[8,128,64]{1,2,0:T(8,128)(2,1)}), bf16[8,128,64]{1,2,0:T(8,128)(2,1)S(1)}, u32[]{:S(2)}, u32[]{:S(2)}) async-start(bf16[8,128,64]{1,2,0:T(8,128)(2,1)} %copy.57), calls=%async_computation.1 | async-start | bytes 262144 | tf_op jit(solution)/shard_map/all_to_all | solution.py:130
  158.8 11.7 %copy-start.5 = (f32[2048]{0:T(1024)S(1)}, f32[2048]{0:T(1024)}, u32[]{:S(2)}) copy-start(f32[2048]{0:T(1024)} %param.19) | copy-start | bytes 24580
  177.6 5.8 %copy-start.8 = (bf16[1,2048,256]{2,1,0:T(8,128)(2,1)S(1)}, bf16[1,2048,256]{2,1,0:T(8,128)(2,1)}, u32[]{:S(2)}) copy-start(bf16[1,2048,256]{2,1,0:T(8,128)(2,1)} %param.22) | copy-start | bytes 3145732
  177.6 86.8 %all-to-all-start.2 = ((bf16[64,20,2048]{2,1,0:T(8,128)(2,1)}), bf16[64,20,2048]{2,1,0:T(8,128)(2,1)}, u32[]{:S(2)}, u32[]{:S(2)}) async-start(bf16[64,20,2048]{2,1,0:T(8,128)(2,1)} %copy.60), calls=%async_computation.2 | async-start | bytes 12582912 | tf_op jit(solution)/shard_map/all_to_all | solution.py:149
  183.4 95.2 %collective-permute-start = (bf16[1,2048,256]{2,1,0:T(8,128)(2,1)S(1)}, bf16[1,2048,256]{2,1,0:T(8,128)(2,1)}, u32[]{:S(2)}, u32[]{:S(2)}) collective-permute-start(bf16[1,2048,256]{2,1,0:T(8,128)(2,1)S(1)} %copy-done.8), channel_id=1, source_target_pairs={{0,1},{1,0},{2,3},{3,2},{4,5},{5,4},{6,7},{7,6},{8,9},{9,8},{10,11... | collective-permute-start | bytes 3145736 | tf_op jit(solution)/shard_map/ppermute | solution.py:123
  183.5 110.7 %collective-permute-start.1 = (bf16[1,2048,256]{2,1,0:T(8,128)(2,1)}, bf16[1,2048,256]{2,1,0:T(8,128)(2,1)}, u32[]{:S(2)}, u32[]{:S(2)}) collective-permute-start(bf16[1,2048,256]{2,1,0:T(8,128)(2,1)} %param.23), channel_id=1, source_target_pairs={{0,1},{1,0},{2,3},{3,2},{4,5},{5,4},{6,7},{7,6},{8,9},{9,8},{10,11... | collective-permute-start | bytes 3145736 | tf_op jit(solution)/shard_map/ppermute | solution.py:124
  184.0 110.2 %collective-permute-start.2 = (bf16[1,256,2048]{2,1,0:T(8,128)(2,1)}, bf16[1,256,2048]{2,1,0:T(8,128)(2,1)}, u32[]{:S(2)}, u32[]{:S(2)}) collective-permute-start(bf16[1,256,2048]{2,1,0:T(8,128)(2,1)} %param.24), channel_id=1, source_target_pairs={{0,1},{1,0},{2,3},{3,2},{4,5},{5,4},{6,7},{7,6},{8,9},{9,8},{10,11... | collective-permute-start | bytes 3145736 | tf_op jit(solution)/shard_map/ppermute | solution.py:125
  273.4 5.2 %copy-start.3 = (bf16[1280,2048]{1,0:T(8,128)(2,1)S(1)}, bf16[1280,2048]{1,0:T(8,128)(2,1)}, u32[]{:S(2)}) copy-start(bf16[1280,2048]{1,0:T(8,128)(2,1)} %reshape.60) | copy-start | bytes 15728644
  316.9 95.1 %all-to-all-start.3 = ((bf16[64,20,2048]{2,1,0:T(8,128)(2,1)}), bf16[64,20,2048]{2,1,0:T(8,128)(2,1)}, u32[]{:S(2)}, u32[]{:S(2)}) async-start(bf16[64,20,2048]{2,1,0:T(8,128)(2,1)} %reshape.61), calls=%async_computation.3 | async-start | bytes 12582912 | tf_op jit(solution)/shard_map/all_to_all | solution.py:160
  331.1 0.7 copy-start.7
  332.1 2.0 copy-start.4
  421.0 10.2 %copy-start.1 = (bf16[512,2048]{1,0:T(8,128)(2,1)S(1)}, bf16[512,2048]{1,0:T(8,128)(2,1)}, u32[]{:S(2)}) copy-start(bf16[512,2048]{1,0:T(8,128)(2,1)} %param.18) | copy-start | bytes 6291460
Sparse Core Ops, SparseCore 0:
  34.4 46.3 all-gather.2

commit v2 on v1

--- a/solution.py
+++ b/solution.py
@@ -80,6 +80,184 @@
         ),
         name="attend",
     )(meta, query, kv)
+
+
+MAIN = 16
+TAIL = 4
+
+
+def dispatch_kernel(
+    attended_ref, residual_ref, weight_ref, gain_ref, main_ref, tail_ref, mixed_ref, normed_ref, out_ref
+):
+    half = out_ref.shape[2]
+
+    @pl.when(pl.program_id(0) == 0)
+    def _():
+        projected = jnp.dot(attended_ref[...], weight_ref[...], preferred_element_type=jnp.float32)
+        mixed = (residual_ref[...].astype(jnp.float32) + projected).astype(jnp.bfloat16)
+        mixed_ref[...] = mixed
+        mixed = mixed.astype(jnp.float32)
+        inverse = lax.rsqrt(jnp.mean(mixed * mixed, axis=1, keepdims=True) + norm_eps)
+        normed_ref[...] = (mixed * inverse * gain_ref[...]).astype(jnp.bfloat16)
+
+    left, right = normed_ref[:, :half], normed_ref[:, half:]
+    experts = out_ref.shape[0]
+    main, tail = main_ref[...], tail_ref[...]
+
+    def pick(rows, side):
+        return jnp.dot(rows, side, preferred_element_type=jnp.float32)
+
+    out_ref[:, 0:MAIN, :] = pick(main, left).astype(jnp.bfloat16).reshape(experts, MAIN, half)
+    out_ref[:, MAIN : 2 * MAIN, :] = pick(main, right).astype(jnp.bfloat16).reshape(experts, MAIN, half)
+    first = lax.broadcasted_iota(jnp.int32, (tail.shape[0], half), 0) % (2 * TAIL) < TAIL
+    both = jnp.where(first, pick(tail, left), pick(tail, right))
+    out_ref[:, 2 * MAIN :, :] = both.astype(jnp.bfloat16).reshape(experts, 2 * TAIL, half)
+
+
+def dispatch(attended, residual, out_weight, gain, main, tail):
+    tokens, width = residual.shape
+    experts = main.shape[0] // MAIN
+    step = 16
+    whole = lambda i: (0, 0)
+    return pl.pallas_call(
+        dispatch_kernel,
+        grid=(experts // step,),
+        in_specs=[
+            pl.BlockSpec(attended.shape, whole),
+            pl.BlockSpec(residual.shape, whole),
+            pl.BlockSpec(out_weight.shape, whole),
+            pl.BlockSpec(gain.shape, whole),
+            pl.BlockSpec((step * MAIN, tokens), lambda i: (i, 0)),
+            pl.BlockSpec((step * 2 * TAIL, tokens), lambda i: (i, 0)),
+        ],
+        out_specs=[
+            pl.BlockSpec((tokens, width), whole),
+            pl.BlockSpec((tokens, width), whole),
+            pl.BlockSpec((step, 2 * (MAIN + TAIL), width // 2), lambda i: (i, 0, 0)),
+        ],
+        out_shape=[
+            jax.ShapeDtypeStruct((tokens, width), jnp.bfloat16),
+            jax.ShapeDtypeStruct((tokens, width), jnp.bfloat16),
+            jax.ShapeDtypeStruct((experts, 2 * (MAIN + TAIL), width // 2), jnp.bfloat16),
+        ],
+        compiler_params=pltpu.CompilerParams(vmem_limit_bytes=32 * 2**20),
+        cost_estimate=pl.CostEstimate(flops=10**9, bytes_accessed=10**7, transcendentals=0),
+        name="dispatch",
+    )(attended, residual, out_weight, gain, main, tail)
+
+
+def expert_kernel(
+    rows_ref, gate0_ref, up0_ref, down0_ref, gate1_ref, up1_ref, down1_ref, out_ref, spread_ref, rows2_ref
+):
+    sources, _, half = rows_ref.shape
+    tails = sources * TAIL
+
+    @pl.when(pl.program_id(0) == 0)
+    def _():
+        row = lax.broadcasted_iota(jnp.int32, (2 * tails, 2 * tails), 0)
+        col = lax.broadcasted_iota(jnp.int32, (2 * tails, 2 * tails), 1)
+        slot = row % tails
+        home = slot // TAIL * (2 * TAIL) + row // tails * TAIL + slot % TAIL
+        spread_ref[...] = (home == col).astype(jnp.bfloat16)
+
+    spread = spread_ref[...]
+    mains = sources * MAIN
+    rows2_ref[:mains, :half] = rows_ref[:, 0:MAIN, :].reshape(mains, half)
+    rows2_ref[:mains, half:] = rows_ref[:, MAIN : 2 * MAIN, :].reshape(mains, half)
+    ends = jnp.dot(
+        spread, rows_ref[:, 2 * MAIN :, :].reshape(2 * tails, half), preferred_element_type=jnp.float32
+    ).astype(jnp.bfloat16)
+    rows2_ref[mains:, :half] = ends[:tails]
+    rows2_ref[mains:, half:] = ends[tails:]
+    rows = rows2_ref[...]
+
+    def hidden(gate_ref, up_ref):
+        gate = jnp.dot(rows, gate_ref[0], preferred_element_type=jnp.float32)
+        upward = jnp.dot(rows, up_ref[0], preferred_element_type=jnp.float32)
+        return (jax.nn.silu(gate) * upward).astype(jnp.bfloat16)
+
+    act0 = hidden(gate0_ref, up0_ref)
+    act1 = hidden(gate1_ref, up1_ref)
+    for part in range(2):
+        span = pl.ds(part * half, half)
+        result = jnp.dot(act0, down0_ref[0, :, span], preferred_element_type=jnp.float32) + jnp.dot(
+            act1, down1_ref[0, :, span], preferred_element_type=jnp.float32
+        )
+        result = result.astype(jnp.bfloat16)
+        out_ref[:, part * MAIN : (part + 1) * MAIN, :] = result[:mains].reshape(sources, MAIN, half)
+        if part == 0:
+            first = result[mains:]
+        else:
+            ends = jnp.concatenate([first, result[mains:]], axis=0)
+            ends = lax.dot_general(
+                spread, ends, (((0,), (0,)), ((), ())), preferred_element_type=jnp.float32
+            )
+            out_ref[:, 2 * MAIN :, :] = ends.astype(jnp.bfloat16).reshape(sources, 2 * TAIL, half)
+
+
+def expert(rows, mine, other):
+    step = 16
+    whole = [pl.BlockSpec(memory_space=pltpu.VMEM)] * 6
+    block = pl.BlockSpec((step,) + rows.shape[1:], lambda i: (i, 0, 0))
+    return pl.pallas_call(
+        expert_kernel,
+        grid=(rows.shape[0] // step,),
+        in_specs=[block] + whole,
+        out_specs=block,
+        out_shape=jax.ShapeDtypeStruct(rows.shape, jnp.bfloat16),
+        scratch_shapes=[
+            pltpu.VMEM((step * 2 * TAIL, step * 2 * TAIL), jnp.bfloat16),
+            pltpu.VMEM((step * (MAIN + TAIL), 2 * rows.shape[2]), jnp.bfloat16),
+        ],
+        compiler_params=pltpu.CompilerParams(vmem_limit_bytes=32 * 2**20),
+        cost_estimate=pl.CostEstimate(flops=8 * 10**9, bytes_accessed=17 * 10**6, transcendentals=10**6),
+        name="expert",
+    )(rows, *mine, *other)
+
+
+def combine_kernel(rows_ref, main_ref, left_ref, right_ref, base_ref, out_ref, acc_ref):
+    sources, _, half = rows_ref.shape
+    tokens = base_ref.shape[0]
+    at = pl.program_id(0)
+
+    @pl.when(at == 0)
+    def _():
+        acc_ref[...] = base_ref[...]
+
+    ends = rows_ref[:, 2 * MAIN :, :].reshape(sources * 2 * TAIL, half)
+    for part, tail_ref in ((0, left_ref), (1, right_ref)):
+        rows = rows_ref[:, part * MAIN : (part + 1) * MAIN, :].reshape(sources * MAIN, half)
+        total = jnp.dot(main_ref[...], rows, preferred_element_type=jnp.float32) + jnp.dot(
+            tail_ref[...], ends, preferred_element_type=jnp.float32
+        )
+        span = pl.ds(part * half, half)
+        acc_ref[:, span] += total[:tokens] + total[tokens:]
+
+    @pl.when(at == pl.num_programs(0) - 1)
+    def _():
+        out_ref[...] = acc_ref[...].astype(jnp.bfloat16)
+
+
+def combine(rows, main, left, right, base):
+    step = 16
+    whole = lambda i: (0, 0)
+    return pl.pallas_call(
+        combine_kernel,
+        grid=(rows.shape[0] // step,),
+        in_specs=[
+            pl.BlockSpec((step,) + rows.shape[1:], lambda i: (i, 0, 0)),
+            pl.BlockSpec((main.shape[0], step * MAIN), lambda i: (0, i)),
+            pl.BlockSpec((main.shape[0], step * 2 * TAIL), lambda i: (0, i)),
+            pl.BlockSpec((main.shape[0], step * 2 * TAIL), lambda i: (0, i)),
+            pl.BlockSpec(base.shape, whole),
+        ],
+        out_specs=pl.BlockSpec(base.shape, whole),
+        out_shape=jax.ShapeDtypeStruct(base.shape, jnp.bfloat16),
+        scratch_shapes=[pltpu.VMEM(base.shape, jnp.float32)],
+        compiler_params=pltpu.CompilerParams(vmem_limit_bytes=32 * 2**20),
+        cost_estimate=pl.CostEstimate(flops=10**9, bytes_accessed=10**7, transcendentals=0),
+        name="combine",
+    )(rows, main, left, right, base)
 
 
 def local(
@@ -130,49 +308,45 @@
     attended = lax.all_to_all(attended, ("sp", "tp"), 0, 0, axis_index_groups=eights, tiled=True)
     attended = attended.reshape(4, 2, tokens, HEAD_DIM).transpose(2, 1, 0, 3).reshape(tokens, 512)
 
-    projected = jnp.dot(attended, out_weight, preferred_element_type=jnp.float32)
-    mixed = (residual.astype(jnp.float32) + projected).astype(jnp.bfloat16).astype(jnp.float32)
-    inverse = lax.rsqrt(jnp.mean(mixed * mixed, axis=1, keepdims=True) + norm_eps)
-    normed = (mixed * inverse * norm_gain).astype(jnp.bfloat16)
-    width = normed.shape[1]
     experts = lax.axis_size("sp")
-    capacity = 20
     named = routes[:, :, None] == jnp.arange(experts, dtype=jnp.int32)
     pick = jnp.any(named, axis=1)
     share = jnp.sum(jnp.where(named, route_weight[:, :, None], 0.0), axis=1)
     below = jnp.tril(jnp.ones((tokens, tokens), jnp.bfloat16), -1)
     rank = jnp.dot(below, pick.astype(jnp.bfloat16), preferred_element_type=jnp.float32)
-    rank = jnp.where(pick, rank, -1.0).T
-    slot = rank[:, None, :] == jnp.arange(capacity, dtype=jnp.float32)[None, :, None]
-    send = slot.astype(jnp.bfloat16).reshape(experts * capacity, tokens)
-    outgoing = jnp.dot(send, normed, preferred_element_type=jnp.bfloat16)
-    incoming = lax.all_to_all(
-        outgoing.reshape(experts, capacity, width), "sp", 0, 0, tiled=True
-    ).reshape(experts * capacity, width)
-
-    def half(gate_half, up_half, down_half):
-        gate = jnp.dot(incoming, gate_half[0], preferred_element_type=jnp.float32)
-        upward = jnp.dot(incoming, up_half[0], preferred_element_type=jnp.float32)
-        hidden = (jax.nn.silu(gate) * upward).astype(jnp.bfloat16)
-        return jnp.dot(hidden, down_half[0], preferred_element_type=jnp.float32)
-
-    result = half(expert_gate, expert_up, expert_down) + half(gate_other, up_other, down_other)
-    returned = lax.all_to_all(
-        result.astype(jnp.bfloat16).reshape(experts, capacity, width), "sp", 0, 0, tiled=True
-    ).reshape(experts * capacity, width)
-    weighted = jnp.where(slot, share.T[:, None, :], 0.0).reshape(experts * capacity, tokens)
-    high = weighted.astype(jnp.bfloat16)
-    low = (weighted - high.astype(jnp.float32)).astype(jnp.bfloat16)
-    both = jnp.concatenate([high, low], axis=1)
-    routed = lax.dot_general(
-        both, returned, (((0,), (0,)), ((), ())), preferred_element_type=jnp.float32
-    )
-    routed = routed[:tokens] + routed[tokens:]
+    rank = jnp.where(pick, rank, -1.0).astype(jnp.int32)
+
+    def slots(numbers):
+        numbers = jnp.asarray(numbers, jnp.int32)
+        send = rank.T[:, None, :] == numbers[None, :, None]
+        back = rank[:, :, None] == numbers[None, None, :]
+        send = send.astype(jnp.bfloat16).reshape(-1, tokens)
+        weight = jnp.where(back, share[:, :, None], 0.0).reshape(tokens, -1)
+        high = weight.astype(jnp.bfloat16)
+        low = (weight - high.astype(jnp.float32)).astype(jnp.bfloat16)
+        return send, jnp.concatenate([high, low], axis=0)
+
+    ends = list(range(MAIN, MAIN + TAIL))
+    none = [-2] * TAIL
+    send_main, back_main = slots(list(range(MAIN)))
+    send_tail, _ = slots(ends + ends)
+    _, back_left = slots(ends + none)
+    _, back_right = slots(none + ends)
+    mixed, normed, outgoing = dispatch(
+        attended, residual, out_weight, norm_gain[None, :], send_main, send_tail
+    )
+    incoming = lax.all_to_all(outgoing, "sp", 0, 0, tiled=True)
     shared_gate_out = jnp.dot(normed, shared_gate, preferred_element_type=jnp.float32)
     shared_up_out = jnp.dot(normed, shared_up, preferred_element_type=jnp.float32)
     shared_act = (jax.nn.silu(shared_gate_out) * shared_up_out).astype(jnp.bfloat16)
-    shared_out = jnp.dot(shared_act, shared_down, preferred_element_type=jnp.float32)
-    return (mixed + routed + shared_out).astype(jnp.bfloat16)
+    base = mixed.astype(jnp.float32) + jnp.dot(
+        shared_act, shared_down, preferred_element_type=jnp.float32
+    )
+    result = expert(
+        incoming, (expert_gate, expert_up, expert_down), (gate_other, up_other, down_other)
+    )
+    returned = lax.all_to_all(result, "sp", 0, 0, tiled=True)
+    return combine(returned, back_main, back_left, back_right, base)
 
 
 def solution(mesh):

time: 444 us -> 367 us (0.83)
  matrix products: 48.7 us -> 4.09 us
  waiting for transfers between devices: 214 us -> 172 us
  Pallas kernels: 68.2 us -> 88.3 us
  local copies, waits for them, and re-layouts: 41 us -> 34.7 us
    all_to_all x2, waiting for transfers between devices: 158 us -> 113 us  [the longest x1 59.4 us: local(): incoming = lax.all_to_all(outgoing, 'sp', 0, 0, tiled=True)]
    dot_general x7 -> x0, matrix products: 43.5 us -> none  [the longest x2 26.6 us: half(): return jnp.dot(hidden, down_half[0], preferred_element_type=jnp.float32)]
    reshape x3 -> x1, local copies, waits for them, and re-layouts: 26.9 us -> 0.11 us  [local(): attended.reshape(4, 2, tokens, HEAD_DIM).transpose(2, 1, 0, 3)]
    pallas_call x0 -> x3, Pallas kernels: none -> 20.1 us  [the longest x1 11.4 us: expert(): pl.pallas_call(expert_kernel, grid=(rows.shape[0] // step,), in_specs=[bl...]
    unnamed x21 -> x57, local copies, waits for them, and re-layouts: 5.94 us -> 26 us
    dot_general x1 -> x0, local copies, waits for them, and re-layouts: 5.57 us -> none  [local(): outgoing = jnp.dot(send, normed, preferred_element_type=jnp.bfloat16)]
  transfers between devices with their start and end apart: 7 -> 7, of which waited for: 4 -> 7; matrix products, arithmetic and copies ran while one was open for 8% -> 4% of each run, Pallas kernels for 0% -> 0%
where the time goes in v2:
time: 367 us; the launch traced here: 365 us
  waiting for transfers between devices  172 us (47%)
  Pallas kernels  88.3 us (24%)
  local copies, waits for them, and re-layouts  34.7 us (9%)
  starting transfers between devices  24.9 us (7%)
  blocking collectives  22.9 us (6%)
  between operations  13.8 us (4%)
  other arithmetic  4.69 us (1%)
  matrix products  4.09 us (1%)
    pallas_call x1, Pallas kernels, attention(): pl.pallas_call(attention_kernel, out_shape=jax.ShapeDtypeStruct((4, side,...  68.2 us
    all_to_all x1, waiting for transfers between devices, local(): incoming = lax.all_to_all(outgoing, 'sp', 0, 0, tiled=True)  59.4 us
    all_to_all x1, waiting for transfers between devices, local(): returned = lax.all_to_all(result, 'sp', 0, 0, tiled=True)  53.4 us
    all_gather x1, waiting for transfers between devices, local(): lax.all_gather(packed[:, :, LANES:], 'sp', axis_index_groups=planes, axis=0)  45.7 us
    unnamed x57, local copies, waits for them, and re-layouts  26 us
    all_to_all x1, blocking collectives, local(): lax.all_to_all(packed, 'sp', 0, 0, axis_index_groups=columns, tiled=True)  22.9 us
    all_to_all x1, starting transfers between devices, local(): returned = lax.all_to_all(result, 'sp', 0, 0, tiled=True)  11.9 us
    pallas_call x1, Pallas kernels, expert(): pl.pallas_call(expert_kernel, grid=(rows.shape[0] // step,), in_specs=[bl...  11.4 us
  transfers between devices with their start and end apart: 7, of which 7 were waited for; matrix products, arithmetic and copies ran while one was open for 4% of the time, Pallas kernels for 0%

profile of v2, /device:TPU:0, one launch (start us, length us, event | category | flops | bytes accessed | tf_op | source)
XLA Modules:
  0.0 365.0 jit_solution(886309845417267741)
XLA Ops:
  6.5 1.1 copy.57
  7.9 1.0 copy.59
  9.1 1.0 copy.61
  10.6 22.9 %all_to_all.20 = bf16[4,256,256]{2,1,0:T(8,128)(2,1)S(1)} all-to-all(bf16[4,256,256]{2,1,0:T(8,128)(2,1)S(1)} %pad_maximum_fusion), channel_id=1, replica_groups={{0,62,64,126},{2,60,66,124},{4,58,68,122},{6,56,70,120},{8,54,72,118},{..., dimensions={0} | all-to-all | bytes 1048576 | tf_op jit(solution)/shard_map/all_to_all | solution.py:295
  33.5 0.8 fusion.22
  35.1 45.7 %all-gather.3.cloned.1.call-done = bf16[64,256,128]{2,1,0:T(8,128)(2,1)} async-done(((bf16[4,256,128]{2,1,0:T(8,128)(2,1)}), bf16[64,256,128]{2,1,0:T(8,128)(2,1)}) %all-gather.3.cloned.1.call-update) | async-done | bytes 4194320 | tf_op jit(solution)/shard_map/all_gather | solution.py:296
  80.8 2.2 copy-done.7
  83.0 68.2 %attend.1 = bf16[4,256,128]{2,1,0:T(8,128)(2,1)S(1)} custom-call(s32[2]{0:T(128)S(1)} %pad_add_fusion.meta_ref, bf16[4,256,128]{2,1,0:T(8,128)(2,1)S(1)} %get-tuple-element.24.query_ref, bf16[16,4,256,128]{3,2,1,0:T(8,128)(2,1)S(1)} %bitcast.36), custom_call_target="tpu_custom_call" | custom-call | flops 13287555072 | bytes 6291456 | tf_op jit(solution)/shard_map/attend/pallas_call | solution.py:71
  151.3 0.8 copy.63
  152.1 6.6 %all-to-all-start.1 = ((bf16[8,128,64]{1,2,0:T(8,128)(2,1)}), bf16[8,128,64]{1,2,0:T(8,128)(2,1)S(1)}, u32[]{:S(2)}, u32[]{:S(2)}) async-start(bf16[8,128,64]{1,2,0:T(8,128)(2,1)} %copy.63), calls=%async_computation.1 | async-start | bytes 262144 | tf_op jit(solution)/shard_map/all_to_all | solution.py:308
  158.9 9.9 %all-to-all-done.1 = bf16[8,128,64]{1,2,0:T(8,128)(2,1)S(1)} async-done(((bf16[8,128,64]{1,2,0:T(8,128)(2,1)}), bf16[8,128,64]{1,2,0:T(8,128)(2,1)S(1)}, u32[]{:S(2)}, u32[]{:S(2)}) %all-to-all-start.1) | async-done | bytes 131104 | tf_op jit(solution)/shard_map/all_to_all | solution.py:308
  168.9 1.6 copy-done.8
  170.5 1.0 copy-done.18
  171.6 2.9 dispatch.1
  174.5 2.4 copy-done.2
  176.9 0.8 copy-done.6
  177.7 5.7 %all-to-all-start.2 = ((bf16[64,40,1024]{2,1,0:T(8,128)(2,1)}), bf16[64,40,1024]{2,1,0:T(8,128)(2,1)}, u32[]{:S(2)}, u32[]{:S(2)}) async-start(bf16[64,40,1024]{2,1,0:T(8,128)(2,1)} %copy-done.2), calls=%async_computation.2 | async-start | bytes 10485760 | tf_op jit(solution)/shard_map/all_to_all | solution.py:338
  183.5 0.5 collective-permute-start.1
  184.1 2.3 collective-permute-done.gate1_ref
  186.4 1.0 copy-done.12
  187.3 0.5 collective-permute-done.1.up1_ref
  187.9 1.0 copy-done.14
  189.4 1.0 copy-done.16
  190.3 59.4 %all-to-all-done.2.rows_ref = bf16[64,40,1024]{2,1,0:T(8,128)(2,1)} async-done(((bf16[64,40,1024]{2,1,0:T(8,128)(2,1)}), bf16[64,40,1024]{2,1,0:T(8,128)(2,1)}, u32[]{:S(2)}, u32[]{:S(2)}) %all-to-all-start.2) | async-done | bytes 5242912 | tf_op jit(solution)/shard_map/all_to_all | solution.py:338
  249.7 1.2 copy-done.9
  251.0 1.2 copy-done.10
  252.2 1.2 copy-done.11
  253.4 1.2 copy-done.13
  254.6 1.2 copy-done.15
  255.9 1.2 copy-done.17
  257.1 11.4 %expert.1 = bf16[64,40,1024]{2,1,0:T(8,128)(2,1)S(1)} custom-call(bf16[64,40,1024]{2,1,0:T(8,128)(2,1)} %all-to-all-done.2.rows_ref, bf16[1,2048,256]{2,1,0:T(8,128)(2,1)S(1)} %copy-done.9, bf16[1,2048,256]{2,1,0:T(8,128)(2,1)S(1)} %copy-done.10, bf16[1,256,2048]{2,1,0:T(8,128)(2,1)S(1)} %copy-done.11, bf16[1,2048,256]{2,1,0:T(8,128)(2,1)S(1)} %copy-done.13, ...), custom_call_target="tpu_custom_call" | custom-call | flops 8000000000 | bytes 17000000 | tf_op jit(solution)/shard_map/expert/pallas_call | solution.py:202
  268.5 2.4 copy-done.1
  270.9 11.9 %all-to-all-start.3 = ((bf16[64,40,1024]{2,1,0:T(8,128)(2,1)}), bf16[64,40,1024]{2,1,0:T(8,128)(2,1)}, u32[]{:S(2)}, u32[]{:S(2)}) async-start(bf16[64,40,1024]{2,1,0:T(8,128)(2,1)} %copy-done.1), calls=%async_computation.3 | async-start | bytes 10485760 | tf_op jit(solution)/shard_map/all_to_all | solution.py:348
  283.0 0.8 copy.69
  284.1 0.8 eq.127
  284.9 1.2 copy.66
  286.2 0.8 broadcast_in_dim.84
  287.0 2.0 copy.67
  289.0 1.1 fusion.10
  290.2 1.1 subtract_convert_fusion
  291.3 0.8 pad_maximum_fusion.1.main_ref
  292.3 0.7 pad_maximum_fusion.2
  293.1 1.2 fusion.23
  294.2 2.7 convolution_add_fusion.base_ref
  297.0 53.4 %all-to-all-done.3.rows_ref = bf16[64,40,1024]{2,1,0:T(8,128)(2,1)} async-done(((bf16[64,40,1024]{2,1,0:T(8,128)(2,1)}), bf16[64,40,1024]{2,1,0:T(8,128)(2,1)}, u32[]{:S(2)}, u32[]{:S(2)}) %all-to-all-start.3) | async-done | bytes 5242912 | tf_op jit(solution)/shard_map/all_to_all | solution.py:348
  350.4 1.0 copy-done.4
  351.5 0.9 copy-done.5
  352.4 5.8 %combine.1 = bf16[128,2048]{1,0:T(8,128)(2,1)} custom-call(bf16[64,40,1024]{2,1,0:T(8,128)(2,1)} %all-to-all-done.3.rows_ref, bf16[256,1024]{1,0:T(8,128)(2,1)S(1)} %copy-done.4, bf16[256,512]{1,0:T(8,128)(2,1)S(1)} %get-tuple-element.25.left_ref, bf16[256,512]{1,0:T(8,128)(2,1)S(1)} %copy-done.5, f32[128,2048]{1,0:T(8,128)S(1)} %convolution_add_fusion.base_ref), custom_call_target="tpu_custom_call" | custom-call | flops 1000000000 | bytes 10000000 | tf_op jit(solution)/shard_map/combine/pallas_call | solution.py:244
  (71 shorter events, 3.2 us)
Async XLA Ops:
  6.5 287.7 %copy-start = (bf16[512,2048]{1,0:T(8,128)(2,1)S(1)}, bf16[512,2048]{1,0:T(8,128)(2,1)}, u32[]{:S(2)}) copy-start(bf16[512,2048]{1,0:T(8,128)(2,1)} %param.31) | copy-start | bytes 6291460
  6.5 74.3 %all-gather.3.cloned.1.call-start = ((), (), s32[]{:S(2)}) async-start(), calls=%async_computation.4 | async-start | bytes 4456448 | tf_op jit(solution)/shard_map/all_gather | solution.py:296
  10.1 24.4 %copy-start.26 = (s32[8]{0:T(128)S(1)}, s32[8]{0:T(128)}, u32[]{:S(2)}) copy-start(s32[8]{0:T(128)} %constant.68.clone) | copy-start | bytes 100
  10.1 24.5 %copy-start.22 = (s32[128,8]{0,1:T(8,128)S(1)}, s32[128,8]{0,1:T(8,128)}, u32[]{:S(2)}) copy-start(s32[128,8]{0,1:T(8,128)} %param.24) | copy-start | bytes 12292
  80.8 2.2 copy-start.7
  83.0 85.9 %copy-start.19 = (f32[2048]{0:T(1024)S(1)}, f32[2048]{0:T(1024)}, u32[]{:S(2)}) copy-start(f32[2048]{0:T(1024)} %param.23) | copy-start | bytes 24580
  152.1 16.7 %all-to-all-start.1 = ((bf16[8,128,64]{1,2,0:T(8,128)(2,1)}), bf16[8,128,64]{1,2,0:T(8,128)(2,1)S(1)}, u32[]{:S(2)}, u32[]{:S(2)}) async-start(bf16[8,128,64]{1,2,0:T(8,128)(2,1)} %copy.63), calls=%async_computation.1 | async-start | bytes 262144 | tf_op jit(solution)/shard_map/all_to_all | solution.py:308
  168.9 1.6 copy-start.8
  170.5 1.0 copy-start.18
  174.5 2.4 copy-start.2
  176.9 0.8 copy-start.6
  177.7 115.3 %copy-start.3 = (bf16[128,2048]{1,0:T(8,128)(2,1)}, bf16[128,2048]{1,0:T(8,128)(2,1)S(1)}, u32[]{:S(2)}) copy-start(bf16[128,2048]{1,0:T(8,128)(2,1)S(1)} %get-tuple-element.18) | copy-start | bytes 1572868
  177.7 72.0 %all-to-all-start.2 = ((bf16[64,40,1024]{2,1,0:T(8,128)(2,1)}), bf16[64,40,1024]{2,1,0:T(8,128)(2,1)}, u32[]{:S(2)}, u32[]{:S(2)}) async-start(bf16[64,40,1024]{2,1,0:T(8,128)(2,1)} %copy-done.2), calls=%async_computation.2 | async-start | bytes 10485760 | tf_op jit(solution)/shard_map/all_to_all | solution.py:338
  183.4 3.0 collective-permute-start
  183.5 4.4 %collective-permute-start.1 = (bf16[1,2048,256]{2,1,0:T(8,128)(2,1)}, bf16[1,2048,256]{2,1,0:T(8,128)(2,1)S(1)}, u32[]{:S(2)}, u32[]{:S(2)}) collective-permute-start(bf16[1,2048,256]{2,1,0:T(8,128)(2,1)} %up0_ref.1), channel_id=1, source_target_pairs={{0,1},{1,0},{2,3},{3,2},{4,5},{5,4},{6,7},{7,6},{8,9},{9,8},{10,11... | collective-permute-start | bytes 3145736 | tf_op jit(solution)/shard_map/ppermute | solution.py:302
  184.0 5.4 %collective-permute-start.2 = (bf16[1,256,2048]{2,1,0:T(8,128)(2,1)}, bf16[1,256,2048]{2,1,0:T(8,128)(2,1)S(1)}, u32[]{:S(2)}, u32[]{:S(2)}) collective-permute-start(bf16[1,256,2048]{2,1,0:T(8,128)(2,1)} %down0_ref.1), channel_id=1, source_target_pairs={{0,1},{1,0},{2,3},{3,2},{4,5},{5,4},{6,7},{7,6},{8,9},{9,8},{10,11... | collective-permute-start | bytes 3145736 | tf_op jit(solution)/shard_map/ppermute | solution.py:303
  186.4 1.0 copy-start.12
  187.9 1.0 copy-start.14
  189.4 1.0 copy-start.16
  249.7 1.2 copy-start.9
  251.0 1.2 copy-start.10
  252.2 1.2 copy-start.11
  253.4 1.2 copy-start.13
  254.6 1.2 copy-start.15
  255.9 1.2 copy-start.17
  268.5 2.4 copy-start.1
  270.9 12.1 %copy-start.23 = (f32[128,8]{0,1:T(8,128)S(1)}, f32[128,8]{0,1:T(8,128)}, u32[]{:S(2)}) copy-start(f32[128,8]{0,1:T(8,128)} %param.25) | copy-start | bytes 12292
  270.9 13.0 %copy-start.25 = (s32[8]{0:T(128)S(1)}, s32[8]{0:T(128)}, u32[]{:S(2)}) copy-start(s32[8]{0:T(128)} %constant.69.clone) | copy-start | bytes 100
  270.9 13.1 %copy-start.24 = (s32[8]{0:T(128)S(1)}, s32[8]{0:T(128)}, u32[]{:S(2)}) copy-start(s32[8]{0:T(128)} %constant.70.clone) | copy-start | bytes 100
  270.9 79.5 %all-to-all-start.3 = ((bf16[64,40,1024]{2,1,0:T(8,128)(2,1)}), bf16[64,40,1024]{2,1,0:T(8,128)(2,1)}, u32[]{:S(2)}, u32[]{:S(2)}) async-start(bf16[64,40,1024]{2,1,0:T(8,128)(2,1)} %copy-done.1), calls=%async_computation.3 | async-start | bytes 10485760 | tf_op jit(solution)/shard_map/all_to_all | solution.py:348
  289.0 3.1 copy-start.20
  291.3 1.8 copy-start.21
  350.4 1.0 copy-start.4
  351.5 0.9 copy-start.5
Sparse Core Ops, SparseCore 0:
  34.4 46.3 all-gather.2

commit v3 on v2

--- a/solution.py
+++ b/solution.py
@@ -12,74 +12,115 @@
 norm_eps = 1e-06
 
 
-def attention_kernel(meta_ref, query_ref, kv_ref, out_ref, tri_ref, acc_ref):
-    own, plane = meta_ref[0], meta_ref[1]
+def pack_kernel(core_ref, query_ref, key_ref, value_ref, query_out, keep_out, send_out):
+    core = core_ref[0]
+    heads, rows, _ = keep_out.shape
+    mine, peers = pl.ds(core * rows, rows), pl.ds((1 - core) * rows, rows)
+    for head in range(heads):
+        span = slice(head * HEAD_DIM, (head + 1) * HEAD_DIM)
+        query = query_ref[:, span]
+        query_out[head] = jnp.concatenate([query, jnp.zeros_like(query)], axis=1)
+        keep_out[head] = jnp.concatenate([key_ref[mine, span], value_ref[mine, span]], axis=1)
+        send_out[head] = jnp.concatenate([key_ref[peers, span], value_ref[peers, span]], axis=1)
+
+
+def pack(core, queries, key_rows, value_rows):
+    side, width = queries.shape
+    heads = width // HEAD_DIM
+    half = jax.ShapeDtypeStruct((heads, side // 2, LANES), jnp.bfloat16)
+    return pl.pallas_call(
+        pack_kernel,
+        in_specs=[pl.BlockSpec(memory_space=pltpu.SMEM)] + [pl.BlockSpec(memory_space=pltpu.VMEM)] * 3,
+        out_specs=[pl.BlockSpec(memory_space=pltpu.VMEM)] * 3,
+        out_shape=[jax.ShapeDtypeStruct((heads, side, LANES), jnp.bfloat16), half, half],
+        name="pack",
+    )(core, queries, key_rows, value_rows)
+
+
+GROUP = 4
+
+
+def attention_kernel(meta_ref, q0, q1, q2, q3, mine_ref, peer_ref, out_ref, kv_ref, tri_ref, query_ref, acc_ref, sems):
+    core = meta_ref[0]
     side = tri_ref.shape[0]
+    rows = mine_ref.shape[1]
+    loads = [
+        pltpu.make_async_copy(mine_ref, kv_ref.at[:, pl.ds(core * rows, rows)], sems.at[0]),
+        pltpu.make_async_copy(peer_ref, kv_ref.at[:, pl.ds((1 - core) * rows, rows)], sems.at[1]),
+    ]
+    for load in loads:
+        load.start()
     row = lax.broadcasted_iota(jnp.int32, (side, side), 0)
     col = lax.broadcasted_iota(jnp.int32, (side, side), 1)
-    tri_ref[...] = (row > col).astype(jnp.bfloat16)
-
-    def key_block(block):
-        quarter, place = block // 16, block % 16
-        slot = jnp.where((quarter + plane) % 2 == 1, 15 - place, place)
-        return kv_ref[slot, quarter]
-
-    def tile(query, block, diagonal):
-        kv = key_block(block)
-        score = lax.dot_general(
-            query, kv, (((1,), (1,)), ((), ())), preferred_element_type=jnp.float32
-        ) * (HEAD_DIM**-0.5 * LOG2E)
-        cost = jnp.maximum(score, 0.0) + jnp.log2(1.0 + jnp.exp2(-jnp.abs(score)))
-        slack = score - cost
-        if diagonal is not None:
-            live = col + block * side < row + diagonal * side
-            cost = jnp.where(live, cost, 0.0)
-        high = cost.astype(jnp.bfloat16)
-        low = (cost - high.astype(jnp.float32)).astype(jnp.bfloat16)
+    tri_ref[...] = (row > col).astype(jnp.float32)
+    for turn, ref in enumerate((q0, q1, q2, q3)):
+        query_ref[turn] = ref[...]
+    for load in loads:
+        load.wait()
+
+    def advance(query, first, own):
+        keys = [kv_ref[first + i] for i in range(GROUP)]
+        scores = [
+            lax.dot_general(query, kv, (((1,), (1,)), ((), ())), preferred_element_type=jnp.float32)
+            * (HEAD_DIM**-0.5 * LOG2E)
+            for kv in keys
+        ]
+        costs = [jnp.maximum(s, 0.0) + jnp.log2(1.0 + jnp.exp2(-jnp.abs(s))) for s in scores]
+        slacks = [s - c for s, c in zip(scores, costs)]
+        if own is not None:
+            live = [col + (first + i - own) * side < row for i in range(GROUP)]
+            costs = [jnp.where(l, c, 0.0) for l, c in zip(live, costs)]
         tri = tri_ref[...]
-        inside = jnp.dot(high, tri, preferred_element_type=jnp.float32) + jnp.dot(
-            low, tri, preferred_element_type=jnp.float32
-        )
-        weight = jnp.exp2(slack - inside)
-        if diagonal is not None:
-            weight = jnp.where(live, weight, 0.0)
-        part = jnp.dot(weight.astype(jnp.bfloat16), kv, preferred_element_type=jnp.float32)
-        decay = jnp.exp2(-(inside[:, 0:1] + cost[:, 0:1]))
-        return part, decay
+        insides = [jnp.dot(c, tri, preferred_element_type=jnp.float32) for c in costs]
+        acc = acc_ref[...]
+        for i in range(GROUP):
+            weight = jnp.exp2(slacks[i] - insides[i])
+            if own is not None:
+                weight = jnp.where(live[i], weight, 0.0)
+            part = jnp.dot(weight.astype(jnp.bfloat16), keys[i], preferred_element_type=jnp.float32)
+            acc = acc * jnp.exp2(-(insides[i][:, 0:1] + costs[i][:, 0:1])) + part
+        acc_ref[...] = acc
 
     @pl.loop(0, 4)
-    def _(quarter):
-        block = quarter * 16 + jnp.where(quarter % 2 == 1, 15 - own, own)
-        query = query_ref[quarter]
+    def _(turn):
+        own = meta_ref[1 + turn]
+        query = query_ref[turn]
         acc_ref[...] = jnp.zeros_like(acc_ref)
 
-        @pl.loop(0, block // 2)
-        def _(pair):
-            part0, decay0 = tile(query, pair * 2, None)
-            part1, decay1 = tile(query, pair * 2 + 1, None)
-            acc_ref[...] = (acc_ref[...] * decay0 + part0) * decay1 + part1
-
-        last = block // 2 * 2
-        part0, decay0 = tile(query, last, block)
-        part1, decay1 = tile(query, last + 1, block)
-        out_ref[quarter] = ((acc_ref[...] * decay0 + part0) * decay1 + part1).astype(jnp.bfloat16)
-
-
-def attention(meta, query, kv):
-    side = query.shape[1]
-    pairs = 132 * side * side
+        @pl.loop(0, own // GROUP)
+        def _(step):
+            advance(query, step * GROUP, None)
+
+        advance(query, own // GROUP * GROUP, own)
+        done = acc_ref[:, HEAD_DIM:].astype(jnp.bfloat16)
+        slot = meta_ref[5 + turn]
+        out_ref[slot] = done[:rows]
+        out_ref[slot + 1] = done[rows:]
+
+
+def attention(meta, queries, mine, peer):
+    side = queries[0].shape[0]
+    pairs = 136 * side * side
     return pl.pallas_call(
         attention_kernel,
-        out_shape=jax.ShapeDtypeStruct((4, side, LANES), jnp.bfloat16),
-        in_specs=[pl.BlockSpec(memory_space=pltpu.SMEM)] + [pl.BlockSpec(memory_space=pltpu.VMEM)] * 2,
+        out_shape=jax.ShapeDtypeStruct((16, side // 2, HEAD_DIM), jnp.bfloat16),
+        in_specs=[pl.BlockSpec(memory_space=pltpu.SMEM)]
+        + [pl.BlockSpec(memory_space=pltpu.VMEM)] * 4
+        + [pl.BlockSpec(memory_space=pl.ANY)] * 2,
         out_specs=pl.BlockSpec(memory_space=pltpu.VMEM),
-        scratch_shapes=[pltpu.VMEM((side, side), jnp.bfloat16), pltpu.VMEM((side, LANES), jnp.float32)],
-        compiler_params=pltpu.CompilerParams(vmem_limit_bytes=24 * 2**20),
+        scratch_shapes=[
+            pltpu.VMEM((mine.shape[0], side, LANES), jnp.bfloat16),
+            pltpu.VMEM((side, side), jnp.float32),
+            pltpu.VMEM((4, side, LANES), jnp.bfloat16),
+            pltpu.VMEM((side, LANES), jnp.float32),
+            pltpu.SemaphoreType.DMA((2,)),
+        ],
+        compiler_params=pltpu.CompilerParams(vmem_limit_bytes=56 * 2**20),
         cost_estimate=pl.CostEstimate(
             flops=pairs * 2 * 768, bytes_accessed=6 * 2**20, transcendentals=pairs * 3
         ),
         name="attend",
-    )(meta, query, kv)
+    )(meta, *queries, mine, peer)
 
 
 MAIN = 16
@@ -87,13 +128,25 @@
 
 
 def dispatch_kernel(
-    attended_ref, residual_ref, weight_ref, gain_ref, main_ref, tail_ref, mixed_ref, normed_ref, out_ref
+    side_ref,
+    attended_ref,
+    residual_ref,
+    weight_ref,
+    gain_ref,
+    main_ref,
+    tail_ref,
+    mixed_ref,
+    normed_ref,
+    out_ref,
+    heads_ref,
 ):
     half = out_ref.shape[2]
 
     @pl.when(pl.program_id(0) == 0)
     def _():
-        projected = jnp.dot(attended_ref[...], weight_ref[...], preferred_element_type=jnp.float32)
+        for head in range(8):
+            heads_ref[:, head * HEAD_DIM : (head + 1) * HEAD_DIM] = attended_ref[2 * head + side_ref[0]]
+        projected = jnp.dot(heads_ref[...], weight_ref[...], preferred_element_type=jnp.float32)
         mixed = (residual_ref[...].astype(jnp.float32) + projected).astype(jnp.bfloat16)
         mixed_ref[...] = mixed
         mixed = mixed.astype(jnp.float32)
@@ -114,7 +167,7 @@
     out_ref[:, 2 * MAIN :, :] = both.astype(jnp.bfloat16).reshape(experts, 2 * TAIL, half)
 
 
-def dispatch(attended, residual, out_weight, gain, main, tail):
+def dispatch(side, attended, residual, out_weight, gain, main, tail):
     tokens, width = residual.shape
     experts = main.shape[0] // MAIN
     step = 16
@@ -123,7 +176,8 @@
         dispatch_kernel,
         grid=(experts // step,),
         in_specs=[
-            pl.BlockSpec(attended.shape, whole),
+            pl.BlockSpec(memory_space=pltpu.SMEM),
+            pl.BlockSpec(attended.shape, lambda i: (0, 0, 0)),
             pl.BlockSpec(residual.shape, whole),
             pl.BlockSpec(out_weight.shape, whole),
             pl.BlockSpec(gain.shape, whole),
@@ -140,20 +194,59 @@
             jax.ShapeDtypeStruct((tokens, width), jnp.bfloat16),
             jax.ShapeDtypeStruct((experts, 2 * (MAIN + TAIL), width // 2), jnp.bfloat16),
         ],
-        compiler_params=pltpu.CompilerParams(vmem_limit_bytes=32 * 2**20),
+        scratch_shapes=[pltpu.VMEM((tokens, 8 * HEAD_DIM), jnp.bfloat16)],
+        compiler_params=pltpu.CompilerParams(vmem_limit_bytes=60 * 2**20),
         cost_estimate=pl.CostEstimate(flops=10**9, bytes_accessed=10**7, transcendentals=0),
         name="dispatch",
-    )(attended, residual, out_weight, gain, main, tail)
+    )(side, attended, residual, out_weight, gain, main, tail)
 
 
 def expert_kernel(
-    rows_ref, gate0_ref, up0_ref, down0_ref, gate1_ref, up1_ref, down1_ref, out_ref, spread_ref, rows2_ref
+    rows_ref,
+    gate0,
+    up0,
+    gate1,
+    up1,
+    down0,
+    down1,
+    out_ref,
+    spread_ref,
+    rows2_ref,
+    gate0_ref,
+    up0_ref,
+    gate1_ref,
+    up1_ref,
+    down0_ref,
+    down1_ref,
+    sems,
 ):
     sources, _, half = rows_ref.shape
     tails = sources * TAIL
-
-    @pl.when(pl.program_id(0) == 0)
+    first_step = pl.program_id(0) == 0
+    loads = [
+        pltpu.make_async_copy(source, target, sems.at[i])
+        for i, (source, target) in enumerate(
+            (
+                (gate0, gate0_ref),
+                (up0, up0_ref),
+                (gate1, gate1_ref),
+                (up1, up1_ref),
+                (down0, down0_ref),
+                (down1, down1_ref),
+            )
+        )
+    ]
+
+    def arrived(*which):
+        @pl.when(first_step)
+        def _():
+            for i in which:
+                loads[i].wait()
+
+    @pl.when(first_step)
     def _():
+        for load in loads:
+            load.start()
         row = lax.broadcasted_iota(jnp.int32, (2 * tails, 2 * tails), 0)
         col = lax.broadcasted_iota(jnp.int32, (2 * tails, 2 * tails), 1)
         slot = row % tails
@@ -176,8 +269,11 @@
         upward = jnp.dot(rows, up_ref[0], preferred_element_type=jnp.float32)
         return (jax.nn.silu(gate) * upward).astype(jnp.bfloat16)
 
+    arrived(0, 1)
     act0 = hidden(gate0_ref, up0_ref)
+    arrived(2, 3)
     act1 = hidden(gate1_ref, up1_ref)
+    arrived(4, 5)
     for part in range(2):
         span = pl.ds(part * half, half)
         result = jnp.dot(act0, down0_ref[0, :, span], preferred_element_type=jnp.float32) + jnp.dot(
@@ -195,24 +291,25 @@
             out_ref[:, 2 * MAIN :, :] = ends.astype(jnp.bfloat16).reshape(sources, 2 * TAIL, half)
 
 
-def expert(rows, mine, other):
+def expert(rows, weights):
     step = 16
-    whole = [pl.BlockSpec(memory_space=pltpu.VMEM)] * 6
     block = pl.BlockSpec((step,) + rows.shape[1:], lambda i: (i, 0, 0))
     return pl.pallas_call(
         expert_kernel,
         grid=(rows.shape[0] // step,),
-        in_specs=[block] + whole,
+        in_specs=[block] + [pl.BlockSpec(memory_space=pl.ANY)] * 6,
         out_specs=block,
         out_shape=jax.ShapeDtypeStruct(rows.shape, jnp.bfloat16),
         scratch_shapes=[
             pltpu.VMEM((step * 2 * TAIL, step * 2 * TAIL), jnp.bfloat16),
             pltpu.VMEM((step * (MAIN + TAIL), 2 * rows.shape[2]), jnp.bfloat16),
-        ],
-        compiler_params=pltpu.CompilerParams(vmem_limit_bytes=32 * 2**20),
+        ]
+        + [pltpu.VMEM(w.shape, w.dtype) for w in weights]
+        + [pltpu.SemaphoreType.DMA((6,))],
+        compiler_params=pltpu.CompilerParams(vmem_limit_bytes=60 * 2**20),
         cost_estimate=pl.CostEstimate(flops=8 * 10**9, bytes_accessed=17 * 10**6, transcendentals=10**6),
         name="expert",
-    )(rows, *mine, *other)
+    )(rows, *weights)
 
 
 def combine_kernel(rows_ref, main_ref, left_ref, right_ref, base_ref, out_ref, acc_ref):
@@ -254,7 +351,7 @@
         out_specs=pl.BlockSpec(base.shape, whole),
         out_shape=jax.ShapeDtypeStruct(base.shape, jnp.bfloat16),
         scratch_shapes=[pltpu.VMEM(base.shape, jnp.float32)],
-        compiler_params=pltpu.CompilerParams(vmem_limit_bytes=32 * 2**20),
+        compiler_params=pltpu.CompilerParams(vmem_limit_bytes=60 * 2**20),
         cost_estimate=pl.CostEstimate(flops=10**9, bytes_accessed=10**7, transcendentals=0),
         name="combine",
     )(rows, main, left, right, base)
@@ -276,37 +373,47 @@
     shared_up,
     shared_down,
 ):
-    side = queries.shape[0]
+    chips = [[i, 31 - i, 32 + i, 63 - i, 8 + i, 23 - i, 40 + i, 55 - i] for i in range(8)]
+    devices = [[2 * s + c for s in g for c in range(2)] for g in chips]
+    core = lax.axis_index("tp")
     position = lax.axis_index("sp")
-    plane = position // 16
-    spot = position % 16
-    own = jnp.where(plane % 2 == 1, 15 - spot, spot)
-    meta = jnp.stack([own, plane]).astype(jnp.int32)
-    columns = [[i, 31 - i, 32 + i, 63 - i] for i in range(16)]
-    planes = [[16 * z + j for j in range(16)] for z in range(4)]
-
-    def heads(rows):
-        return rows.reshape(side, 4, HEAD_DIM).transpose(1, 0, 2)
-
-    query_heads = heads(queries)
-    packed = jnp.concatenate(
-        [query_heads, jnp.zeros_like(query_heads), heads(key_rows), heads(value_rows)], axis=2
+    plane, spot = position // 16, position % 16
+    place = jnp.where(plane % 2 == 1, 15 - spot, spot)
+    group, member = place % 8, plane + place // 8 * 4
+
+    query_heads, keep, send = pack(core[None].astype(jnp.int32), queries, key_rows, value_rows)
+    swap = [(0, 1), (1, 0)]
+    taken = lax.ppermute(send, "tp", swap)
+    low, high = jnp.where(core == 0, keep, taken), jnp.where(core == 0, taken, keep)
+    order = jnp.stack([low[0], high[0], high[1], low[1], low[2], high[2], high[3], low[3]])
+    order = jnp.broadcast_to(order[:, None], (8,) + order.shape)
+    mine = lax.all_to_all(order.reshape((64,) + order.shape[2:]), "sp", 0, 0, tiled=True)
+    turns = []
+    for turn in range(4):
+        pairs = [
+            (devices[g][2 * m + c], devices[g][2 * (4 * c + ((m % 4) ^ turn)) + m // 4])
+            for g in range(8)
+            for m in range(8)
+            for c in range(2)
+        ]
+        head = lax.dynamic_index_in_dim(query_heads, (member % 4) ^ turn, 0, keepdims=False)
+        turns.append(lax.ppermute(head, ("sp", "tp"), pairs))
+    peer = lax.ppermute(mine, "tp", swap)
+    sender = [4 * core + ((member % 4) ^ turn) for turn in range(4)]
+    block = [
+        16 * (m % 4) + jnp.where(m % 2 == 1, 15 - group - m // 4 * 8, group + m // 4 * 8) for m in sender
+    ]
+    meta = jnp.stack([core] + block + [2 * m for m in sender]).astype(jnp.int32)
+    attended = attention(meta, turns, mine, peer)
+    peer, expert_gate_, expert_up_, expert_down_ = lax.optimization_barrier(
+        (peer, expert_gate, expert_up, expert_down)
     )
-    packed = lax.all_to_all(packed, "sp", 0, 0, axis_index_groups=columns, tiled=True)
-    kv = lax.all_gather(packed[:, :, LANES:], "sp", axis_index_groups=planes, axis=0)
-    peer = [(0, 1), (1, 0)]
-    kv, expert_gate_, expert_up_, expert_down_ = lax.optimization_barrier(
-        (kv, expert_gate, expert_up, expert_down)
-    )
-    gate_other = lax.ppermute(expert_gate_, "tp", peer)
-    up_other = lax.ppermute(expert_up_, "tp", peer)
-    down_other = lax.ppermute(expert_down_, "tp", peer)
-    attended = attention(meta, packed[:, :, :LANES], kv)[:, :, HEAD_DIM:]
+    gate_other = lax.ppermute(expert_gate_, "tp", swap)
+    up_other = lax.ppermute(expert_up_, "tp", swap)
+    down_other = lax.ppermute(expert_down_, "tp", swap)
     tokens = residual.shape[0]
-    eights = [[2 * s + c for s in g for c in range(2)] for g in columns]
-    attended = attended.reshape(8, tokens, HEAD_DIM)
-    attended = lax.all_to_all(attended, ("sp", "tp"), 0, 0, axis_index_groups=eights, tiled=True)
-    attended = attended.reshape(4, 2, tokens, HEAD_DIM).transpose(2, 1, 0, 3).reshape(tokens, 512)
+    attended = lax.all_to_all(attended, ("sp", "tp"), 0, 0, axis_index_groups=devices, tiled=True)
+    side = (member // 4)[None].astype(jnp.int32)
 
     experts = lax.axis_size("sp")
     named = routes[:, :, None] == jnp.arange(experts, dtype=jnp.int32)
@@ -333,7 +440,7 @@
     _, back_left = slots(ends + none)
     _, back_right = slots(none + ends)
     mixed, normed, outgoing = dispatch(
-        attended, residual, out_weight, norm_gain[None, :], send_main, send_tail
+        side, attended, residual, out_weight, norm_gain[None, :], send_main, send_tail
     )
     incoming = lax.all_to_all(outgoing, "sp", 0, 0, tiled=True)
     shared_gate_out = jnp.dot(normed, shared_gate, preferred_element_type=jnp.float32)
@@ -343,7 +450,7 @@
         shared_act, shared_down, preferred_element_type=jnp.float32
     )
     result = expert(
-        incoming, (expert_gate, expert_up, expert_down), (gate_other, up_other, down_other)
+        incoming, (expert_gate, expert_up, gate_other, up_other, expert_down, down_other)
     )
     returned = lax.all_to_all(result, "sp", 0, 0, tiled=True)
     return combine(returned, back_main, back_left, back_right, base)

time: 367 us -> 302 us (0.82)
  waiting for transfers between devices: 172 us -> 137 us
  local copies, waits for them, and re-layouts: 34.7 us -> 8.49 us
  Pallas kernels: 88.3 us -> 66.2 us
  blocking collectives: 22.9 us -> 42 us
  between operations: 13.8 us -> 0.42 us
  starting transfers between devices: 24.9 us -> 36 us
    all_gather x1 -> x0, waiting for transfers between devices: 45.7 us -> none  [local(): lax.all_gather(packed[:, :, LANES:], 'sp', axis_index_groups=planes, axis=0)]
    pallas_call x1 -> x2, Pallas kernels: 68.2 us -> 37.2 us  [the longest x1 35.1 us: attention(): pl.pallas_call(attention_kernel, out_shape=jax.ShapeDtypeStruct((16, side...]
    unnamed x57 -> x34, local copies, waits for them, and re-layouts: 26 us -> 0.72 us
    all_to_all x1, blocking collectives: 22.9 us -> 42 us  [local(): lax.all_to_all(order.reshape((64,) + order.shape[2:]), 'sp', 0, 0, tiled=...]
    ppermute x3 -> x9, starting transfers between devices: 0.68 us -> 10.3 us  [the longest x4 9.66 us: local(): turns.append(lax.ppermute(head, ('sp', 'tp'), pairs))]
    ppermute x3 -> x9, waiting for transfers between devices: 3.28 us -> 9.83 us  [the longest x4 2.87 us: local(): turns.append(lax.ppermute(head, ('sp', 'tp'), pairs))]
    pallas_call x1, Pallas kernels: 11.4 us -> 15.9 us  [expert(): pl.pallas_call(expert_kernel, grid=(rows.shape[0] // step,), in_specs=[bl...]
    pallas_call x1, Pallas kernels: 2.93 us -> 6.85 us  [dispatch(): pl.pallas_call(dispatch_kernel, grid=(experts // step,), in_specs=[pl.Blo...]
  transfers between devices with their start and end apart: 7 -> 12, of which waited for: 7 -> 8; matrix products, arithmetic and copies ran while one was open for 4% -> 4% of each run, Pallas kernels for 0% -> 0%
where the time goes in v3:
time: 302 us; the launch traced here: 298 us
  waiting for transfers between devices  137 us (45%)
  Pallas kernels  66.2 us (22%)
  blocking collectives  42 us (14%)
  starting transfers between devices  36 us (12%)
  local copies, waits for them, and re-layouts  8.49 us (3%)
  other arithmetic  4.68 us (2%)
  matrix products  4.05 us (1%)
    all_to_all x1, waiting for transfers between devices, local(): incoming = lax.all_to_all(outgoing, 'sp', 0, 0, tiled=True)  61.4 us
    all_to_all x1, waiting for transfers between devices, local(): returned = lax.all_to_all(result, 'sp', 0, 0, tiled=True)  57.3 us
    all_to_all x1, blocking collectives, local(): lax.all_to_all(order.reshape((64,) + order.shape[2:]), 'sp', 0, 0, tiled=...  42 us
    pallas_call x1, Pallas kernels, attention(): pl.pallas_call(attention_kernel, out_shape=jax.ShapeDtypeStruct((16, side...  35.1 us
    pallas_call x1, Pallas kernels, expert(): pl.pallas_call(expert_kernel, grid=(rows.shape[0] // step,), in_specs=[bl...  15.9 us
    all_to_all x1, starting transfers between devices, local(): returned = lax.all_to_all(result, 'sp', 0, 0, tiled=True)  11.3 us
    ppermute x4, starting transfers between devices, local(): turns.append(lax.ppermute(head, ('sp', 'tp'), pairs))  9.66 us
    all_to_all x1, waiting for transfers between devices, local(): lax.all_to_all(attended, ('sp', 'tp'), 0, 0, axis_index_groups=devices, t...  8.06 us
  transfers between devices with their start and end apart: 12, of which 8 were waited for; matrix products, arithmetic and copies ran while one was open for 4% of the time, Pallas kernels for 0%

profile of v3, /device:TPU:0, one launch (start us, length us, event | category | flops | bytes accessed | tf_op | source)
XLA Modules:
  0.0 298.4 jit_solution(3835157885956558647)
XLA Ops:
  0.0 2.1 pack.1
  2.1 1.6 collective-permute-done.4
  3.7 0.9 broadcast_select_fusion
  4.7 0.5 broadcast_in_dim.85
  5.2 42.0 %all_to_all.20.mine_ref = bf16[64,128,128]{2,1,0:T(8,128)(2,1)} all-to-all(bf16[64,128,128]{2,1,0:T(8,128)(2,1)S(1)} %bitcast.41), channel_id=1, replica_groups=mesh['sp'=64,'tp'=2] {'sp'}, dimensions={0} | all-to-all | bytes 4194304 | tf_op jit(solution)/shard_map/all_to_all | solution.py:390
  47.2 0.7 collective-permute-start
  47.9 1.0 collective-permute-start.1
  48.9 1.7 collective-permute-start.2
  50.5 6.3 %collective-permute-start.3 = (bf16[256,128]{1,0:T(8,128)(2,1)S(1)}, bf16[256,128]{1,0:T(8,128)(2,1)S(1)}, u32[]{:S(2)}, u32[]{:S(2)}) collective-permute-start(bf16[256,128]{1,0:T(8,128)(2,1)S(1)} %get-tuple-element.29), channel_id=1, source_target_pairs={{0,126},{1,110},{62,64},{63,80},{64,62},{65,46},{126,0},{127,16},{... | collective-permute-start | bytes 196616 | tf_op jit(solution)/shard_map/ppermute | solution.py:400
  56.9 0.6 stack.43.meta_ref
  57.6 2.9 collective-permute-done.3.q3
  60.5 0.6 copy-done.14
  61.1 35.1 %attend.1 = bf16[16,128,64]{2,1,0:T(8,128)(2,1)} custom-call(s32[9]{0:T(128)} %stack.43.meta_ref, bf16[256,128]{1,0:T(8,128)(2,1)} %copy-done.11, bf16[256,128]{1,0:T(8,128)(2,1)} %copy-done.12, bf16[256,128]{1,0:T(8,128)(2,1)} %copy-done.13, bf16[256,128]{1,0:T(8,128)(2,1)} %copy-done.14, bf16[64,128,128]{2,1,0:T(8,128)(2,1)} %all_to_all.20.mine_ref, ...), custom_call_target="tpu_custom_call" | custom-call | flops 13690208256 | bytes 6291456 | tf_op jit(solution)/shard_map/attend/pallas_call | solution.py:104
  96.1 1.9 copy.41
  98.1 7.9 %all-to-all-start.1 = ((bf16[16,128,64]{1,2,0:T(8,128)(2,1)}), bf16[16,128,64]{1,2,0:T(8,128)(2,1)S(1)}, u32[]{:S(2)}, u32[]{:S(2)}) async-start(bf16[16,128,64]{1,2,0:T(8,128)(2,1)} %copy.41), calls=%async_computation.1 | async-start | bytes 524288 | tf_op jit(solution)/shard_map/all_to_all | solution.py:415
  106.0 0.2 fusion.1
  106.2 0.1 eq.156
  106.3 0.1 eq.162
  106.4 0.9 fusion.2.main_ref
  107.3 0.8 fusion.9.tail_ref
  108.1 8.1 %all-to-all-done.1 = bf16[16,128,64]{1,2,0:T(8,128)(2,1)S(1)} async-done(((bf16[16,128,64]{1,2,0:T(8,128)(2,1)}), bf16[16,128,64]{1,2,0:T(8,128)(2,1)S(1)}, u32[]{:S(2)}, u32[]{:S(2)}) %all-to-all-start.1) | async-done | bytes 262176 | tf_op jit(solution)/shard_map/all_to_all | solution.py:415
  116.2 1.0 copy.42.attended_ref
  117.2 6.8 %dispatch.1 = (bf16[128,2048]{1,0:T(8,128)(2,1)}, bf16[128,2048]{1,0:T(8,128)(2,1)}, bf16[64,40,1024]{2,1,0:T(8,128)(2,1)}) custom-call(s32[1]{0:T(128)} %bitcast.side_ref, bf16[16,128,64]{2,1,0:T(8,128)(2,1)} %copy.42.attended_ref, bf16[128,2048]{1,0:T(8,128)(2,1)} %residual_ref.1, bf16[512,2048]{1,0:T(8,128)(2,1)} %weight_ref.1, f32[1,2048]{1,0:T(1,128)} %bitcast.46, ...), custom_call_target="tpu_custom_call" | custom-call | flops 1000000000 | bytes 10000000 | tf_op jit(solution)/shard_map/dispatch/pallas_call | solution.py:175
  124.0 6.4 %all-to-all-start.2 = ((bf16[64,40,1024]{2,1,0:T(8,128)(2,1)}), bf16[64,40,1024]{2,1,0:T(8,128)(2,1)}, u32[]{:S(2)}, u32[]{:S(2)}) async-start(bf16[64,40,1024]{2,1,0:T(8,128)(2,1)} %get-tuple-element.17), calls=%async_computation.2 | async-start | bytes 10485760 | tf_op jit(solution)/shard_map/all_to_all | solution.py:445
  130.4 0.1 collective-permute-start.6
  130.5 0.5 collective-permute-start.7
  131.0 0.1 collective-permute-start.8
  131.1 2.4 collective-permute-done.6.gate1
  133.5 1.5 collective-permute-done.7.up1
  135.0 1.5 collective-permute-done.8.down1
  136.5 61.4 %all-to-all-done.2.rows_ref = bf16[64,40,1024]{2,1,0:T(8,128)(2,1)} async-done(((bf16[64,40,1024]{2,1,0:T(8,128)(2,1)}), bf16[64,40,1024]{2,1,0:T(8,128)(2,1)}, u32[]{:S(2)}, u32[]{:S(2)}) %all-to-all-start.2) | async-done | bytes 5242912 | tf_op jit(solution)/shard_map/all_to_all | solution.py:445
  197.9 15.9 %expert.1 = bf16[64,40,1024]{2,1,0:T(8,128)(2,1)} custom-call(bf16[64,40,1024]{2,1,0:T(8,128)(2,1)} %all-to-all-done.2.rows_ref, bf16[1,2048,256]{2,1,0:T(8,128)(2,1)} %gate0.1, bf16[1,2048,256]{2,1,0:T(8,128)(2,1)} %up0.1, bf16[1,2048,256]{2,1,0:T(8,128)(2,1)} %collective-permute-done.6.gate1, bf16[1,2048,256]{2,1,0:T(8,128)(2,1)} %collective-permute-done.7.up1, ...), custom_call_target="tpu_custom_call" | custom-call | flops 8000000000 | bytes 17000000 | tf_op jit(solution)/shard_map/expert/pallas_call | solution.py:297
  213.9 11.3 %all-to-all-start.3 = ((bf16[64,40,1024]{2,1,0:T(8,128)(2,1)}), bf16[64,40,1024]{2,1,0:T(8,128)(2,1)}, u32[]{:S(2)}, u32[]{:S(2)}) async-start(bf16[64,40,1024]{2,1,0:T(8,128)(2,1)} %expert.1), calls=%async_computation.3 | async-start | bytes 10485760 | tf_op jit(solution)/shard_map/all_to_all | solution.py:455
  225.2 0.1 copy.45
  225.5 0.8 copy.46
  226.3 0.1 eq.172
  226.4 0.1 eq.176
  226.6 0.2 copy.43
  226.8 0.8 broadcast_in_dim.92
  227.6 1.2 copy.44
  228.9 0.1 subtract_convert_fusion
  229.0 0.8 pad_maximum_fusion.main_ref
  229.9 0.1 subtract_convert_fusion.1
  230.0 0.9 pad_maximum_fusion.1
  230.9 0.4 fusion.22
  231.4 3.4 %convolution_add_fusion.base_ref = f32[128,2048]{1,0:T(8,128)} fusion(bf16[512,2048]{1,0:T(8,128)(2,1)S(1)} %copy-done, bf16[128,2048]{1,0:T(8,128)(2,1)S(1)} %copy-done.3, bf16[2048,512]{1,0:T(8,128)(2,1)} %param.30, bf16[128,2048]{1,0:T(8,128)(2,1)S(1)} %copy-done.4, f32[128,512]{1,0:T(8,128)S(1)} %fusion.22), kind=kOutput, calls=%fused_computation | convolution fusion | flops 537788416 | bytes 6553600 | tf_op jit(solution)/shard_map/dot_general | solution.py:449
  234.8 57.3 %all-to-all-done.3.rows_ref = bf16[64,40,1024]{2,1,0:T(8,128)(2,1)} async-done(((bf16[64,40,1024]{2,1,0:T(8,128)(2,1)}), bf16[64,40,1024]{2,1,0:T(8,128)(2,1)}, u32[]{:S(2)}, u32[]{:S(2)}) %all-to-all-start.3) | async-done | bytes 5242912 | tf_op jit(solution)/shard_map/all_to_all | solution.py:455
  292.1 6.3 %combine.1 = bf16[128,2048]{1,0:T(8,128)(2,1)} custom-call(bf16[64,40,1024]{2,1,0:T(8,128)(2,1)} %all-to-all-done.3.rows_ref, bf16[256,1024]{1,0:T(8,128)(2,1)} %pad_maximum_fusion.main_ref, bf16[256,512]{1,0:T(8,128)(2,1)} %get-tuple-element.33.left_ref, bf16[256,512]{1,0:T(8,128)(2,1)} %get-tuple-element.34.right_ref, f32[128,2048]{1,0:T(8,128)} %convolution_add_fusion.base_ref), custom_call_target="tpu_custom_call" | custom-call | flops 1000000000 | bytes 10000000 | tf_op jit(solution)/shard_map/combine/pallas_call | solution.py:341
  (53 shorter events, 0.5 us)
Async XLA Ops:
  0.0 231.3 %copy-start = (bf16[512,2048]{1,0:T(8,128)(2,1)S(1)}, bf16[512,2048]{1,0:T(8,128)(2,1)}, u32[]{:S(2)}) copy-start(bf16[512,2048]{1,0:T(8,128)(2,1)} %param.31) | copy-start | bytes 6291460
  2.1 1.6 collective-permute-start.4
  5.2 42.0 %copy-start.5 = (bf16[4,256,128]{2,1,0:T(8,128)(2,1)S(1)}, bf16[4,256,128]{2,1,0:T(8,128)(2,1)}, u32[]{:S(2)}) copy-start(bf16[4,256,128]{2,1,0:T(8,128)(2,1)} %get-tuple-element.14) | copy-start | bytes 786436
  5.2 52.3 %copy-start.6 = (s32[128,8]{0,1:T(8,128)S(1)}, s32[128,8]{0,1:T(8,128)}, u32[]{:S(2)}) copy-start(s32[128,8]{0,1:T(8,128)} %param.24) | copy-start | bytes 12292
  47.1 13.3 %collective-permute-start.5 = (bf16[64,128,128]{2,1,0:T(8,128)(2,1)}, bf16[64,128,128]{2,1,0:T(8,128)(2,1)}, u32[]{:S(2)}, u32[]{:S(2)}) collective-permute-start(bf16[64,128,128]{2,1,0:T(8,128)(2,1)} %all_to_all.20.mine_ref), channel_id=1, source_target_pairs={{0,1},{1,0},{2,3},{3,2},{4,5},{5,4},{6,7},{7,6},{8,9},{9,8},{10,11... | collective-permute-start | bytes 6291464 | tf_op jit(solution)/shard_map/ppermute | solution.py:401
  47.2 10.3 %collective-permute-start = (bf16[256,128]{1,0:T(8,128)(2,1)S(1)}, bf16[256,128]{1,0:T(8,128)(2,1)S(1)}, u32[]{:S(2)}, u32[]{:S(2)}) collective-permute-start(bf16[256,128]{1,0:T(8,128)(2,1)S(1)} %get-tuple-element.32), channel_id=1, source_target_pairs={{0,0},{1,16},{62,62},{63,46},{64,64},{65,80},{126,126},{127,110},{... | collective-permute-start | bytes 196616 | tf_op jit(solution)/shard_map/ppermute | solution.py:400
  47.9 9.7 %collective-permute-start.1 = (bf16[256,128]{1,0:T(8,128)(2,1)S(1)}, bf16[256,128]{1,0:T(8,128)(2,1)S(1)}, u32[]{:S(2)}, u32[]{:S(2)}) collective-permute-start(bf16[256,128]{1,0:T(8,128)(2,1)S(1)} %get-tuple-element.31), channel_id=1, source_target_pairs={{0,62},{1,46},{62,0},{63,16},{64,126},{65,110},{126,64},{127,80},{... | collective-permute-start | bytes 196616 | tf_op jit(solution)/shard_map/ppermute | solution.py:400
  48.9 8.7 %collective-permute-start.2 = (bf16[256,128]{1,0:T(8,128)(2,1)S(1)}, bf16[256,128]{1,0:T(8,128)(2,1)S(1)}, u32[]{:S(2)}, u32[]{:S(2)}) collective-permute-start(bf16[256,128]{1,0:T(8,128)(2,1)S(1)} %get-tuple-element.30), channel_id=1, source_target_pairs={{0,64},{1,80},{62,126},{63,110},{64,0},{65,16},{126,62},{127,46},{... | collective-permute-start | bytes 196616 | tf_op jit(solution)/shard_map/ppermute | solution.py:400
  50.5 9.9 %collective-permute-start.3 = (bf16[256,128]{1,0:T(8,128)(2,1)S(1)}, bf16[256,128]{1,0:T(8,128)(2,1)S(1)}, u32[]{:S(2)}, u32[]{:S(2)}) collective-permute-start(bf16[256,128]{1,0:T(8,128)(2,1)S(1)} %get-tuple-element.29), channel_id=1, source_target_pairs={{0,126},{1,110},{62,64},{63,80},{64,62},{65,46},{126,0},{127,16},{... | collective-permute-start | bytes 196616 | tf_op jit(solution)/shard_map/ppermute | solution.py:400
  57.5 48.8 %copy-start.10 = (s32[8]{0:T(128)S(1)}, s32[8]{0:T(128)}, u32[]{:S(2)}) copy-start(s32[8]{0:T(128)} %constant.198.clone) | copy-start | bytes 100
  57.5 2.9 copy-start.11
  57.6 2.9 copy-start.12
  57.6 2.9 copy-start.13
  60.5 0.6 copy-start.14
  98.1 18.1 %all-to-all-start.1 = ((bf16[16,128,64]{1,2,0:T(8,128)(2,1)}), bf16[16,128,64]{1,2,0:T(8,128)(2,1)S(1)}, u32[]{:S(2)}, u32[]{:S(2)}) async-start(bf16[16,128,64]{1,2,0:T(8,128)(2,1)} %copy.41), calls=%async_computation.1 | async-start | bytes 524288 | tf_op jit(solution)/shard_map/all_to_all | solution.py:415
  124.0 73.9 %all-to-all-start.2 = ((bf16[64,40,1024]{2,1,0:T(8,128)(2,1)}), bf16[64,40,1024]{2,1,0:T(8,128)(2,1)}, u32[]{:S(2)}, u32[]{:S(2)}) async-start(bf16[64,40,1024]{2,1,0:T(8,128)(2,1)} %get-tuple-element.17), calls=%async_computation.2 | async-start | bytes 10485760 | tf_op jit(solution)/shard_map/all_to_all | solution.py:445
  130.4 3.1 %collective-permute-start.6 = (bf16[1,2048,256]{2,1,0:T(8,128)(2,1)}, bf16[1,2048,256]{2,1,0:T(8,128)(2,1)}, u32[]{:S(2)}, u32[]{:S(2)}) collective-permute-start(bf16[1,2048,256]{2,1,0:T(8,128)(2,1)} %gate0.1), channel_id=1, source_target_pairs={{0,1},{1,0},{2,3},{3,2},{4,5},{5,4},{6,7},{7,6},{8,9},{9,8},{10,11... | collective-permute-start | bytes 3145736 | tf_op jit(solution)/shard_map/ppermute | solution.py:411
  130.5 4.5 %collective-permute-start.7 = (bf16[1,2048,256]{2,1,0:T(8,128)(2,1)}, bf16[1,2048,256]{2,1,0:T(8,128)(2,1)}, u32[]{:S(2)}, u32[]{:S(2)}) collective-permute-start(bf16[1,2048,256]{2,1,0:T(8,128)(2,1)} %up0.1), channel_id=1, source_target_pairs={{0,1},{1,0},{2,3},{3,2},{4,5},{5,4},{6,7},{7,6},{8,9},{9,8},{10,11... | collective-permute-start | bytes 3145736 | tf_op jit(solution)/shard_map/ppermute | solution.py:412
  131.0 5.5 %collective-permute-start.8 = (bf16[1,256,2048]{2,1,0:T(8,128)(2,1)}, bf16[1,256,2048]{2,1,0:T(8,128)(2,1)}, u32[]{:S(2)}, u32[]{:S(2)}) collective-permute-start(bf16[1,256,2048]{2,1,0:T(8,128)(2,1)} %down0.1), channel_id=1, source_target_pairs={{0,1},{1,0},{2,3},{3,2},{4,5},{5,4},{6,7},{7,6},{8,9},{9,8},{10,11... | collective-permute-start | bytes 3145736 | tf_op jit(solution)/shard_map/ppermute | solution.py:413
  213.9 11.5 %copy-start.7 = (f32[128,8]{0,1:T(8,128)S(1)}, f32[128,8]{0,1:T(8,128)}, u32[]{:S(2)}) copy-start(f32[128,8]{0,1:T(8,128)} %param.25) | copy-start | bytes 12292
  213.9 12.4 %copy-start.9 = (s32[8]{0:T(128)S(1)}, s32[8]{0:T(128)}, u32[]{:S(2)}) copy-start(s32[8]{0:T(128)} %constant.199.clone) | copy-start | bytes 100
  213.9 12.5 %copy-start.8 = (s32[8]{0:T(128)S(1)}, s32[8]{0:T(128)}, u32[]{:S(2)}) copy-start(s32[8]{0:T(128)} %constant.200.clone) | copy-start | bytes 100
  213.9 78.2 %all-to-all-start.3 = ((bf16[64,40,1024]{2,1,0:T(8,128)(2,1)}), bf16[64,40,1024]{2,1,0:T(8,128)(2,1)}, u32[]{:S(2)}, u32[]{:S(2)}) async-start(bf16[64,40,1024]{2,1,0:T(8,128)(2,1)} %expert.1), calls=%async_computation.3 | async-start | bytes 10485760 | tf_op jit(solution)/shard_map/all_to_all | solution.py:455
  228.8 1.0 copy-start.1
  229.0 1.9 copy-start.2
  229.0 1.9 copy-start.3
  230.0 1.3 copy-start.4

commit v4 on v3

--- a/solution.py
+++ b/solution.py
@@ -12,29 +12,77 @@
 norm_eps = 1e-06
 
 
-def pack_kernel(core_ref, query_ref, key_ref, value_ref, query_out, keep_out, send_out):
-    core = core_ref[0]
+def pack_kernel(meta_ref, key_ref, value_ref, keep_out, send_out):
+    core = meta_ref[0]
     heads, rows, _ = keep_out.shape
     mine, peers = pl.ds(core * rows, rows), pl.ds((1 - core) * rows, rows)
     for head in range(heads):
         span = slice(head * HEAD_DIM, (head + 1) * HEAD_DIM)
-        query = query_ref[:, span]
-        query_out[head] = jnp.concatenate([query, jnp.zeros_like(query)], axis=1)
         keep_out[head] = jnp.concatenate([key_ref[mine, span], value_ref[mine, span]], axis=1)
         send_out[head] = jnp.concatenate([key_ref[peers, span], value_ref[peers, span]], axis=1)
 
 
-def pack(core, queries, key_rows, value_rows):
-    side, width = queries.shape
+def pack(meta, key_rows, value_rows):
+    side, width = key_rows.shape
     heads = width // HEAD_DIM
     half = jax.ShapeDtypeStruct((heads, side // 2, LANES), jnp.bfloat16)
     return pl.pallas_call(
         pack_kernel,
-        in_specs=[pl.BlockSpec(memory_space=pltpu.SMEM)] + [pl.BlockSpec(memory_space=pltpu.VMEM)] * 3,
-        out_specs=[pl.BlockSpec(memory_space=pltpu.VMEM)] * 3,
-        out_shape=[jax.ShapeDtypeStruct((heads, side, LANES), jnp.bfloat16), half, half],
+        in_specs=[pl.BlockSpec(memory_space=pltpu.SMEM)] + [pl.BlockSpec(memory_space=pltpu.VMEM)] * 2,
+        out_specs=[pl.BlockSpec(memory_space=pltpu.VMEM)] * 2,
+        out_shape=[half, half],
         name="pack",
-    )(core, queries, key_rows, value_rows)
+    )(meta, key_rows, value_rows)
+
+
+def turn_kernel(meta_ref, query_ref, *refs):
+    outs, held_ref = refs[:-1], refs[-1]
+    for head in range(4):
+        query = query_ref[:, head * HEAD_DIM : (head + 1) * HEAD_DIM]
+        held_ref[head] = jnp.concatenate([query, jnp.zeros_like(query)], axis=1)
+    for turn, out in enumerate(outs):
+        out[...] = held_ref[meta_ref[1] ^ turn]
+
+
+def split_queries(meta, queries):
+    side = queries.shape[0]
+    return pl.pallas_call(
+        turn_kernel,
+        in_specs=[pl.BlockSpec(memory_space=pltpu.SMEM), pl.BlockSpec(memory_space=pltpu.VMEM)],
+        out_specs=[pl.BlockSpec(memory_space=pltpu.VMEM)] * 4,
+        out_shape=[jax.ShapeDtypeStruct((side, LANES), jnp.bfloat16)] * 4,
+        scratch_shapes=[pltpu.VMEM((4, side, LANES), jnp.bfloat16)],
+        name="turns",
+    )(meta, queries)
+
+
+def route_kernel(routes_ref, weight_ref, out_ref):
+    tokens, experts = routes_ref.shape[0], out_ref.shape[1]
+    names = lax.broadcasted_iota(jnp.int32, (tokens, experts), 1)
+    pick = jnp.zeros((tokens, experts), jnp.float32)
+    share = jnp.zeros((tokens, experts), jnp.float32)
+    for k in range(TOPK):
+        named = routes_ref[:, k : k + 1] == names
+        pick = jnp.where(named, 1.0, pick)
+        share = jnp.where(named, weight_ref[:, k : k + 1], share)
+    row = lax.broadcasted_iota(jnp.int32, (tokens, tokens), 0)
+    col = lax.broadcasted_iota(jnp.int32, (tokens, tokens), 1)
+    below = (col < row).astype(jnp.bfloat16)
+    rank = jnp.dot(below, pick.astype(jnp.bfloat16), preferred_element_type=jnp.float32)
+    out_ref[0:tokens] = jnp.where(pick > 0.0, rank, -1.0).astype(jnp.bfloat16)
+    high = share.astype(jnp.bfloat16)
+    out_ref[tokens : 2 * tokens] = high
+    out_ref[2 * tokens :] = (share - high.astype(jnp.float32)).astype(jnp.bfloat16)
+
+
+def route(routes, route_weight, experts):
+    return pl.pallas_call(
+        route_kernel,
+        out_shape=jax.ShapeDtypeStruct((3 * routes.shape[0], experts), jnp.bfloat16),
+        in_specs=[pl.BlockSpec(memory_space=pltpu.VMEM)] * 2,
+        out_specs=pl.BlockSpec(memory_space=pltpu.VMEM),
+        name="route",
+    )(routes, route_weight)
 
 
 GROUP = 4
@@ -92,10 +140,10 @@
             advance(query, step * GROUP, None)
 
         advance(query, own // GROUP * GROUP, own)
-        done = acc_ref[:, HEAD_DIM:].astype(jnp.bfloat16)
+        done = acc_ref[...].T[HEAD_DIM:].astype(jnp.bfloat16)
         slot = meta_ref[5 + turn]
-        out_ref[slot] = done[:rows]
-        out_ref[slot + 1] = done[rows:]
+        out_ref[slot] = done[:, :rows]
+        out_ref[slot + 1] = done[:, rows:]
 
 
 def attention(meta, queries, mine, peer):
@@ -103,7 +151,7 @@
     pairs = 136 * side * side
     return pl.pallas_call(
         attention_kernel,
-        out_shape=jax.ShapeDtypeStruct((16, side // 2, HEAD_DIM), jnp.bfloat16),
+        out_shape=jax.ShapeDtypeStruct((16, HEAD_DIM, side // 2), jnp.bfloat16),
         in_specs=[pl.BlockSpec(memory_space=pltpu.SMEM)]
         + [pl.BlockSpec(memory_space=pltpu.VMEM)] * 4
         + [pl.BlockSpec(memory_space=pl.ANY)] * 2,
@@ -127,26 +175,34 @@
 TAIL = 4
 
 
+def expand(count, slots, experts, first):
+    row = lax.broadcasted_iota(jnp.int32, (count * slots, experts), 0)
+    col = lax.broadcasted_iota(jnp.int32, (count * slots, experts), 1)
+    return (col == first + row // slots).astype(jnp.bfloat16)
+
+
 def dispatch_kernel(
     side_ref,
     attended_ref,
     residual_ref,
     weight_ref,
     gain_ref,
-    main_ref,
-    tail_ref,
+    rank_ref,
     mixed_ref,
     normed_ref,
     out_ref,
     heads_ref,
 ):
-    half = out_ref.shape[2]
+    count, _, half = out_ref.shape
+    tokens, experts = rank_ref.shape
 
     @pl.when(pl.program_id(0) == 0)
     def _():
         for head in range(8):
-            heads_ref[:, head * HEAD_DIM : (head + 1) * HEAD_DIM] = attended_ref[2 * head + side_ref[0]]
-        projected = jnp.dot(heads_ref[...], weight_ref[...], preferred_element_type=jnp.float32)
+            heads_ref[head * HEAD_DIM : (head + 1) * HEAD_DIM] = attended_ref[2 * head + side_ref[0]]
+        projected = lax.dot_general(
+            heads_ref[...], weight_ref[...], (((0,), (0,)), ((), ())), preferred_element_type=jnp.float32
+        )
         mixed = (residual_ref[...].astype(jnp.float32) + projected).astype(jnp.bfloat16)
         mixed_ref[...] = mixed
         mixed = mixed.astype(jnp.float32)
@@ -154,22 +210,31 @@
         normed_ref[...] = (mixed * inverse * gain_ref[...]).astype(jnp.bfloat16)
 
     left, right = normed_ref[:, :half], normed_ref[:, half:]
-    experts = out_ref.shape[0]
-    main, tail = main_ref[...], tail_ref[...]
+    first = pl.program_id(0) * count
+
+    def chosen(slots, lowest):
+        rank = lax.dot_general(
+            expand(count, slots, experts, first),
+            rank_ref[...],
+            (((1,), (1,)), ((), ())),
+            preferred_element_type=jnp.float32,
+        )
+        slot = lowest + lax.broadcasted_iota(jnp.int32, rank.shape, 0) % (slots if lowest == 0 else TAIL)
+        return (rank == slot.astype(jnp.float32)).astype(jnp.bfloat16)
 
     def pick(rows, side):
         return jnp.dot(rows, side, preferred_element_type=jnp.float32)
 
-    out_ref[:, 0:MAIN, :] = pick(main, left).astype(jnp.bfloat16).reshape(experts, MAIN, half)
-    out_ref[:, MAIN : 2 * MAIN, :] = pick(main, right).astype(jnp.bfloat16).reshape(experts, MAIN, half)
-    first = lax.broadcasted_iota(jnp.int32, (tail.shape[0], half), 0) % (2 * TAIL) < TAIL
-    both = jnp.where(first, pick(tail, left), pick(tail, right))
-    out_ref[:, 2 * MAIN :, :] = both.astype(jnp.bfloat16).reshape(experts, 2 * TAIL, half)
-
-
-def dispatch(side, attended, residual, out_weight, gain, main, tail):
+    main, tail = chosen(MAIN, 0), chosen(2 * TAIL, MAIN)
+    out_ref[:, 0:MAIN, :] = pick(main, left).astype(jnp.bfloat16).reshape(count, MAIN, half)
+    out_ref[:, MAIN : 2 * MAIN, :] = pick(main, right).astype(jnp.bfloat16).reshape(count, MAIN, half)
+    early = lax.broadcasted_iota(jnp.int32, (tail.shape[0], half), 0) % (2 * TAIL) < TAIL
+    both = jnp.where(early, pick(tail, left), pick(tail, right))
+    out_ref[:, 2 * MAIN :, :] = both.astype(jnp.bfloat16).reshape(count, 2 * TAIL, half)
+
+
+def dispatch(side, attended, residual, out_weight, gain, ranks, experts):
     tokens, width = residual.shape
-    experts = main.shape[0] // MAIN
     step = 16
     whole = lambda i: (0, 0)
     return pl.pallas_call(
@@ -181,8 +246,7 @@
             pl.BlockSpec(residual.shape, whole),
             pl.BlockSpec(out_weight.shape, whole),
             pl.BlockSpec(gain.shape, whole),
-            pl.BlockSpec((step * MAIN, tokens), lambda i: (i, 0)),
-            pl.BlockSpec((step * 2 * TAIL, tokens), lambda i: (i, 0)),
+            pl.BlockSpec((tokens, experts), whole),
         ],
         out_specs=[
             pl.BlockSpec((tokens, width), whole),
@@ -194,11 +258,11 @@
             jax.ShapeDtypeStruct((tokens, width), jnp.bfloat16),
             jax.ShapeDtypeStruct((experts, 2 * (MAIN + TAIL), width // 2), jnp.bfloat16),
         ],
-        scratch_shapes=[pltpu.VMEM((tokens, 8 * HEAD_DIM), jnp.bfloat16)],
+        scratch_shapes=[pltpu.VMEM((8 * HEAD_DIM, tokens), jnp.bfloat16)],
         compiler_params=pltpu.CompilerParams(vmem_limit_bytes=60 * 2**20),
         cost_estimate=pl.CostEstimate(flops=10**9, bytes_accessed=10**7, transcendentals=0),
         name="dispatch",
-    )(side, attended, residual, out_weight, gain, main, tail)
+    )(side, attended, residual, out_weight, gain, ranks)
 
 
 def expert_kernel(
@@ -209,7 +273,13 @@
     up1,
     down0,
     down1,
+    shared_gate,
+    shared_up,
+    shared_down,
+    mixed_ref,
+    normed_ref,
     out_ref,
+    base_ref,
     spread_ref,
     rows2_ref,
     gate0_ref,
@@ -218,6 +288,9 @@
     up1_ref,
     down0_ref,
     down1_ref,
+    shared_gate_ref,
+    shared_up_ref,
+    shared_down_ref,
     sems,
 ):
     sources, _, half = rows_ref.shape
@@ -233,6 +306,9 @@
                 (up1, up1_ref),
                 (down0, down0_ref),
                 (down1, down1_ref),
+                (shared_gate, shared_gate_ref),
+                (shared_up, shared_up_ref),
+                (shared_down, shared_down_ref),
             )
         )
     ]
@@ -264,15 +340,15 @@
     rows2_ref[mains:, half:] = ends[tails:]
     rows = rows2_ref[...]
 
-    def hidden(gate_ref, up_ref):
-        gate = jnp.dot(rows, gate_ref[0], preferred_element_type=jnp.float32)
-        upward = jnp.dot(rows, up_ref[0], preferred_element_type=jnp.float32)
+    def hidden(rows, gate_matrix, up_matrix):
+        gate = jnp.dot(rows, gate_matrix, preferred_element_type=jnp.float32)
+        upward = jnp.dot(rows, up_matrix, preferred_element_type=jnp.float32)
         return (jax.nn.silu(gate) * upward).astype(jnp.bfloat16)
 
     arrived(0, 1)
-    act0 = hidden(gate0_ref, up0_ref)
+    act0 = hidden(rows, gate0_ref[0], up0_ref[0])
     arrived(2, 3)
-    act1 = hidden(gate1_ref, up1_ref)
+    act1 = hidden(rows, gate1_ref[0], up1_ref[0])
     arrived(4, 5)
     for part in range(2):
         span = pl.ds(part * half, half)
@@ -290,42 +366,73 @@
             )
             out_ref[:, 2 * MAIN :, :] = ends.astype(jnp.bfloat16).reshape(sources, 2 * TAIL, half)
 
-
-def expert(rows, weights):
+    @pl.when(pl.program_id(0) == pl.num_programs(0) - 1)
+    def _():
+        for load in loads[6:]:
+            load.wait()
+        act = hidden(normed_ref[...], shared_gate_ref[...], shared_up_ref[...])
+        base_ref[...] = mixed_ref[...].astype(jnp.float32) + jnp.dot(
+            act, shared_down_ref[...], preferred_element_type=jnp.float32
+        )
+
+
+def expert(rows, weights, mixed, normed):
     step = 16
     block = pl.BlockSpec((step,) + rows.shape[1:], lambda i: (i, 0, 0))
+    whole = pl.BlockSpec(mixed.shape, lambda i: (0, 0))
     return pl.pallas_call(
         expert_kernel,
         grid=(rows.shape[0] // step,),
-        in_specs=[block] + [pl.BlockSpec(memory_space=pl.ANY)] * 6,
-        out_specs=block,
-        out_shape=jax.ShapeDtypeStruct(rows.shape, jnp.bfloat16),
+        in_specs=[block] + [pl.BlockSpec(memory_space=pl.ANY)] * len(weights) + [whole] * 2,
+        out_specs=[block, whole],
+        out_shape=[
+            jax.ShapeDtypeStruct(rows.shape, jnp.bfloat16),
+            jax.ShapeDtypeStruct(mixed.shape, jnp.float32),
+        ],
         scratch_shapes=[
             pltpu.VMEM((step * 2 * TAIL, step * 2 * TAIL), jnp.bfloat16),
             pltpu.VMEM((step * (MAIN + TAIL), 2 * rows.shape[2]), jnp.bfloat16),
         ]
         + [pltpu.VMEM(w.shape, w.dtype) for w in weights]
-        + [pltpu.SemaphoreType.DMA((6,))],
+        + [pltpu.SemaphoreType.DMA((len(weights),))],
         compiler_params=pltpu.CompilerParams(vmem_limit_bytes=60 * 2**20),
         cost_estimate=pl.CostEstimate(flops=8 * 10**9, bytes_accessed=17 * 10**6, transcendentals=10**6),
         name="expert",
-    )(rows, *weights)
-
-
-def combine_kernel(rows_ref, main_ref, left_ref, right_ref, base_ref, out_ref, acc_ref):
-    sources, _, half = rows_ref.shape
+    )(rows, *weights, mixed, normed)
+
+
+def combine_kernel(rows_ref, ranks_ref, base_ref, out_ref, acc_ref):
+    count, _, half = rows_ref.shape
     tokens = base_ref.shape[0]
+    experts = ranks_ref.shape[1]
     at = pl.program_id(0)
 
     @pl.when(at == 0)
     def _():
         acc_ref[...] = base_ref[...]
 
-    ends = rows_ref[:, 2 * MAIN :, :].reshape(sources * 2 * TAIL, half)
-    for part, tail_ref in ((0, left_ref), (1, right_ref)):
-        rows = rows_ref[:, part * MAIN : (part + 1) * MAIN, :].reshape(sources * MAIN, half)
-        total = jnp.dot(main_ref[...], rows, preferred_element_type=jnp.float32) + jnp.dot(
-            tail_ref[...], ends, preferred_element_type=jnp.float32
+    def weights(slots, wanted):
+        spread = lax.dot_general(
+            ranks_ref[...],
+            expand(count, slots, experts, at * count),
+            (((1,), (1,)), ((), ())),
+            preferred_element_type=jnp.float32,
+        )
+        rank = spread[:tokens]
+        slot = wanted(lax.broadcasted_iota(jnp.int32, rank.shape, 1) % slots).astype(jnp.float32)
+        here = rank == slot
+        parts = [jnp.where(here, spread[i * tokens : (i + 1) * tokens], 0.0) for i in (1, 2)]
+        return jnp.concatenate(parts, axis=0).astype(jnp.bfloat16)
+
+    main = weights(MAIN, lambda slot: slot)
+    ends = rows_ref[:, 2 * MAIN :, :].reshape(count * 2 * TAIL, half)
+    for part in range(2):
+        tail = weights(
+            2 * TAIL, lambda slot: jnp.where(slot // TAIL == part, MAIN + slot % TAIL, -2)
+        )
+        rows = rows_ref[:, part * MAIN : (part + 1) * MAIN, :].reshape(count * MAIN, half)
+        total = jnp.dot(main, rows, preferred_element_type=jnp.float32) + jnp.dot(
+            tail, ends, preferred_element_type=jnp.float32
         )
         span = pl.ds(part * half, half)
         acc_ref[:, span] += total[:tokens] + total[tokens:]
@@ -335,7 +442,7 @@
         out_ref[...] = acc_ref[...].astype(jnp.bfloat16)
 
 
-def combine(rows, main, left, right, base):
+def combine(rows, ranks, base):
     step = 16
     whole = lambda i: (0, 0)
     return pl.pallas_call(
@@ -343,9 +450,7 @@
         grid=(rows.shape[0] // step,),
         in_specs=[
             pl.BlockSpec((step,) + rows.shape[1:], lambda i: (i, 0, 0)),
-            pl.BlockSpec((main.shape[0], step * MAIN), lambda i: (0, i)),
-            pl.BlockSpec((main.shape[0], step * 2 * TAIL), lambda i: (0, i)),
-            pl.BlockSpec((main.shape[0], step * 2 * TAIL), lambda i: (0, i)),
+            pl.BlockSpec(ranks.shape, whole),
             pl.BlockSpec(base.shape, whole),
         ],
         out_specs=pl.BlockSpec(base.shape, whole),
@@ -354,7 +459,7 @@
         compiler_params=pltpu.CompilerParams(vmem_limit_bytes=60 * 2**20),
         cost_estimate=pl.CostEstimate(flops=10**9, bytes_accessed=10**7, transcendentals=0),
         name="combine",
-    )(rows, main, left, right, base)
+    )(rows, ranks, base)
 
 
 def local(
@@ -381,13 +486,14 @@
     place = jnp.where(plane % 2 == 1, 15 - spot, spot)
     group, member = place % 8, plane + place // 8 * 4
 
-    query_heads, keep, send = pack(core[None].astype(jnp.int32), queries, key_rows, value_rows)
+    place_meta = jnp.stack([core, member % 4]).astype(jnp.int32)
+    turn_heads = split_queries(place_meta, queries)
+    keep, send = pack(place_meta, key_rows, value_rows)
     swap = [(0, 1), (1, 0)]
     taken = lax.ppermute(send, "tp", swap)
     low, high = jnp.where(core == 0, keep, taken), jnp.where(core == 0, taken, keep)
     order = jnp.stack([low[0], high[0], high[1], low[1], low[2], high[2], high[3], low[3]])
-    order = jnp.broadcast_to(order[:, None], (8,) + order.shape)
-    mine = lax.all_to_all(order.reshape((64,) + order.shape[2:]), "sp", 0, 0, tiled=True)
+    order = jnp.broadcast_to(order[:, None], (8,) + order.shape).reshape((64,) + order.shape[1:])
     turns = []
     for turn in range(4):
         pairs = [
@@ -396,8 +502,10 @@
             for m in range(8)
             for c in range(2)
         ]
-        head = lax.dynamic_index_in_dim(query_heads, (member % 4) ^ turn, 0, keepdims=False)
-        turns.append(lax.ppermute(head, ("sp", "tp"), pairs))
+        turns.append(lax.ppermute(turn_heads[turn], ("sp", "tp"), pairs))
+    ranks = route(routes, route_weight, 64)
+    order, ranks, *turns = lax.optimization_barrier((order, ranks, *turns))
+    mine = lax.all_to_all(order, "sp", 0, 0, tiled=True)
     peer = lax.ppermute(mine, "tp", swap)
     sender = [4 * core + ((member % 4) ^ turn) for turn in range(4)]
     block = [
@@ -411,49 +519,35 @@
     gate_other = lax.ppermute(expert_gate_, "tp", swap)
     up_other = lax.ppermute(expert_up_, "tp", swap)
     down_other = lax.ppermute(expert_down_, "tp", swap)
-    tokens = residual.shape[0]
+    attended, gate_other, up_other, down_other = lax.optimization_barrier(
+        (attended, gate_other, up_other, down_other)
+    )
     attended = lax.all_to_all(attended, ("sp", "tp"), 0, 0, axis_index_groups=devices, tiled=True)
     side = (member // 4)[None].astype(jnp.int32)
 
     experts = lax.axis_size("sp")
-    named = routes[:, :, None] == jnp.arange(experts, dtype=jnp.int32)
-    pick = jnp.any(named, axis=1)
-    share = jnp.sum(jnp.where(named, route_weight[:, :, None], 0.0), axis=1)
-    below = jnp.tril(jnp.ones((tokens, tokens), jnp.bfloat16), -1)
-    rank = jnp.dot(below, pick.astype(jnp.bfloat16), preferred_element_type=jnp.float32)
-    rank = jnp.where(pick, rank, -1.0).astype(jnp.int32)
-
-    def slots(numbers):
-        numbers = jnp.asarray(numbers, jnp.int32)
-        send = rank.T[:, None, :] == numbers[None, :, None]
-        back = rank[:, :, None] == numbers[None, None, :]
-        send = send.astype(jnp.bfloat16).reshape(-1, tokens)
-        weight = jnp.where(back, share[:, :, None], 0.0).reshape(tokens, -1)
-        high = weight.astype(jnp.bfloat16)
-        low = (weight - high.astype(jnp.float32)).astype(jnp.bfloat16)
-        return send, jnp.concatenate([high, low], axis=0)
-
-    ends = list(range(MAIN, MAIN + TAIL))
-    none = [-2] * TAIL
-    send_main, back_main = slots(list(range(MAIN)))
-    send_tail, _ = slots(ends + ends)
-    _, back_left = slots(ends + none)
-    _, back_right = slots(none + ends)
     mixed, normed, outgoing = dispatch(
-        side, attended, residual, out_weight, norm_gain[None, :], send_main, send_tail
+        side, attended, residual, out_weight, norm_gain[None, :], ranks, experts
     )
     incoming = lax.all_to_all(outgoing, "sp", 0, 0, tiled=True)
-    shared_gate_out = jnp.dot(normed, shared_gate, preferred_element_type=jnp.float32)
-    shared_up_out = jnp.dot(normed, shared_up, preferred_element_type=jnp.float32)
-    shared_act = (jax.nn.silu(shared_gate_out) * shared_up_out).astype(jnp.bfloat16)
-    base = mixed.astype(jnp.float32) + jnp.dot(
-        shared_act, shared_down, preferred_element_type=jnp.float32
-    )
-    result = expert(
-        incoming, (expert_gate, expert_up, gate_other, up_other, expert_down, down_other)
+    result, base = expert(
+        incoming,
+        (
+            expert_gate,
+            expert_up,
+            gate_other,
+            up_other,
+            expert_down,
+            down_other,
+            shared_gate,
+            shared_up,
+            shared_down,
+        ),
+        mixed,
+        normed,
     )
     returned = lax.all_to_all(result, "sp", 0, 0, tiled=True)
-    return combine(returned, back_main, back_left, back_right, base)
+    return combine(returned, ranks, base)
 
 
 def solution(mesh):

time: 302 us -> 293 us (0.970)
  blocking collectives: 42 us -> 177 us
  waiting for transfers between devices: 137 us -> 17.5 us
  starting transfers between devices: 36 us -> 16.7 us
  Pallas kernels: 66.2 us -> 72 us
  matrix products: 4.05 us -> 0 us
  other arithmetic: 4.68 us -> 1.56 us
    all_to_all x1 -> x3, blocking collectives: 42 us -> 177 us  [the longest x1 70.5 us: local(): incoming = lax.all_to_all(outgoing, 'sp', 0, 0, tiled=True)]
    all_to_all x2 -> x0, waiting for transfers between devices: 119 us -> none  [the longest x1 61.4 us: local(): incoming = lax.all_to_all(outgoing, 'sp', 0, 0, tiled=True)]
    all_to_all x2 -> x0, starting transfers between devices: 17.7 us -> none  [the longest x1 11.3 us: local(): returned = lax.all_to_all(result, 'sp', 0, 0, tiled=True)]
    unnamed x34 -> x24, local copies, waits for them, and re-layouts: 0.72 us -> 5.65 us
    all_to_all x1, starting transfers between devices: 7.91 us -> 3.53 us  [local(): lax.all_to_all(attended, ('sp', 'tp'), 0, 0, axis_index_groups=devices, t...]
    dot_general x3 -> x0, matrix products: 4.05 us -> none  [the longest x1 3.4 us: local(): jnp.dot(shared_act, shared_down, preferred_element_type=jnp.float32)]
    pallas_call x1 -> x3, Pallas kernels: 35.1 us -> 38.6 us  [the longest x1 34.9 us: attention(): pl.pallas_call(attention_kernel, out_shape=jax.ShapeDtypeStruct((16, HEAD...]
    ppermute x1, waiting for transfers between devices: 0.01 us -> 3.25 us  [local(): peer = lax.ppermute(mine, 'tp', swap)]
  transfers between devices with their start and end apart: 12 -> 10, of which waited for: 8 -> 3; matrix products, arithmetic and copies ran while one was open for 4% -> 2% of each run, Pallas kernels for 0% -> 13%
where the time goes in v4:
time: 293 us; the launch traced here: 292 us
  blocking collectives  177 us (60%)
  Pallas kernels  72 us (25%)
  waiting for transfers between devices  17.5 us (6%)
  starting transfers between devices  16.7 us (6%)
  local copies, waits for them, and re-layouts  6.82 us (2%)
    all_to_all x1, blocking collectives, local(): incoming = lax.all_to_all(outgoing, 'sp', 0, 0, tiled=True)  70.5 us
    all_to_all x1, blocking collectives, local(): returned = lax.all_to_all(result, 'sp', 0, 0, tiled=True)  69.1 us
    all_to_all x1, blocking collectives, local(): mine = lax.all_to_all(order, 'sp', 0, 0, tiled=True)  37.6 us
    pallas_call x1, Pallas kernels, attention(): pl.pallas_call(attention_kernel, out_shape=jax.ShapeDtypeStruct((16, HEAD...  34.9 us
    pallas_call x1, Pallas kernels, expert(): pl.pallas_call(expert_kernel, grid=(rows.shape[0] // step,), in_specs=[bl...  17.7 us
    ppermute x4, starting transfers between devices, local(): turns.append(lax.ppermute(turn_heads[turn], ('sp', 'tp'), pairs))  11.7 us
    all_to_all x1, waiting for transfers between devices, local(): lax.all_to_all(attended, ('sp', 'tp'), 0, 0, axis_index_groups=devices, t...  10.2 us
    pallas_call x1, Pallas kernels, combine(): pl.pallas_call(combine_kernel, grid=(rows.shape[0] // step,), in_specs=[p...  7 us
  transfers between devices with their start and end apart: 10, of which 3 were waited for; matrix products, arithmetic and copies ran while one was open for 2% of the time, Pallas kernels for 13%

profile of v4, /device:TPU:0, one launch (start us, length us, event | category | flops | bytes accessed | tf_op | source)
XLA Modules:
  0.0 292.0 jit_solution(12462100867157025338)
XLA Ops:
  0.0 0.6 pad_add_fusion.meta_ref
  0.6 1.8 pack.1
  2.4 0.0 collective-permute-start
  2.4 1.7 turns.1
  4.2 1.5 collective-permute-start.1
  5.6 6.7 %collective-permute-start.2 = (bf16[256,128]{1,0:T(8,128)(2,1)}, bf16[256,128]{1,0:T(8,128)(2,1)S(1)}, u32[]{:S(2)}, u32[]{:S(2)}) collective-permute-start(bf16[256,128]{1,0:T(8,128)(2,1)} %get-tuple-element.32), channel_id=1, source_target_pairs={{0,62},{1,46},{62,0},{63,16},{64,126},{65,110},{126,64},{127,80},{... | collective-permute-start | bytes 196616 | tf_op jit(solution)/shard_map/ppermute | solution.py:505
  12.3 3.6 %collective-permute-start.3 = (bf16[256,128]{1,0:T(8,128)(2,1)}, bf16[256,128]{1,0:T(8,128)(2,1)S(1)}, u32[]{:S(2)}, u32[]{:S(2)}) collective-permute-start(bf16[256,128]{1,0:T(8,128)(2,1)} %get-tuple-element.33), channel_id=1, source_target_pairs={{0,64},{1,80},{62,126},{63,110},{64,0},{65,16},{126,62},{127,46},{... | collective-permute-start | bytes 196616 | tf_op jit(solution)/shard_map/ppermute | solution.py:505
  15.9 0.0 collective-permute-start.4
  15.9 1.4 copy.15.routes_ref
  17.3 1.4 copy.16.weight_ref
  18.7 1.9 route.1.rank_ref.ranks_ref
  20.7 0.0 collective-permute-done
  20.7 0.9 broadcast_select_fusion
  21.7 0.0 collective-permute-done.1.q0
  21.7 0.0 copy-start.5
  21.7 0.0 collective-permute-done.2.q1
  21.7 0.0 copy-start.6
  21.7 0.0 collective-permute-done.3.q2
  21.7 0.0 copy-start.7
  21.7 4.1 %collective-permute-done.4.q3 = bf16[256,128]{1,0:T(8,128)(2,1)S(1)} collective-permute-done((bf16[256,128]{1,0:T(8,128)(2,1)}, bf16[256,128]{1,0:T(8,128)(2,1)S(1)}, u32[]{:S(2)}, u32[]{:S(2)}) %collective-permute-start.4) | collective-permute-done | bytes 65568 | tf_op jit(solution)/shard_map/ppermute | solution.py:505
  25.8 0.5 broadcast_in_dim.13
  26.3 0.0 copy-start.2
  26.3 37.6 %all_to_all.20.mine_ref = bf16[64,128,128]{2,1,0:T(8,128)(2,1)S(1)} all-to-all(bf16[64,128,128]{2,1,0:T(8,128)(2,1)S(1)} %bitcast.13), channel_id=1, replica_groups=mesh['sp'=64,'tp'=2] {'sp'}, dimensions={0} | all-to-all | bytes 4194304 | tf_op jit(solution)/shard_map/all_to_all | solution.py:508
  63.9 0.0 copy-done.5
  63.9 0.0 copy-done.6
  63.9 0.0 copy-done.7
  63.9 0.0 copy-done.8
  64.0 0.5 collective-permute-start.5
  64.5 0.7 stack.50.meta_ref
  65.1 3.3 %collective-permute-done.5.peer_ref = bf16[64,128,128]{2,1,0:T(8,128)(2,1)} collective-permute-done((bf16[64,128,128]{2,1,0:T(8,128)(2,1)S(1)}, bf16[64,128,128]{2,1,0:T(8,128)(2,1)}, u32[]{:S(2)}, u32[]{:S(2)}) %collective-permute-start.5) | collective-permute-done | bytes 2097184 | tf_op jit(solution)/shard_map/ppermute | solution.py:509
  68.4 0.0 copy-done.2
  68.4 0.4 collective-permute-start.6
  68.8 0.1 collective-permute-start.7
  68.9 0.4 collective-permute-start.8
  69.3 34.9 %attend.1 = bf16[16,64,128]{2,1,0:T(8,128)(2,1)} custom-call(s32[9]{0:T(128)} %stack.50.meta_ref, bf16[256,128]{1,0:T(8,128)(2,1)} %copy-done.5, bf16[256,128]{1,0:T(8,128)(2,1)} %copy-done.6, bf16[256,128]{1,0:T(8,128)(2,1)} %copy-done.7, bf16[256,128]{1,0:T(8,128)(2,1)} %copy-done.8, bf16[64,128,128]{2,1,0:T(8,128)(2,1)} %copy-done, ...), custom_call_target="tpu_custom_call" | custom-call | flops 13690208256 | bytes 6291456 | tf_op jit(solution)/shard_map/attend/pallas_call | solution.py:152
  104.2 0.0 collective-permute-done.6.gate1
  104.2 1.0 copy-done.3
  105.2 0.0 collective-permute-done.7.up1
  105.2 1.0 copy-done.4
  106.3 0.0 collective-permute-done.8.down1
  106.3 3.5 %all-to-all-start.1 = ((bf16[16,64,128]{2,1,0:T(8,128)(2,1)}), bf16[16,64,128]{2,1,0:T(8,128)(2,1)S(1)}, u32[]{:S(2)}, u32[]{:S(2)}) async-start(bf16[16,64,128]{2,1,0:T(8,128)(2,1)} %attend.1), calls=%async_computation.1 | async-start | bytes 524288 | tf_op jit(solution)/shard_map/all_to_all | solution.py:525
  109.8 10.2 %all-to-all-done.1.attended_ref = bf16[16,64,128]{2,1,0:T(8,128)(2,1)S(1)} async-done(((bf16[16,64,128]{2,1,0:T(8,128)(2,1)}), bf16[16,64,128]{2,1,0:T(8,128)(2,1)S(1)}, u32[]{:S(2)}, u32[]{:S(2)}) %all-to-all-start.1) | async-done | bytes 262176 | tf_op jit(solution)/shard_map/all_to_all | solution.py:525
  120.0 0.7 copy-done.1
  120.7 6.9 %dispatch.1 = (bf16[128,2048]{1,0:T(8,128)(2,1)}, bf16[128,2048]{1,0:T(8,128)(2,1)}, bf16[64,40,1024]{2,1,0:T(8,128)(2,1)}) custom-call(s32[1]{0:T(128)} %bitcast.side_ref, bf16[16,64,128]{2,1,0:T(8,128)(2,1)} %copy-done.1, bf16[128,2048]{1,0:T(8,128)(2,1)} %residual_ref.1, bf16[512,2048]{1,0:T(8,128)(2,1)} %weight_ref.2, f32[1,2048]{1,0:T(1,128)} %bitcast.14, ...), custom_call_target="tpu_custom_call" | custom-call | flops 1000000000 | bytes 10000000 | tf_op jit(solution)/shard_map/dispatch/pallas_call | solution.py:240
  127.7 70.5 %all_to_all.21.rows_ref = bf16[64,40,1024]{2,1,0:T(8,128)(2,1)} all-to-all(bf16[64,40,1024]{2,1,0:T(8,128)(2,1)} %get-tuple-element.45), channel_id=1, replica_groups=mesh['sp'=64,'tp'=2] {'sp'}, dimensions={0} | all-to-all | bytes 10485760 | tf_op jit(solution)/shard_map/all_to_all | solution.py:532
  198.2 17.7 %expert.1 = (bf16[64,40,1024]{2,1,0:T(8,128)(2,1)}, f32[128,2048]{1,0:T(8,128)}) custom-call(bf16[64,40,1024]{2,1,0:T(8,128)(2,1)} %all_to_all.21.rows_ref, bf16[1,2048,256]{2,1,0:T(8,128)(2,1)} %gate0.1, bf16[1,2048,256]{2,1,0:T(8,128)(2,1)} %up0.1, bf16[1,2048,256]{2,1,0:T(8,128)(2,1)} %copy-done.3, bf16[1,2048,256]{2,1,0:T(8,128)(2,1)} %copy-done.4, ...), custom_call_target="tpu_custom_call" | custom-call | flops 8000000000 | bytes 17000000 | tf_op jit(solution)/shard_map/expert/pallas_call | solution.py:383
  215.9 69.1 %all_to_all.22.rows_ref = bf16[64,40,1024]{2,1,0:T(8,128)(2,1)} all-to-all(bf16[64,40,1024]{2,1,0:T(8,128)(2,1)} %get-tuple-element.51), channel_id=1, replica_groups=mesh['sp'=64,'tp'=2] {'sp'}, dimensions={0} | all-to-all | bytes 10485760 | tf_op jit(solution)/shard_map/all_to_all | solution.py:549
  285.0 7.0 %combine.1 = bf16[128,2048]{1,0:T(8,128)(2,1)} custom-call(bf16[64,40,1024]{2,1,0:T(8,128)(2,1)} %all_to_all.22.rows_ref, bf16[384,64]{1,0:T(8,128)(2,1)} %route.1.rank_ref.ranks_ref, f32[128,2048]{1,0:T(8,128)} %get-tuple-element.52.base_ref), custom_call_target="tpu_custom_call" | custom-call | flops 1000000000 | bytes 10000000 | tf_op jit(solution)/shard_map/combine/pallas_call | solution.py:448
  (11 shorter events, 0.1 us)
Async XLA Ops:
  2.4 18.2 %collective-permute-start = (bf16[4,128,128]{2,1,0:T(8,128)(2,1)}, bf16[4,128,128]{2,1,0:T(8,128)(2,1)S(1)}, u32[]{:S(2)}, u32[]{:S(2)}) collective-permute-start(bf16[4,128,128]{2,1,0:T(8,128)(2,1)} %get-tuple-element.30), channel_id=1, source_target_pairs={{0,1},{1,0},{2,3},{3,2},{4,5},{5,4},{6,7},{7,6},{8,9},{9,8},{10,11... | collective-permute-start | bytes 393224 | tf_op jit(solution)/shard_map/ppermute | solution.py:493
  4.2 17.5 %collective-permute-start.1 = (bf16[256,128]{1,0:T(8,128)(2,1)}, bf16[256,128]{1,0:T(8,128)(2,1)S(1)}, u32[]{:S(2)}, u32[]{:S(2)}) collective-permute-start(bf16[256,128]{1,0:T(8,128)(2,1)} %get-tuple-element.31), channel_id=1, source_target_pairs={{0,0},{1,16},{62,62},{63,46},{64,64},{65,80},{126,126},{127,110},{... | collective-permute-start | bytes 196616 | tf_op jit(solution)/shard_map/ppermute | solution.py:505
  5.6 16.1 %collective-permute-start.2 = (bf16[256,128]{1,0:T(8,128)(2,1)}, bf16[256,128]{1,0:T(8,128)(2,1)S(1)}, u32[]{:S(2)}, u32[]{:S(2)}) collective-permute-start(bf16[256,128]{1,0:T(8,128)(2,1)} %get-tuple-element.32), channel_id=1, source_target_pairs={{0,62},{1,46},{62,0},{63,16},{64,126},{65,110},{126,64},{127,80},{... | collective-permute-start | bytes 196616 | tf_op jit(solution)/shard_map/ppermute | solution.py:505
  12.3 9.4 %collective-permute-start.3 = (bf16[256,128]{1,0:T(8,128)(2,1)}, bf16[256,128]{1,0:T(8,128)(2,1)S(1)}, u32[]{:S(2)}, u32[]{:S(2)}) collective-permute-start(bf16[256,128]{1,0:T(8,128)(2,1)} %get-tuple-element.33), channel_id=1, source_target_pairs={{0,64},{1,80},{62,126},{63,110},{64,0},{65,16},{126,62},{127,46},{... | collective-permute-start | bytes 196616 | tf_op jit(solution)/shard_map/ppermute | solution.py:505
  15.9 9.9 %collective-permute-start.4 = (bf16[256,128]{1,0:T(8,128)(2,1)}, bf16[256,128]{1,0:T(8,128)(2,1)S(1)}, u32[]{:S(2)}, u32[]{:S(2)}) collective-permute-start(bf16[256,128]{1,0:T(8,128)(2,1)} %get-tuple-element.34), channel_id=1, source_target_pairs={{0,126},{1,110},{62,64},{63,80},{64,62},{65,46},{126,0},{127,16},{... | collective-permute-start | bytes 196616 | tf_op jit(solution)/shard_map/ppermute | solution.py:505
  21.7 42.2 %copy-start.5 = (bf16[256,128]{1,0:T(8,128)(2,1)}, bf16[256,128]{1,0:T(8,128)(2,1)S(1)}, u32[]{:S(2)}) copy-start(bf16[256,128]{1,0:T(8,128)(2,1)S(1)} %collective-permute-done.1.q0) | copy-start | bytes 196612
  21.7 42.2 %copy-start.6 = (bf16[256,128]{1,0:T(8,128)(2,1)}, bf16[256,128]{1,0:T(8,128)(2,1)S(1)}, u32[]{:S(2)}) copy-start(bf16[256,128]{1,0:T(8,128)(2,1)S(1)} %collective-permute-done.2.q1) | copy-start | bytes 196612
  21.7 42.2 %copy-start.7 = (bf16[256,128]{1,0:T(8,128)(2,1)}, bf16[256,128]{1,0:T(8,128)(2,1)S(1)}, u32[]{:S(2)}) copy-start(bf16[256,128]{1,0:T(8,128)(2,1)S(1)} %collective-permute-done.3.q2) | copy-start | bytes 196612
  25.8 38.1 %copy-start.8 = (bf16[256,128]{1,0:T(8,128)(2,1)}, bf16[256,128]{1,0:T(8,128)(2,1)S(1)}, u32[]{:S(2)}) copy-start(bf16[256,128]{1,0:T(8,128)(2,1)S(1)} %collective-permute-done.4.q3) | copy-start | bytes 196612
  26.3 42.1 %copy-start.2 = (bf16[1,2048,256]{2,1,0:T(8,128)(2,1)S(1)}, bf16[1,2048,256]{2,1,0:T(8,128)(2,1)}, u32[]{:S(2)}) copy-start(bf16[1,2048,256]{2,1,0:T(8,128)(2,1)} %gate0.1) | copy-start | bytes 3145732
  64.0 5.3 %copy-start = (bf16[64,128,128]{2,1,0:T(8,128)(2,1)}, bf16[64,128,128]{2,1,0:T(8,128)(2,1)S(1)}, u32[]{:S(2)}) copy-start(bf16[64,128,128]{2,1,0:T(8,128)(2,1)S(1)} %all_to_all.20.mine_ref) | copy-start | bytes 6291460
  64.0 4.4 %collective-permute-start.5 = (bf16[64,128,128]{2,1,0:T(8,128)(2,1)S(1)}, bf16[64,128,128]{2,1,0:T(8,128)(2,1)}, u32[]{:S(2)}, u32[]{:S(2)}) collective-permute-start(bf16[64,128,128]{2,1,0:T(8,128)(2,1)S(1)} %all_to_all.20.mine_ref), channel_id=1, source_target_pairs={{0,1},{1,0},{2,3},{3,2},{4,5},{5,4},{6,7},{7,6},{8,9},{9,8},{10,11... | collective-permute-start | bytes 6291464 | tf_op jit(solution)/shard_map/ppermute | solution.py:509
  68.4 35.8 %collective-permute-start.6 = (bf16[1,2048,256]{2,1,0:T(8,128)(2,1)S(1)}, bf16[1,2048,256]{2,1,0:T(8,128)(2,1)S(1)}, u32[]{:S(2)}, u32[]{:S(2)}) collective-permute-start(bf16[1,2048,256]{2,1,0:T(8,128)(2,1)S(1)} %copy-done.2), channel_id=1, source_target_pairs={{0,1},{1,0},{2,3},{3,2},{4,5},{5,4},{6,7},{7,6},{8,9},{9,8},{10,11... | collective-permute-start | bytes 3145736 | tf_op jit(solution)/shard_map/ppermute | solution.py:519
  68.8 36.5 %collective-permute-start.7 = (bf16[1,2048,256]{2,1,0:T(8,128)(2,1)}, bf16[1,2048,256]{2,1,0:T(8,128)(2,1)S(1)}, u32[]{:S(2)}, u32[]{:S(2)}) collective-permute-start(bf16[1,2048,256]{2,1,0:T(8,128)(2,1)} %up0.1), channel_id=1, source_target_pairs={{0,1},{1,0},{2,3},{3,2},{4,5},{5,4},{6,7},{7,6},{8,9},{9,8},{10,11... | collective-permute-start | bytes 3145736 | tf_op jit(solution)/shard_map/ppermute | solution.py:520
  68.9 37.4 %collective-permute-start.8 = (bf16[1,256,2048]{2,1,0:T(8,128)(2,1)}, bf16[1,256,2048]{2,1,0:T(8,128)(2,1)}, u32[]{:S(2)}, u32[]{:S(2)}) collective-permute-start(bf16[1,256,2048]{2,1,0:T(8,128)(2,1)} %down0.1), channel_id=1, source_target_pairs={{0,1},{1,0},{2,3},{3,2},{4,5},{5,4},{6,7},{7,6},{8,9},{9,8},{10,11... | collective-permute-start | bytes 3145736 | tf_op jit(solution)/shard_map/ppermute | solution.py:521
  104.2 1.0 copy-start.3
  105.2 1.0 copy-start.4
  106.3 13.7 %all-to-all-start.1 = ((bf16[16,64,128]{2,1,0:T(8,128)(2,1)}), bf16[16,64,128]{2,1,0:T(8,128)(2,1)S(1)}, u32[]{:S(2)}, u32[]{:S(2)}) async-start(bf16[16,64,128]{2,1,0:T(8,128)(2,1)} %attend.1), calls=%async_computation.1 | async-start | bytes 524288 | tf_op jit(solution)/shard_map/all_to_all | solution.py:525
  120.0 0.7 copy-start.1

commit v5 on v4

v5 whole, which is shorter than its diff:
```python
import jax
import jax.numpy as jnp
from jax import lax
from jax.experimental import pallas as pl
from jax.experimental.pallas import tpu as pltpu
from jax.sharding import PartitionSpec as P

HEAD_DIM = 64
LANES = 128
TOPK = 8
LOG2E = 1.4426950408889634
norm_eps = 1e-06


VMEM_BYTES = 67043328


def pack_kernel(core_ref, query_ref, key_ref, value_ref, keep_out, send_out):
    heads, rows = keep_out.shape[0], query_ref.shape[0] // 2
    core = core_ref[0]
    for out, half in ((keep_out, core), (send_out, 1 - core)):
        own = pl.ds(half * rows, rows)
        for head in range(heads):
            span = slice(head * HEAD_DIM, (head + 1) * HEAD_DIM)
            out[head, :rows] = jnp.concatenate([key_ref[own, span], value_ref[own, span]], axis=1)
            query = query_ref[own, span].reshape(rows // 16, 16, HEAD_DIM)
            query = jnp.concatenate([query[:, :8], query[:, 8:]], axis=2)
            out[head, rows:] = query.reshape(rows // 2, LANES)


def pack(core, queries, key_rows, value_rows):
    side, width = key_rows.shape
    half = jax.ShapeDtypeStruct((width // HEAD_DIM, side // 2 + side // 4, LANES), jnp.bfloat16)
    return pl.pallas_call(
        pack_kernel,
        in_specs=[pl.BlockSpec(memory_space=pltpu.SMEM)] + [pl.BlockSpec(memory_space=pltpu.VMEM)] * 3,
        out_specs=[pl.BlockSpec(memory_space=pltpu.VMEM)] * 2,
        out_shape=[half, half],
        name="pack",
    )(core, queries, key_rows, value_rows)


def spread_kernel(core_ref, keep_ref, taken_ref, out_ref):
    head = pl.program_id(0)
    mine = head // 4 == core_ref[0]
    count, depth, _ = out_ref.shape
    rows = depth - 8
    held = jnp.where(mine, keep_ref[head % 4], taken_ref[head % 4])
    for chip in range(count):
        out_ref[chip, :rows] = held[:rows]
        out_ref[chip, rows:] = held[rows + 8 * chip : rows + 8 * chip + 8]


def spread(core, keep, taken):
    heads = 8
    rows = keep.shape[1] * 2 // 3
    whole = pl.BlockSpec(keep.shape, lambda i: (0, 0, 0))
    return pl.pallas_call(
        spread_kernel,
        grid=(heads,),
        in_specs=[pl.BlockSpec(memory_space=pltpu.SMEM), whole, whole],
        out_specs=pl.BlockSpec((8, rows + 8, LANES), lambda i: (i, 0, 0)),
        out_shape=jax.ShapeDtypeStruct((8 * heads, rows + 8, LANES), jnp.bfloat16),
        compiler_params=pltpu.CompilerParams(vmem_limit_bytes=VMEM_BYTES),
        name="spread",
    )(core, keep, taken)


def route_kernel(routes_ref, weight_ref, out_ref):
    tokens, experts = routes_ref.shape[1], out_ref.shape[0] // 3
    names = lax.broadcasted_iota(jnp.int32, (experts, tokens), 0)
    pick = jnp.zeros((experts, tokens), jnp.float32)
    share = jnp.zeros((experts, tokens), jnp.float32)
    for k in range(TOPK):
        named = routes_ref[k : k + 1, :] == names
        pick = jnp.where(named, 1.0, pick)
        share = jnp.where(named, weight_ref[k : k + 1, :], share)
    row = lax.broadcasted_iota(jnp.int32, (tokens, tokens), 0)
    col = lax.broadcasted_iota(jnp.int32, (tokens, tokens), 1)
    above = (row < col).astype(jnp.bfloat16)
    rank = jnp.dot(pick.astype(jnp.bfloat16), above, preferred_element_type=jnp.float32)
    out_ref[0:experts] = jnp.where(pick > 0.0, rank, -1.0).astype(jnp.bfloat16)
    high = share.astype(jnp.bfloat16)
    out_ref[experts : 2 * experts] = high
    out_ref[2 * experts :] = (share - high.astype(jnp.float32)).astype(jnp.bfloat16)


def route(routes, route_weight, experts):
    return pl.pallas_call(
        route_kernel,
        out_shape=jax.ShapeDtypeStruct((3 * experts, routes.shape[1]), jnp.bfloat16),
        in_specs=[pl.BlockSpec(memory_space=pltpu.VMEM)] * 2,
        out_specs=pl.BlockSpec(memory_space=pltpu.VMEM),
        name="route",
    )(routes, route_weight)


GROUP = 4


def attention_kernel(meta_ref, mine_ref, peer_ref, out_ref, kv_ref, tri_ref, raw_ref, query_ref, acc_ref, sems):
    core, offset = meta_ref[0], meta_ref[1]
    side = tri_ref.shape[0]
    rows = side // 2
    loads = [
        pltpu.make_async_copy(mine_ref.at[:, pl.ds(rows, 8)], raw_ref, sems.at[0]),
        pltpu.make_async_copy(mine_ref.at[:, pl.ds(0, rows)], kv_ref.at[:, pl.ds(core * rows, rows)], sems.at[1]),
        pltpu.make_async_copy(
            peer_ref.at[:, pl.ds(0, rows)], kv_ref.at[:, pl.ds((1 - core) * rows, rows)], sems.at[2]
        ),
    ]
    for load in loads:
        load.start()
    row = lax.broadcasted_iota(jnp.int32, (side, side), 0)
    col = lax.broadcasted_iota(jnp.int32, (side, side), 1)
    tri_ref[...] = (row > col).astype(jnp.float32)
    loads[0].wait()
    raw = raw_ref[...]
    none = jnp.zeros(raw.shape[:2] + (HEAD_DIM,), jnp.bfloat16)
    early = jnp.concatenate([raw[:, :, :HEAD_DIM], none], axis=2)
    late = jnp.concatenate([raw[:, :, HEAD_DIM:], none], axis=2)
    query_ref[...] = jnp.concatenate([early, late], axis=1).reshape(query_ref.shape)
    loads[1].wait()
    loads[2].wait()

    def advance(tile, first, skip, diagonal):
        query = query_ref[tile, skip:]
        keys = [kv_ref[first + i] for i in range(GROUP)]
        scores = [
            lax.dot_general(query, kv, (((1,), (1,)), ((), ())), preferred_element_type=jnp.float32)
            * (HEAD_DIM**-0.5 * LOG2E)
            for kv in keys
        ]
        costs = [jnp.maximum(s, 0.0) + jnp.log2(1.0 + jnp.exp2(-jnp.abs(s))) for s in scores]
        slacks = [s - c for s, c in zip(scores, costs)]
        if diagonal is not None:
            shape = scores[0].shape
            place = skip + lax.broadcasted_iota(jnp.int32, shape, 0)
            place = place // 16 * side + place % 16 + offset - lax.broadcasted_iota(jnp.int32, shape, 1)
            live = [place > (diagonal + i) * side for i in range(GROUP)]
            costs = [jnp.where(l, c, 0.0) for l, c in zip(live, costs)]
        tri = tri_ref[...]
        insides = [jnp.dot(c, tri, preferred_element_type=jnp.float32) for c in costs]
        acc = acc_ref[skip:]
        for i in range(GROUP):
            weight = jnp.exp2(slacks[i] - insides[i])
            if diagonal is not None:
                weight = jnp.where(live[i], weight, 0.0)
            part = jnp.dot(weight.astype(jnp.bfloat16), keys[i], preferred_element_type=jnp.float32)
            acc = acc * jnp.exp2(-(insides[i][:, 0:1] + costs[i][:, 0:1])) + part
        acc_ref[skip:] = acc

    @pl.loop(0, 4)
    def _(tile):
        acc_ref[...] = jnp.zeros_like(acc_ref)

        @pl.loop(0, 4 * tile)
        def _(step):
            advance(tile, step * GROUP, 0, None)

        for step in range(4):
            advance(tile, 16 * tile + step * GROUP, step * GROUP * 16, step * GROUP)
        done = acc_ref[:, HEAD_DIM:].reshape(16, 16, HEAD_DIM)
        done = jnp.concatenate([done[:, :8], done[:, 8:]], axis=2).astype(jnp.bfloat16)
        out_ref[pl.ds(tile * 16, 16)] = done


def attention(meta, mine, peer):
    chips, depth, _ = mine.shape
    side = 2 * (depth - 8)
    pairs = 136 * side * side
    return pl.pallas_call(
        attention_kernel,
        out_shape=jax.ShapeDtypeStruct((chips, 8, LANES), jnp.bfloat16),
        in_specs=[pl.BlockSpec(memory_space=pltpu.SMEM)] + [pl.BlockSpec(memory_space=pl.ANY)] * 2,
        out_specs=pl.BlockSpec(memory_space=pltpu.VMEM),
        scratch_shapes=[
            pltpu.VMEM((chips, side, LANES), jnp.bfloat16),
            pltpu.VMEM((side, side), jnp.float32),
            pltpu.VMEM((chips, 8, LANES), jnp.bfloat16),
            pltpu.VMEM((4, side, LANES), jnp.bfloat16),
            pltpu.VMEM((side, LANES), jnp.float32),
            pltpu.SemaphoreType.DMA((3,)),
        ],
        compiler_params=pltpu.CompilerParams(vmem_limit_bytes=VMEM_BYTES),
        cost_estimate=pl.CostEstimate(
            flops=pairs * 2 * 768, bytes_accessed=6 * 2**20, transcendentals=pairs * 3
        ),
        name="attend",
    )(meta, mine, peer)


MAIN = 16
TAIL = 4


def expand(count, slots, experts, first):
    row = lax.broadcasted_iota(jnp.int32, (count * slots, experts), 0)
    col = lax.broadcasted_iota(jnp.int32, (count * slots, experts), 1)
    return (col == first + row // slots).astype(jnp.bfloat16)


def dispatch_kernel(
    attended_ref,
    residual_ref,
    weight_ref,
    gain_ref,
    rank_ref,
    mixed_ref,
    normed_ref,
    out_ref,
    heads_ref,
):
    count, _, half = out_ref.shape
    experts, tokens = rank_ref.shape

    @pl.when(pl.program_id(0) == 0)
    def _():
        for head in range(8):
            rows = attended_ref[8 * head : 8 * head + 8]
            rows = jnp.concatenate([rows[:, :, :HEAD_DIM], rows[:, :, HEAD_DIM:]], axis=1)
            heads_ref[:, head * HEAD_DIM : (head + 1) * HEAD_DIM] = rows.reshape(tokens, HEAD_DIM)
        projected = jnp.dot(heads_ref[...], weight_ref[...], preferred_element_type=jnp.float32)
        mixed = (residual_ref[...].astype(jnp.float32) + projected).astype(jnp.bfloat16)
        mixed_ref[...] = mixed
        mixed = mixed.astype(jnp.float32)
        inverse = lax.rsqrt(jnp.mean(mixed * mixed, axis=1, keepdims=True) + norm_eps)
        normed_ref[...] = (mixed * inverse * gain_ref[...]).astype(jnp.bfloat16)

    left, right = normed_ref[:, :half], normed_ref[:, half:]
    first = pl.program_id(0) * count

    def chosen(slots, lowest):
        rank = jnp.dot(
            expand(count, slots, experts, first), rank_ref[...], preferred_element_type=jnp.float32
        )
        slot = lowest + lax.broadcasted_iota(jnp.int32, rank.shape, 0) % (slots if lowest == 0 else TAIL)
        return (rank == slot.astype(jnp.float32)).astype(jnp.bfloat16)

    def pick(rows, side):
        return jnp.dot(rows, side, preferred_element_type=jnp.float32)

    main, tail = chosen(MAIN, 0), chosen(2 * TAIL, MAIN)
    out_ref[:, 0:MAIN, :] = pick(main, left).astype(jnp.bfloat16).reshape(count, MAIN, half)
    out_ref[:, MAIN : 2 * MAIN, :] = pick(main, right).astype(jnp.bfloat16).reshape(count, MAIN, half)
    early = lax.broadcasted_iota(jnp.int32, (tail.shape[0], half), 0) % (2 * TAIL) < TAIL
    both = jnp.where(early, pick(tail, left), pick(tail, right))
    out_ref[:, 2 * MAIN :, :] = both.astype(jnp.bfloat16).reshape(count, 2 * TAIL, half)


def dispatch(attended, residual, out_weight, gain, ranks, experts):
    tokens, width = residual.shape
    step = 16
    whole = lambda i: (0, 0)
    return pl.pallas_call(
        dispatch_kernel,
        grid=(experts // step,),
        in_specs=[
            pl.BlockSpec(attended.shape, lambda i: (0, 0, 0)),
            pl.BlockSpec(residual.shape, whole),
            pl.BlockSpec(out_weight.shape, whole),
            pl.BlockSpec(gain.shape, whole),
            pl.BlockSpec((experts, tokens), whole),
        ],
        out_specs=[
            pl.BlockSpec((tokens, width), whole),
            pl.BlockSpec((tokens, width), whole),
            pl.BlockSpec((step, 2 * (MAIN + TAIL), width // 2), lambda i: (i, 0, 0)),
        ],
        out_shape=[
            jax.ShapeDtypeStruct((tokens, width), jnp.bfloat16),
            jax.ShapeDtypeStruct((tokens, width), jnp.bfloat16),
            jax.ShapeDtypeStruct((experts, 2 * (MAIN + TAIL), width // 2), jnp.bfloat16),
        ],
        scratch_shapes=[pltpu.VMEM((tokens, 8 * HEAD_DIM), jnp.bfloat16)],
        compiler_params=pltpu.CompilerParams(vmem_limit_bytes=VMEM_BYTES),
        cost_estimate=pl.CostEstimate(flops=10**9, bytes_accessed=10**7, transcendentals=0),
        name="dispatch",
    )(attended, residual, out_weight, gain, ranks)


def expert_kernel(
    rows_ref,
    gate0,
    up0,
    gate1,
    up1,
    down0,
    down1,
    shared_gate,
    shared_up,
    shared_down,
    mixed_ref,
    normed_ref,
    out_ref,
    base_ref,
    spread_ref,
    rows2_ref,
    gate0_ref,
    up0_ref,
    gate1_ref,
    up1_ref,
    down0_ref,
    down1_ref,
    shared_gate_ref,
    shared_up_ref,
    shared_down_ref,
    sems,
):
    sources, _, half = rows_ref.shape
    tails = sources * TAIL
    first_step = pl.program_id(0) == 0
    loads = [
        pltpu.make_async_copy(source, target, sems.at[i])
        for i, (source, target) in enumerate(
            (
                (gate0, gate0_ref),
                (up0, up0_ref),
                (gate1, gate1_ref),
                (up1, up1_ref),
                (down0, down0_ref),
                (down1, down1_ref),
                (shared_gate, shared_gate_ref),
                (shared_up, shared_up_ref),
                (shared_down, shared_down_ref),
            )
        )
    ]

    def arrived(*which):
        @pl.when(first_step)
        def _():
            for i in which:
                loads[i].wait()

    @pl.when(first_step)
    def _():
        for load in loads:
            load.start()
        row = lax.broadcasted_iota(jnp.int32, (2 * tails, 2 * tails), 0)
        col = lax.broadcasted_iota(jnp.int32, (2 * tails, 2 * tails), 1)
        slot = row % tails
        home = slot // TAIL * (2 * TAIL) + row // tails * TAIL + slot % TAIL
        spread_ref[...] = (home == col).astype(jnp.bfloat16)

    spread = spread_ref[...]
    mains = sources * MAIN
    rows2_ref[:mains, :half] = rows_ref[:, 0:MAIN, :].reshape(mains, half)
    rows2_ref[:mains, half:] = rows_ref[:, MAIN : 2 * MAIN, :].reshape(mains, half)
    ends = jnp.dot(
        spread, rows_ref[:, 2 * MAIN :, :].reshape(2 * tails, half), preferred_element_type=jnp.float32
    ).astype(jnp.bfloat16)
    rows2_ref[mains:, :half] = ends[:tails]
    rows2_ref[mains:, half:] = ends[tails:]
    rows = rows2_ref[...]

    def hidden(rows, gate_matrix, up_matrix):
        gate = jnp.dot(rows, gate_matrix, preferred_element_type=jnp.float32)
        upward = jnp.dot(rows, up_matrix, preferred_element_type=jnp.float32)
        return (jax.nn.silu(gate) * upward).astype(jnp.bfloat16)

    arrived(0, 1)
    act0 = hidden(rows, gate0_ref[0], up0_ref[0])
    arrived(2, 3)
    act1 = hidden(rows, gate1_ref[0], up1_ref[0])
    arrived(4, 5)
    for part in range(2):
        span = pl.ds(part * half, half)
        result = jnp.dot(act0, down0_ref[0, :, span], preferred_element_type=jnp.float32) + jnp.dot(
            act1, down1_ref[0, :, span], preferred_element_type=jnp.float32
        )
        result = result.astype(jnp.bfloat16)
        out_ref[:, part * MAIN : (part + 1) * MAIN, :] = result[:mains].reshape(sources, MAIN, half)
        if part == 0:
            first = result[mains:]
        else:
            ends = jnp.concatenate([first, result[mains:]], axis=0)
            ends = lax.dot_general(
                spread, ends, (((0,), (0,)), ((), ())), preferred_element_type=jnp.float32
            )
            out_ref[:, 2 * MAIN :, :] = ends.astype(jnp.bfloat16).reshape(sources, 2 * TAIL, half)

    @pl.when(pl.program_id(0) == pl.num_programs(0) - 1)
    def _():
        for load in loads[6:]:
            load.wait()
        act = hidden(normed_ref[...], shared_gate_ref[...], shared_up_ref[...])
        base_ref[...] = mixed_ref[...].astype(jnp.float32) + jnp.dot(
            act, shared_down_ref[...], preferred_element_type=jnp.float32
        )


def expert(rows, weights, mixed, normed):
    step = 16
    block = pl.BlockSpec((step,) + rows.shape[1:], lambda i: (i, 0, 0))
    whole = pl.BlockSpec(mixed.shape, lambda i: (0, 0))
    return pl.pallas_call(
        expert_kernel,
        grid=(rows.shape[0] // step,),
        in_specs=[block] + [pl.BlockSpec(memory_space=pl.ANY)] * len(weights) + [whole] * 2,
        out_specs=[block, whole],
        out_shape=[
            jax.ShapeDtypeStruct(rows.shape, jnp.bfloat16),
            jax.ShapeDtypeStruct(mixed.shape, jnp.float32),
        ],
        scratch_shapes=[
            pltpu.VMEM((step * 2 * TAIL, step * 2 * TAIL), jnp.bfloat16),
            pltpu.VMEM((step * (MAIN + TAIL), 2 * rows.shape[2]), jnp.bfloat16),
        ]
        + [pltpu.VMEM(w.shape, w.dtype) for w in weights]
        + [pltpu.SemaphoreType.DMA((len(weights),))],
        compiler_params=pltpu.CompilerParams(vmem_limit_bytes=VMEM_BYTES),
        cost_estimate=pl.CostEstimate(flops=8 * 10**9, bytes_accessed=17 * 10**6, transcendentals=10**6),
        name="expert",
    )(rows, *weights, mixed, normed)


def combine_kernel(rows_ref, ranks_ref, base_ref, out_ref, acc_ref):
    count, _, half = rows_ref.shape
    tokens = base_ref.shape[0]
    experts = ranks_ref.shape[0] // 3
    at = pl.program_id(0)

    @pl.when(at == 0)
    def _():
        acc_ref[...] = base_ref[...]

    def weights(slots, wanted):
        chosen = expand(count, slots, experts, at * count)
        rank, high, low = [
            jnp.dot(chosen, ranks_ref[i * experts : (i + 1) * experts], preferred_element_type=jnp.float32)
            for i in range(3)
        ]
        slot = wanted(lax.broadcasted_iota(jnp.int32, rank.shape, 0) % slots).astype(jnp.float32)
        here = rank == slot
        parts = [jnp.where(here, part, 0.0) for part in (high, low)]
        return jnp.concatenate(parts, axis=1).T.astype(jnp.bfloat16)

    main = weights(MAIN, lambda slot: slot)
    ends = rows_ref[:, 2 * MAIN :, :].reshape(count * 2 * TAIL, half)
    for part in range(2):
        tail = weights(
            2 * TAIL, lambda slot: jnp.where(slot // TAIL == part, MAIN + slot % TAIL, -2)
        )
        rows = rows_ref[:, part * MAIN : (part + 1) * MAIN, :].reshape(count * MAIN, half)
        total = jnp.dot(main, rows, preferred_element_type=jnp.float32) + jnp.dot(
            tail, ends, preferred_element_type=jnp.float32
        )
        span = pl.ds(part * half, half)
        acc_ref[:, span] += total[:tokens] + total[tokens:]

    @pl.when(at == pl.num_programs(0) - 1)
    def _():
        out_ref[...] = acc_ref[...].astype(jnp.bfloat16)


def combine(rows, ranks, base):
    step = 16
    whole = lambda i: (0, 0)
    return pl.pallas_call(
        combine_kernel,
        grid=(rows.shape[0] // step,),
        in_specs=[
            pl.BlockSpec((step,) + rows.shape[1:], lambda i: (i, 0, 0)),
            pl.BlockSpec(ranks.shape, whole),
            pl.BlockSpec(base.shape, whole),
        ],
        out_specs=pl.BlockSpec(base.shape, whole),
        out_shape=jax.ShapeDtypeStruct(base.shape, jnp.bfloat16),
        scratch_shapes=[pltpu.VMEM(base.shape, jnp.float32)],
        compiler_params=pltpu.CompilerParams(vmem_limit_bytes=VMEM_BYTES),
        cost_estimate=pl.CostEstimate(flops=10**9, bytes_accessed=10**7, transcendentals=0),
        name="combine",
    )(rows, ranks, base)


def local(
    queries,
    key_rows,
    value_rows,
    residual,
    out_weight,
    norm_gain,
    routes,
    route_weight,
    expert_gate,
    expert_up,
    expert_down,
    shared_gate,
    shared_up,
    shared_down,
):
    core = lax.axis_index("tp")
    offset = 128 * core + 16 * (lax.axis_index("sp") % 8)
    swap = [(0, 1), (1, 0)]
    cores = core[None].astype(jnp.int32)
    keep, send = pack(cores, queries, key_rows, value_rows)
    taken = lax.ppermute(send, "tp", swap)
    mine = lax.all_to_all(spread(cores, keep, taken), "sp", 0, 0, tiled=True)
    peer = lax.ppermute(mine, "tp", swap)
    mine, routes, route_weight = lax.optimization_barrier((mine, routes, route_weight))
    ranks = route(routes.T, route_weight.T, 64)
    peer, ranks, expert_gate_, expert_up_, expert_down_ = lax.optimization_barrier(
        (peer, ranks, expert_gate, expert_up, expert_down)
    )
    attended = attention(jnp.stack([core, offset]).astype(jnp.int32), mine, peer)
    gate_other = lax.ppermute(expert_gate_, "tp", swap)
    up_other = lax.ppermute(expert_up_, "tp", swap)
    down_other = lax.ppermute(expert_down_, "tp", swap)
    attended, gate_other, up_other, down_other = lax.optimization_barrier(
        (attended, gate_other, up_other, down_other)
    )
    attended = lax.all_to_all(attended, "sp", 0, 0, tiled=True)
    experts = lax.axis_size("sp")
    mixed, normed, outgoing = dispatch(
        attended, residual, out_weight, norm_gain[None, :], ranks, experts
    )
    incoming = lax.all_to_all(outgoing, "sp", 0, 0, tiled=True)
    result, base = expert(
        incoming,
        (
            expert_gate,
            expert_up,
            gate_other,
            up_other,
            expert_down,
            down_other,
            shared_gate,
            shared_up,
            shared_down,
        ),
        mixed,
        normed,
    )
    returned = lax.all_to_all(result, "sp", 0, 0, tiled=True)
    return combine(returned, ranks, base)


def solution(mesh):
    return jax.shard_map(
        local,
        mesh=mesh,
        in_specs=(
            P("sp", "tp"),
            P("sp", "tp"),
            P("sp", "tp"),
            P(("sp", "tp"), None),
            P(),
            P(),
            P(("sp", "tp"), None),
            P(("sp", "tp"), None),
            P("sp", None, "tp"),
            P("sp", None, "tp"),
            P("sp", "tp", None),
            P(),
            P(),
            P(),
        ),
        out_specs=P(("sp", "tp"), None),
        check_vma=False,
    )
```

time: 293 us -> 279 us (0.952)
  blocking collectives: 177 us -> 197 us
  starting transfers between devices: 16.7 us -> 0.65 us
  waiting for transfers between devices: 17.5 us -> 4.2 us
  local copies, waits for them, and re-layouts: 6.82 us -> 1.37 us
    all_to_all x1 -> x2, blocking collectives: 37.6 us -> 59 us  [the longest x1 43.5 us: local(): mine = lax.all_to_all(spread(cores, keep, taken), 'sp', 0, 0, tiled=True)]
    ppermute x4 -> x0, starting transfers between devices: 11.7 us -> none  [local(): turns.append(lax.ppermute(turn_heads[turn], ('sp', 'tp'), pairs))]
    all_to_all x1 -> x0, waiting for transfers between devices: 10.2 us -> none  [local(): lax.all_to_all(attended, ('sp', 'tp'), 0, 0, axis_index_groups=devices, t...]
    unnamed x24 -> x2, local copies, waits for them, and re-layouts: 5.65 us -> 1.37 us
    ppermute x4 -> x0, waiting for transfers between devices: 4.07 us -> none  [local(): turns.append(lax.ppermute(turn_heads[turn], ('sp', 'tp'), pairs))]
    all_to_all x1 -> x0, starting transfers between devices: 3.53 us -> none  [local(): lax.all_to_all(attended, ('sp', 'tp'), 0, 0, axis_index_groups=devices, t...]
  transfers between devices with their start and end apart: 10 -> 5, of which waited for: 3 -> 2; matrix products, arithmetic and copies ran while one was open for 2% -> 0% of each run, Pallas kernels for 13% -> 13%
where the time goes in v5:
time: 279 us; the launch traced here: 278 us
  blocking collectives  197 us (71%)
  Pallas kernels  74.8 us (27%)
  waiting for transfers between devices  4.2 us (2%)
    all_to_all x1, blocking collectives, local(): incoming = lax.all_to_all(outgoing, 'sp', 0, 0, tiled=True)  68.9 us
    all_to_all x1, blocking collectives, local(): returned = lax.all_to_all(result, 'sp', 0, 0, tiled=True)  68.9 us
    all_to_all x1, blocking collectives, local(): mine = lax.all_to_all(spread(cores, keep, taken), 'sp', 0, 0, tiled=True)  43.5 us
    pallas_call x1, Pallas kernels, attention(): pl.pallas_call(attention_kernel, out_shape=jax.ShapeDtypeStruct((chips, 8...  35.3 us
    pallas_call x1, Pallas kernels, expert(): pl.pallas_call(expert_kernel, grid=(rows.shape[0] // step,), in_specs=[bl...  17.7 us
    all_to_all x1, blocking collectives, local(): attended = lax.all_to_all(attended, 'sp', 0, 0, tiled=True)  15.5 us
    pallas_call x1, Pallas kernels, combine(): pl.pallas_call(combine_kernel, grid=(rows.shape[0] // step,), in_specs=[p...  7.39 us
    pallas_call x1, Pallas kernels, dispatch(): pl.pallas_call(dispatch_kernel, grid=(experts // step,), in_specs=[pl.Blo...  6.9 us
  transfers between devices with their start and end apart: 5, of which 2 were waited for; matrix products, arithmetic and copies ran while one was open for 0% of the time, Pallas kernels for 13%

profile of v5, /device:TPU:0, one launch (start us, length us, event | category | flops | bytes accessed | tf_op | source)
XLA Modules:
  0.0 278.5 jit_solution(4527539500790005543)
XLA Ops:
  0.0 1.9 pack.1
  1.9 0.0 collective-permute-start
  1.9 1.8 collective-permute-done.taken_ref
  3.7 4.2 %spread.1 = bf16[64,136,128]{2,1,0:T(8,128)(2,1)} custom-call(s32[1]{0:T(128)} %bitcast.core_ref, bf16[4,192,128]{2,1,0:T(8,128)(2,1)} %get-tuple-element.24.keep_ref, bf16[4,192,128]{2,1,0:T(8,128)(2,1)} %collective-permute-done.taken_ref), custom_call_target="tpu_custom_call" | custom-call | tf_op jit(solution)/shard_map/spread/pallas_call | solution.py:58
  7.9 43.5 %all_to_all.20.mine_ref = bf16[64,136,128]{2,1,0:T(8,128)(2,1)S(1)} all-to-all(bf16[64,136,128]{2,1,0:T(8,128)(2,1)} %spread.1), channel_id=1, replica_groups=mesh['sp'=64,'tp'=2] {'sp'}, dimensions={0} | all-to-all | bytes 4456448 | tf_op jit(solution)/shard_map/all_to_all | solution.py:499
  51.4 0.0 copy-start
  51.4 1.4 copy-done
  52.7 0.0 collective-permute-start.1
  52.7 0.6 pad_add_fusion.meta_ref
  53.3 1.5 route.1.rank_ref.ranks_ref
  54.8 2.4 collective-permute-done.1.peer_ref
  57.2 0.1 collective-permute-start.2
  57.4 0.4 collective-permute-start.3
  57.7 0.1 collective-permute-start.4
  57.9 35.3 %attend.1 = bf16[64,8,128]{2,1,0:T(8,128)(2,1)} custom-call(s32[2]{0:T(128)} %pad_add_fusion.meta_ref, bf16[64,136,128]{2,1,0:T(8,128)(2,1)} %copy-done, bf16[64,136,128]{2,1,0:T(8,128)(2,1)} %collective-permute-done.1.peer_ref), custom_call_target="tpu_custom_call" | custom-call | flops 13690208256 | bytes 6291456 | tf_op jit(solution)/shard_map/attend/pallas_call | solution.py:172
  93.2 0.0 collective-permute-done.2.gate1
  93.2 0.0 collective-permute-done.3.up1
  93.2 0.0 collective-permute-done.4.down1
  93.2 15.5 %all_to_all.21.attended_ref = bf16[64,8,128]{2,1,0:T(8,128)(2,1)} all-to-all(bf16[64,8,128]{2,1,0:T(8,128)(2,1)} %attend.1), channel_id=1, replica_groups=mesh['sp'=64,'tp'=2] {'sp'}, dimensions={0} | all-to-all | bytes 262144 | tf_op jit(solution)/shard_map/all_to_all | solution.py:513
  108.7 6.9 %dispatch.1 = (bf16[128,2048]{1,0:T(8,128)(2,1)}, bf16[128,2048]{1,0:T(8,128)(2,1)}, bf16[64,40,1024]{2,1,0:T(8,128)(2,1)}) custom-call(bf16[64,8,128]{2,1,0:T(8,128)(2,1)} %all_to_all.21.attended_ref, bf16[128,2048]{1,0:T(8,128)(2,1)} %residual_ref.1, bf16[512,2048]{1,0:T(8,128)(2,1)} %weight_ref.1, f32[1,2048]{1,0:T(1,128)} %bitcast.7, ...), custom_call_target="tpu_custom_call" | custom-call | flops 1000000000 | bytes 10000000 | tf_op jit(solution)/shard_map/dispatch/pallas_call | solution.py:255
  115.6 68.9 %all_to_all.22.rows_ref = bf16[64,40,1024]{2,1,0:T(8,128)(2,1)} all-to-all(bf16[64,40,1024]{2,1,0:T(8,128)(2,1)} %get-tuple-element.35), channel_id=1, replica_groups=mesh['sp'=64,'tp'=2] {'sp'}, dimensions={0} | all-to-all | bytes 10485760 | tf_op jit(solution)/shard_map/all_to_all | solution.py:518
  184.5 17.7 %expert.1 = (bf16[64,40,1024]{2,1,0:T(8,128)(2,1)}, f32[128,2048]{1,0:T(8,128)}) custom-call(bf16[64,40,1024]{2,1,0:T(8,128)(2,1)} %all_to_all.22.rows_ref, bf16[1,2048,256]{2,1,0:T(8,128)(2,1)} %gate0.1, bf16[1,2048,256]{2,1,0:T(8,128)(2,1)} %up0.1, bf16[1,2048,256]{2,1,0:T(8,128)(2,1)} %collective-permute-done.2.gate1, ...), custom_call_target="tpu_custom_call" | custom-call | flops 8000000000 | bytes 17000000 | tf_op jit(solution)/shard_map/expert/pallas_call | solution.py:397
  202.2 68.9 %all_to_all.23.rows_ref = bf16[64,40,1024]{2,1,0:T(8,128)(2,1)} all-to-all(bf16[64,40,1024]{2,1,0:T(8,128)(2,1)} %get-tuple-element.41), channel_id=1, replica_groups=mesh['sp'=64,'tp'=2] {'sp'}, dimensions={0} | all-to-all | bytes 10485760 | tf_op jit(solution)/shard_map/all_to_all | solution.py:535
  271.1 7.4 %combine.1 = bf16[128,2048]{1,0:T(8,128)(2,1)} custom-call(bf16[64,40,1024]{2,1,0:T(8,128)(2,1)} %all_to_all.23.rows_ref, bf16[192,128]{1,0:T(8,128)(2,1)} %route.1.rank_ref.ranks_ref, f32[128,2048]{1,0:T(8,128)} %get-tuple-element.42.base_ref), custom_call_target="tpu_custom_call" | custom-call | flops 1000000000 | bytes 10000000 | tf_op jit(solution)/shard_map/combine/pallas_call | solution.py:460
Async XLA Ops:
  1.9 1.8 collective-permute-start
  51.4 1.4 copy-start
  52.7 4.5 %collective-permute-start.1 = (bf16[64,136,128]{2,1,0:T(8,128)(2,1)S(1)}, bf16[64,136,128]{2,1,0:T(8,128)(2,1)}, u32[]{:S(2)}, u32[]{:S(2)}) collective-permute-start(bf16[64,136,128]{2,1,0:T(8,128)(2,1)S(1)} %all_to_all.20.mine_ref), channel_id=1, source_target_pairs={{0,1},{1,0},{2,3},{3,2},{4,5},{5,4},{6,7},{7,6},{8,9},{9,8},{10,11... | collective-permute-start | bytes 6684680 | tf_op jit(solution)/shard_map/ppermute | solution.py:500
  57.2 35.9 %collective-permute-start.2 = (bf16[1,2048,256]{2,1,0:T(8,128)(2,1)}, bf16[1,2048,256]{2,1,0:T(8,128)(2,1)}, u32[]{:S(2)}, u32[]{:S(2)}) collective-permute-start(bf16[1,2048,256]{2,1,0:T(8,128)(2,1)} %gate0.1), channel_id=1, source_target_pairs={{0,1},{1,0},{2,3},{3,2},{4,5},{5,4},{6,7},{7,6},{8,9},{9,8},{10,11... | collective-permute-start | bytes 3145736 | tf_op jit(solution)/shard_map/ppermute | solution.py:507
  57.4 35.8 %collective-permute-start.3 = (bf16[1,2048,256]{2,1,0:T(8,128)(2,1)}, bf16[1,2048,256]{2,1,0:T(8,128)(2,1)}, u32[]{:S(2)}, u32[]{:S(2)}) collective-permute-start(bf16[1,2048,256]{2,1,0:T(8,128)(2,1)} %up0.1), channel_id=1, source_target_pairs={{0,1},{1,0},{2,3},{3,2},{4,5},{5,4},{6,7},{7,6},{8,9},{9,8},{10,11... | collective-permute-start | bytes 3145736 | tf_op jit(solution)/shard_map/ppermute | solution.py:508
  57.7 35.4 %collective-permute-start.4 = (bf16[1,256,2048]{2,1,0:T(8,128)(2,1)}, bf16[1,256,2048]{2,1,0:T(8,128)(2,1)}, u32[]{:S(2)}, u32[]{:S(2)}) collective-permute-start(bf16[1,256,2048]{2,1,0:T(8,128)(2,1)} %down0.1), channel_id=1, source_target_pairs={{0,1},{1,0},{2,3},{3,2},{4,5},{5,4},{6,7},{7,6},{8,9},{9,8},{10,11... | collective-permute-start | bytes 3145736 | tf_op jit(solution)/shard_map/ppermute | solution.py:509

commit v6 on v5

--- a/solution.py
+++ b/solution.py
@@ -40,28 +40,33 @@
     )(core, queries, key_rows, value_rows)
 
 
-def spread_kernel(core_ref, keep_ref, taken_ref, out_ref):
-    head = pl.program_id(0)
-    mine = head // 4 == core_ref[0]
-    count, depth, _ = out_ref.shape
+def spread_kernel(core_ref, keep_ref, taken_ref, out_ref, held_ref, sems):
+    chips, depth, _ = held_ref.shape
+    heads = chips // 8
     rows = depth - 8
-    held = jnp.where(mine, keep_ref[head % 4], taken_ref[head % 4])
-    for chip in range(count):
-        out_ref[chip, :rows] = held[:rows]
-        out_ref[chip, rows:] = held[rows + 8 * chip : rows + 8 * chip + 8]
+    copies = []
+    for head in range(heads):
+        mine = head // 4 == core_ref[0]
+        held = jnp.where(mine, keep_ref[head % 4], taken_ref[head % 4])
+        for chip in range(8):
+            held_ref[8 * head + chip, :rows] = held[:rows]
+            held_ref[8 * head + chip, rows:] = held[rows + 8 * chip : rows + 8 * chip + 8]
+        span = pl.ds(8 * head, 8)
+        copies.append(pltpu.make_async_copy(held_ref.at[span], out_ref.at[span], sems.at[head]))
+        copies[-1].start()
+    for copy in copies:
+        copy.wait()
 
 
 def spread(core, keep, taken):
-    heads = 8
-    rows = keep.shape[1] * 2 // 3
-    whole = pl.BlockSpec(keep.shape, lambda i: (0, 0, 0))
+    shape = (64, keep.shape[1] * 2 // 3 + 8, LANES)
     return pl.pallas_call(
         spread_kernel,
-        grid=(heads,),
-        in_specs=[pl.BlockSpec(memory_space=pltpu.SMEM), whole, whole],
-        out_specs=pl.BlockSpec((8, rows + 8, LANES), lambda i: (i, 0, 0)),
-        out_shape=jax.ShapeDtypeStruct((8 * heads, rows + 8, LANES), jnp.bfloat16),
-        compiler_params=pltpu.CompilerParams(vmem_limit_bytes=VMEM_BYTES),
+        in_specs=[pl.BlockSpec(memory_space=pltpu.SMEM)] + [pl.BlockSpec(memory_space=pltpu.VMEM)] * 2,
+        out_specs=pl.BlockSpec(memory_space=pl.ANY),
+        out_shape=jax.ShapeDtypeStruct(shape, jnp.bfloat16),
+        scratch_shapes=[pltpu.VMEM(shape, jnp.bfloat16), pltpu.SemaphoreType.DMA((8,))],
+        compiler_params=pltpu.CompilerParams(vmem_limit_bytes=VMEM_BYTES - 2**20),
         name="spread",
     )(core, keep, taken)
 
@@ -98,17 +103,25 @@
 GROUP = 4
 
 
-def attention_kernel(meta_ref, mine_ref, peer_ref, out_ref, kv_ref, tri_ref, raw_ref, query_ref, acc_ref, sems):
+PIECES = 16
+
+
+def attention_kernel(meta_ref, mine, peer, out_ref, kv_ref, raw_ref, tri_ref, query_ref, acc_ref, sems):
     core, offset = meta_ref[0], meta_ref[1]
     side = tri_ref.shape[0]
     rows = side // 2
-    loads = [
-        pltpu.make_async_copy(mine_ref.at[:, pl.ds(rows, 8)], raw_ref, sems.at[0]),
-        pltpu.make_async_copy(mine_ref.at[:, pl.ds(0, rows)], kv_ref.at[:, pl.ds(core * rows, rows)], sems.at[1]),
-        pltpu.make_async_copy(
-            peer_ref.at[:, pl.ds(0, rows)], kv_ref.at[:, pl.ds((1 - core) * rows, rows)], sems.at[2]
-        ),
-    ]
+    span = kv_ref.shape[0] // PIECES
+    first_rows = pl.ds(pl.multiple_of(core * rows, rows), rows)
+    other_rows = pl.ds(pl.multiple_of((1 - core) * rows, rows), rows)
+    loads = [pltpu.make_async_copy(mine.at[:, pl.ds(rows, 8)], raw_ref, sems.at[2 * PIECES])]
+    for piece in range(PIECES):
+        chips = pl.ds(piece * span, span)
+        for i, (source, place) in enumerate(((mine, first_rows), (peer, other_rows))):
+            loads.append(
+                pltpu.make_async_copy(
+                    source.at[chips, pl.ds(0, rows)], kv_ref.at[chips, place], sems.at[2 * piece + i]
+                )
+            )
     for load in loads:
         load.start()
     row = lax.broadcasted_iota(jnp.int32, (side, side), 0)
@@ -120,8 +133,8 @@
     early = jnp.concatenate([raw[:, :, :HEAD_DIM], none], axis=2)
     late = jnp.concatenate([raw[:, :, HEAD_DIM:], none], axis=2)
     query_ref[...] = jnp.concatenate([early, late], axis=1).reshape(query_ref.shape)
-    loads[1].wait()
-    loads[2].wait()
+    for load in loads[1:]:
+        load.wait()
 
     def advance(tile, first, skip, diagonal):
         query = query_ref[tile, skip:]
@@ -150,19 +163,22 @@
             acc = acc * jnp.exp2(-(insides[i][:, 0:1] + costs[i][:, 0:1])) + part
         acc_ref[skip:] = acc
 
-    @pl.loop(0, 4)
+    blocks = query_ref.shape[1] // 16
+    steps = blocks // GROUP
+
+    @pl.loop(0, query_ref.shape[0])
     def _(tile):
         acc_ref[...] = jnp.zeros_like(acc_ref)
 
-        @pl.loop(0, 4 * tile)
+        @pl.loop(0, steps * tile)
         def _(step):
             advance(tile, step * GROUP, 0, None)
 
-        for step in range(4):
-            advance(tile, 16 * tile + step * GROUP, step * GROUP * 16, step * GROUP)
-        done = acc_ref[:, HEAD_DIM:].reshape(16, 16, HEAD_DIM)
+        for step in range(steps):
+            advance(tile, blocks * tile + step * GROUP, step * GROUP * 16, step * GROUP)
+        done = acc_ref[:, HEAD_DIM:].reshape(blocks, 16, HEAD_DIM)
         done = jnp.concatenate([done[:, :8], done[:, 8:]], axis=2).astype(jnp.bfloat16)
-        out_ref[pl.ds(tile * 16, 16)] = done
+        out_ref[pl.ds(tile * blocks, blocks)] = done
 
 
 def attention(meta, mine, peer):
@@ -172,15 +188,19 @@
     return pl.pallas_call(
         attention_kernel,
         out_shape=jax.ShapeDtypeStruct((chips, 8, LANES), jnp.bfloat16),
-        in_specs=[pl.BlockSpec(memory_space=pltpu.SMEM)] + [pl.BlockSpec(memory_space=pl.ANY)] * 2,
+        in_specs=[
+            pl.BlockSpec(memory_space=pltpu.SMEM),
+            pl.BlockSpec(memory_space=pl.ANY),
+            pl.BlockSpec(memory_space=pl.ANY),
+        ],
         out_specs=pl.BlockSpec(memory_space=pltpu.VMEM),
         scratch_shapes=[
             pltpu.VMEM((chips, side, LANES), jnp.bfloat16),
+            pltpu.VMEM((chips, 8, LANES), jnp.bfloat16),
             pltpu.VMEM((side, side), jnp.float32),
-            pltpu.VMEM((chips, 8, LANES), jnp.bfloat16),
-            pltpu.VMEM((4, side, LANES), jnp.bfloat16),
-            pltpu.VMEM((side, LANES), jnp.float32),
-            pltpu.SemaphoreType.DMA((3,)),
+            pltpu.VMEM((2, 2 * side, LANES), jnp.bfloat16),
+            pltpu.VMEM((2 * side, LANES), jnp.float32),
+            pltpu.SemaphoreType.DMA((2 * PIECES + 1,)),
         ],
         compiler_params=pltpu.CompilerParams(vmem_limit_bytes=VMEM_BYTES),
         cost_estimate=pl.CostEstimate(
@@ -198,6 +218,21 @@
     row = lax.broadcasted_iota(jnp.int32, (count * slots, experts), 0)
     col = lax.broadcasted_iota(jnp.int32, (count * slots, experts), 1)
     return (col == first + row // slots).astype(jnp.bfloat16)
+
+
+STEP = 16
+
+
+def copy_group(source, target, sems, start, count, parts):
+    each = count // parts
+    return [
+        pltpu.make_async_copy(
+            source.at[pl.ds(start + i * each, each)],
+            target.at[pl.ds(start + i * each, each)],
+            sems.at[start // each + i],
+        )
+        for i in range(parts)
+    ]
 
 
 def dispatch_kernel(
@@ -250,7 +285,7 @@
 
 def dispatch(attended, residual, out_weight, gain, ranks, experts):
     tokens, width = residual.shape
-    step = 16
+    step = 32
     whole = lambda i: (0, 0)
     return pl.pallas_call(
         dispatch_kernel,
@@ -279,8 +314,11 @@
     )(attended, residual, out_weight, gain, ranks)
 
 
+PASS = 16
+
+
 def expert_kernel(
-    rows_ref,
+    rows,
     gate0,
     up0,
     gate1,
@@ -290,12 +328,14 @@
     shared_gate,
     shared_up,
     shared_down,
-    mixed_ref,
-    normed_ref,
-    out_ref,
+    mixed,
+    normed,
+    out,
     base_ref,
     spread_ref,
+    rows_ref,
     rows2_ref,
+    out_ref,
     gate0_ref,
     up0_ref,
     gate1_ref,
@@ -305,114 +345,138 @@
     shared_gate_ref,
     shared_up_ref,
     shared_down_ref,
+    mixed_ref,
+    normed_ref,
+    row_sems,
     sems,
+    out_sems,
 ):
-    sources, _, half = rows_ref.shape
-    tails = sources * TAIL
-    first_step = pl.program_id(0) == 0
-    loads = [
-        pltpu.make_async_copy(source, target, sems.at[i])
-        for i, (source, target) in enumerate(
-            (
-                (gate0, gate0_ref),
-                (up0, up0_ref),
-                (gate1, gate1_ref),
-                (up1, up1_ref),
-                (down0, down0_ref),
-                (down1, down1_ref),
-                (shared_gate, shared_gate_ref),
-                (shared_up, shared_up_ref),
-                (shared_down, shared_down_ref),
-            )
-        )
-    ]
-
-    def arrived(*which):
-        @pl.when(first_step)
-        def _():
-            for i in which:
-                loads[i].wait()
-
-    @pl.when(first_step)
-    def _():
-        for load in loads:
-            load.start()
-        row = lax.broadcasted_iota(jnp.int32, (2 * tails, 2 * tails), 0)
-        col = lax.broadcasted_iota(jnp.int32, (2 * tails, 2 * tails), 1)
-        slot = row % tails
-        home = slot // TAIL * (2 * TAIL) + row // tails * TAIL + slot % TAIL
-        spread_ref[...] = (home == col).astype(jnp.bfloat16)
-
-    spread = spread_ref[...]
-    mains = sources * MAIN
-    rows2_ref[:mains, :half] = rows_ref[:, 0:MAIN, :].reshape(mains, half)
-    rows2_ref[:mains, half:] = rows_ref[:, MAIN : 2 * MAIN, :].reshape(mains, half)
-    ends = jnp.dot(
-        spread, rows_ref[:, 2 * MAIN :, :].reshape(2 * tails, half), preferred_element_type=jnp.float32
-    ).astype(jnp.bfloat16)
-    rows2_ref[mains:, :half] = ends[:tails]
-    rows2_ref[mains:, half:] = ends[tails:]
-    rows = rows2_ref[...]
+    total, _, half = rows_ref.shape
+    tails, mains = PASS * TAIL, PASS * MAIN
+
+    def halves(source, target, at):
+        middle = source.shape[0] // 2
+        return [
+            pltpu.make_async_copy(source.at[part], target.at[part], sems.at[at + i])
+            for i, part in enumerate((pl.ds(0, middle), pl.ds(middle, middle)))
+        ]
+
+    loads = []
+    for source, target in (
+        (gate0, gate0_ref),
+        (up0, up0_ref),
+        (gate1, gate1_ref),
+        (up1, up1_ref),
+        (down0, down0_ref),
+        (down1, down1_ref),
+    ):
+        loads.append(halves(source.at[0], target.at[0], 2 * len(loads)))
+    for source, target in (
+        (shared_gate, shared_gate_ref),
+        (shared_up, shared_up_ref),
+        (shared_down, shared_down_ref),
+        (mixed, mixed_ref),
+        (normed, normed_ref),
+    ):
+        loads.append(halves(source, target, 2 * len(loads)))
+    row_loads = [copy_group(rows, rows_ref, row_sems, first, PASS, 4) for first in range(0, total, PASS)]
+
+    def start(groups):
+        for group in groups:
+            for copy in group:
+                copy.start()
+
+    def finish(groups):
+        for group in groups:
+            for copy in group:
+                copy.wait()
+
+    start(row_loads[:1])
+    start(loads[:6])
+    start(row_loads[1:])
+    start(loads[6:])
+    row = lax.broadcasted_iota(jnp.int32, (2 * tails, 2 * tails), 0)
+    col = lax.broadcasted_iota(jnp.int32, (2 * tails, 2 * tails), 1)
+    slot = row % tails
+    home = slot // TAIL * (2 * TAIL) + row // tails * TAIL + slot % TAIL
+    spread_ref[...] = (home == col).astype(jnp.bfloat16)
 
     def hidden(rows, gate_matrix, up_matrix):
         gate = jnp.dot(rows, gate_matrix, preferred_element_type=jnp.float32)
         upward = jnp.dot(rows, up_matrix, preferred_element_type=jnp.float32)
         return (jax.nn.silu(gate) * upward).astype(jnp.bfloat16)
 
-    arrived(0, 1)
-    act0 = hidden(rows, gate0_ref[0], up0_ref[0])
-    arrived(2, 3)
-    act1 = hidden(rows, gate1_ref[0], up1_ref[0])
-    arrived(4, 5)
-    for part in range(2):
-        span = pl.ds(part * half, half)
-        result = jnp.dot(act0, down0_ref[0, :, span], preferred_element_type=jnp.float32) + jnp.dot(
-            act1, down1_ref[0, :, span], preferred_element_type=jnp.float32
+    copies = []
+    for turn, first in enumerate(range(0, total, PASS)):
+        finish(row_loads[turn : turn + 1])
+        part = slice(first, first + PASS)
+        spread = spread_ref[...]
+        rows2_ref[:mains, :half] = rows_ref[part, 0:MAIN, :].reshape(mains, half)
+        rows2_ref[:mains, half:] = rows_ref[part, MAIN : 2 * MAIN, :].reshape(mains, half)
+        ends = jnp.dot(
+            spread, rows_ref[part, 2 * MAIN :, :].reshape(2 * tails, half), preferred_element_type=jnp.float32
+        ).astype(jnp.bfloat16)
+        rows2_ref[mains:, :half] = ends[:tails]
+        rows2_ref[mains:, half:] = ends[tails:]
+        if turn == 0:
+            finish(loads[0:2])
+        act0 = hidden(rows2_ref[...], gate0_ref[0], up0_ref[0])
+        if turn == 0:
+            finish(loads[2:4])
+        act1 = hidden(rows2_ref[...], gate1_ref[0], up1_ref[0])
+        if turn == 0:
+            finish(loads[4:6])
+        ends = []
+        for side in range(2):
+            span = slice(side * half, (side + 1) * half)
+            result = jnp.dot(act0, down0_ref[0, :, span], preferred_element_type=jnp.float32) + jnp.dot(
+                act1, down1_ref[0, :, span], preferred_element_type=jnp.float32
+            )
+            result = result.astype(jnp.bfloat16)
+            out_ref[part, side * MAIN : (side + 1) * MAIN, :] = result[:mains].reshape(PASS, MAIN, half)
+            ends.append(result[mains:])
+        ends = lax.dot_general(
+            spread, jnp.concatenate(ends, axis=0), (((0,), (0,)), ((), ())), preferred_element_type=jnp.float32
         )
-        result = result.astype(jnp.bfloat16)
-        out_ref[:, part * MAIN : (part + 1) * MAIN, :] = result[:mains].reshape(sources, MAIN, half)
-        if part == 0:
-            first = result[mains:]
-        else:
-            ends = jnp.concatenate([first, result[mains:]], axis=0)
-            ends = lax.dot_general(
-                spread, ends, (((0,), (0,)), ((), ())), preferred_element_type=jnp.float32
-            )
-            out_ref[:, 2 * MAIN :, :] = ends.astype(jnp.bfloat16).reshape(sources, 2 * TAIL, half)
-
-    @pl.when(pl.program_id(0) == pl.num_programs(0) - 1)
-    def _():
-        for load in loads[6:]:
-            load.wait()
-        act = hidden(normed_ref[...], shared_gate_ref[...], shared_up_ref[...])
-        base_ref[...] = mixed_ref[...].astype(jnp.float32) + jnp.dot(
-            act, shared_down_ref[...], preferred_element_type=jnp.float32
-        )
+        out_ref[part, 2 * MAIN :, :] = ends.astype(jnp.bfloat16).reshape(PASS, 2 * TAIL, half)
+        group = copy_group(out_ref, out, out_sems, first, PASS, 4)
+        start([group])
+        copies.append(group)
+
+    finish(loads[6:])
+    act = hidden(normed_ref[...], shared_gate_ref[...], shared_up_ref[...])
+    base_ref[...] = mixed_ref[...].astype(jnp.float32) + jnp.dot(
+        act, shared_down_ref[...], preferred_element_type=jnp.float32
+    )
+    finish(copies)
 
 
 def expert(rows, weights, mixed, normed):
-    step = 16
-    block = pl.BlockSpec((step,) + rows.shape[1:], lambda i: (i, 0, 0))
-    whole = pl.BlockSpec(mixed.shape, lambda i: (0, 0))
+    local_refs = list(weights) + [mixed, normed]
     return pl.pallas_call(
         expert_kernel,
-        grid=(rows.shape[0] // step,),
-        in_specs=[block] + [pl.BlockSpec(memory_space=pl.ANY)] * len(weights) + [whole] * 2,
-        out_specs=[block, whole],
+        in_specs=[pl.BlockSpec(memory_space=pl.ANY)] * (1 + len(local_refs)),
+        out_specs=[pl.BlockSpec(memory_space=pl.ANY), pl.BlockSpec(memory_space=pltpu.VMEM)],
         out_shape=[
             jax.ShapeDtypeStruct(rows.shape, jnp.bfloat16),
             jax.ShapeDtypeStruct(mixed.shape, jnp.float32),
         ],
         scratch_shapes=[
-            pltpu.VMEM((step * 2 * TAIL, step * 2 * TAIL), jnp.bfloat16),
-            pltpu.VMEM((step * (MAIN + TAIL), 2 * rows.shape[2]), jnp.bfloat16),
+            pltpu.VMEM((PASS * 2 * TAIL, PASS * 2 * TAIL), jnp.bfloat16),
+            pltpu.VMEM(rows.shape, jnp.bfloat16),
+            pltpu.VMEM((PASS * (MAIN + TAIL), 2 * rows.shape[2]), jnp.bfloat16),
+            pltpu.VMEM(rows.shape, jnp.bfloat16),
         ]
-        + [pltpu.VMEM(w.shape, w.dtype) for w in weights]
-        + [pltpu.SemaphoreType.DMA((len(weights),))],
-        compiler_params=pltpu.CompilerParams(vmem_limit_bytes=VMEM_BYTES),
+        + [pltpu.VMEM(w.shape, w.dtype) for w in local_refs]
+        + [
+            pltpu.SemaphoreType.DMA((16,)),
+            pltpu.SemaphoreType.DMA((2 * len(local_refs),)),
+            pltpu.SemaphoreType.DMA((16,)),
+        ],
+        compiler_params=pltpu.CompilerParams(vmem_limit_bytes=VMEM_BYTES - 2**21),
         cost_estimate=pl.CostEstimate(flops=8 * 10**9, bytes_accessed=17 * 10**6, transcendentals=10**6),
         name="expert",
-    )(rows, *weights, mixed, normed)
+    )(rows, *local_refs)
 
 
 def combine_kernel(rows_ref, ranks_ref, base_ref, out_ref, acc_ref):
@@ -455,7 +519,7 @@
 
 
 def combine(rows, ranks, base):
-    step = 16
+    step = 32
     whole = lambda i: (0, 0)
     return pl.pallas_call(
         combine_kernel,

time: 279 us -> 272 us (0.975)
  Pallas kernels: 74.8 us -> 67.4 us
    pallas_call x2, Pallas kernels: 21.9 us -> 18.4 us  [the longest x1 15.8 us: expert(): pl.pallas_call(expert_kernel, in_specs=[pl.BlockSpec(memory_space=pl.ANY)...]
where the time goes in v6:
time: 272 us
  blocking collectives  197 us (72%)
  Pallas kernels  67.4 us (25%)
  waiting for transfers between devices  4 us (1%)
    all_to_all x1, blocking collectives, local(): incoming = lax.all_to_all(outgoing, 'sp', 0, 0, tiled=True)  68.9 us
    all_to_all x1, blocking collectives, local(): returned = lax.all_to_all(result, 'sp', 0, 0, tiled=True)  68.9 us
    all_to_all x1, blocking collectives, local(): mine = lax.all_to_all(spread(cores, keep, taken), 'sp', 0, 0, tiled=True)  43.5 us
    pallas_call x1, Pallas kernels, attention(): pl.pallas_call(attention_kernel, out_shape=jax.ShapeDtypeStruct((chips, 8...  33.1 us
    pallas_call x1, Pallas kernels, expert(): pl.pallas_call(expert_kernel, in_specs=[pl.BlockSpec(memory_space=pl.ANY)...  15.8 us
    all_to_all x1, blocking collectives, local(): attended = lax.all_to_all(attended, 'sp', 0, 0, tiled=True)  15.5 us
    pallas_call x1, Pallas kernels, dispatch(): pl.pallas_call(dispatch_kernel, grid=(experts // step,), in_specs=[pl.Blo...  6.5 us
    pallas_call x1, Pallas kernels, combine(): pl.pallas_call(combine_kernel, grid=(rows.shape[0] // step,), in_specs=[p...  6.1 us
  transfers between devices with their start and end apart: 5, of which 2 were waited for; matrix products, arithmetic and copies ran while one was open for 0% of the time, Pallas kernels for 13%

profile of v6, /device:TPU:0, one launch (start us, length us, event | category | flops | bytes accessed | tf_op | source)
XLA Modules:
  0.0 271.7 jit_solution(11233227520292335944)
XLA Ops:
  0.0 1.9 pack.1
  1.9 0.0 collective-permute-start
  1.9 1.6 collective-permute-done.taken_ref
  3.6 0.0 copy-start.1
  3.6 0.7 copy-done.1
  4.2 2.5 spread.1
  6.8 43.5 %all_to_all.20.mine = bf16[64,136,128]{2,1,0:T(8,128)(2,1)S(1)} all-to-all(bf16[64,136,128]{2,1,0:T(8,128)(2,1)} %spread.1), channel_id=1, replica_groups=mesh['sp'=64,'tp'=2] {'sp'}, dimensions={0} | all-to-all | bytes 4456448 | tf_op jit(solution)/shard_map/all_to_all | solution.py:563
  50.3 0.0 copy-start
  50.3 1.4 copy-done
  51.7 0.0 collective-permute-start.1
  51.7 0.7 pad_add_fusion.meta_ref
  52.3 1.5 route.1.rank_ref.ranks_ref
  53.8 2.3 collective-permute-done.1.peer
  56.1 0.1 collective-permute-start.2
  56.3 0.4 collective-permute-start.3
  56.7 0.1 collective-permute-start.4
  56.8 33.1 %attend.1 = bf16[64,8,128]{2,1,0:T(8,128)(2,1)} custom-call(s32[2]{0:T(128)} %pad_add_fusion.meta_ref, bf16[64,136,128]{2,1,0:T(8,128)(2,1)} %copy-done, bf16[64,136,128]{2,1,0:T(8,128)(2,1)} %collective-permute-done.1.peer), custom_call_target="tpu_custom_call" | custom-call | flops 13690208256 | bytes 6291456 | tf_op jit(solution)/shard_map/attend/pallas_call | solution.py:188
  89.9 0.0 collective-permute-done.2.gate1
  89.9 0.0 collective-permute-done.3.up1
  89.9 0.0 collective-permute-done.4.down1
  89.9 15.5 %all_to_all.21.attended_ref = bf16[64,8,128]{2,1,0:T(8,128)(2,1)} all-to-all(bf16[64,8,128]{2,1,0:T(8,128)(2,1)} %attend.1), channel_id=1, replica_groups=mesh['sp'=64,'tp'=2] {'sp'}, dimensions={0} | all-to-all | bytes 262144 | tf_op jit(solution)/shard_map/all_to_all | solution.py:577
  105.5 6.5 %dispatch.1 = (bf16[128,2048]{1,0:T(8,128)(2,1)}, bf16[128,2048]{1,0:T(8,128)(2,1)}, bf16[64,40,1024]{2,1,0:T(8,128)(2,1)}) custom-call(bf16[64,8,128]{2,1,0:T(8,128)(2,1)} %all_to_all.21.attended_ref, bf16[128,2048]{1,0:T(8,128)(2,1)} %residual_ref.1, bf16[512,2048]{1,0:T(8,128)(2,1)} %weight_ref.1, f32[1,2048]{1,0:T(1,128)} %bitcast.7, ...), custom_call_target="tpu_custom_call" | custom-call | flops 1000000000 | bytes 10000000 | tf_op jit(solution)/shard_map/dispatch/pallas_call | solution.py:290
  112.0 68.9 %all_to_all.22.rows = bf16[64,40,1024]{2,1,0:T(8,128)(2,1)} all-to-all(bf16[64,40,1024]{2,1,0:T(8,128)(2,1)} %get-tuple-element.35), channel_id=1, replica_groups=mesh['sp'=64,'tp'=2] {'sp'}, dimensions={0} | all-to-all | bytes 10485760 | tf_op jit(solution)/shard_map/all_to_all | solution.py:582
  180.9 15.8 %expert.1 = (bf16[64,40,1024]{2,1,0:T(8,128)(2,1)}, f32[128,2048]{1,0:T(8,128)}) custom-call(bf16[64,40,1024]{2,1,0:T(8,128)(2,1)} %all_to_all.22.rows, bf16[1,2048,256]{2,1,0:T(8,128)(2,1)} %gate0.1, bf16[1,2048,256]{2,1,0:T(8,128)(2,1)} %up0.1, bf16[1,2048,256]{2,1,0:T(8,128)(2,1)} %collective-permute-done.2.gate1, ...), custom_call_target="tpu_custom_call" | custom-call | flops 8000000000 | bytes 17000000 | tf_op jit(solution)/shard_map/expert/pallas_call | solution.py:456
  196.7 68.9 %all_to_all.23.rows_ref = bf16[64,40,1024]{2,1,0:T(8,128)(2,1)} all-to-all(bf16[64,40,1024]{2,1,0:T(8,128)(2,1)} %get-tuple-element.41), channel_id=1, replica_groups=mesh['sp'=64,'tp'=2] {'sp'}, dimensions={0} | all-to-all | bytes 10485760 | tf_op jit(solution)/shard_map/all_to_all | solution.py:599
  265.6 6.1 %combine.1 = bf16[128,2048]{1,0:T(8,128)(2,1)} custom-call(bf16[64,40,1024]{2,1,0:T(8,128)(2,1)} %all_to_all.23.rows_ref, bf16[192,128]{1,0:T(8,128)(2,1)} %route.1.rank_ref.ranks_ref, f32[128,2048]{1,0:T(8,128)} %get-tuple-element.42.base_ref), custom_call_target="tpu_custom_call" | custom-call | flops 1000000000 | bytes 10000000 | tf_op jit(solution)/shard_map/combine/pallas_call | solution.py:524
Async XLA Ops:
  1.9 1.7 collective-permute-start
  3.6 0.7 copy-start.1
  50.3 1.4 copy-start
  51.7 4.5 %collective-permute-start.1 = (bf16[64,136,128]{2,1,0:T(8,128)(2,1)S(1)}, bf16[64,136,128]{2,1,0:T(8,128)(2,1)}, u32[]{:S(2)}, u32[]{:S(2)}) collective-permute-start(bf16[64,136,128]{2,1,0:T(8,128)(2,1)S(1)} %all_to_all.20.mine), channel_id=1, source_target_pairs={{0,1},{1,0},{2,3},{3,2},{4,5},{5,4},{6,7},{7,6},{8,9},{9,8},{10,11... | collective-permute-start | bytes 6684680 | tf_op jit(solution)/shard_map/ppermute | solution.py:564
  56.1 33.8 %collective-permute-start.2 = (bf16[1,2048,256]{2,1,0:T(8,128)(2,1)}, bf16[1,2048,256]{2,1,0:T(8,128)(2,1)}, u32[]{:S(2)}, u32[]{:S(2)}) collective-permute-start(bf16[1,2048,256]{2,1,0:T(8,128)(2,1)} %gate0.1), channel_id=1, source_target_pairs={{0,1},{1,0},{2,3},{3,2},{4,5},{5,4},{6,7},{7,6},{8,9},{9,8},{10,11... | collective-permute-start | bytes 3145736 | tf_op jit(solution)/shard_map/ppermute | solution.py:571
  56.3 33.6 %collective-permute-start.3 = (bf16[1,2048,256]{2,1,0:T(8,128)(2,1)}, bf16[1,2048,256]{2,1,0:T(8,128)(2,1)}, u32[]{:S(2)}, u32[]{:S(2)}) collective-permute-start(bf16[1,2048,256]{2,1,0:T(8,128)(2,1)} %up0.1), channel_id=1, source_target_pairs={{0,1},{1,0},{2,3},{3,2},{4,5},{5,4},{6,7},{7,6},{8,9},{9,8},{10,11... | collective-permute-start | bytes 3145736 | tf_op jit(solution)/shard_map/ppermute | solution.py:572
  56.7 33.3 %collective-permute-start.4 = (bf16[1,256,2048]{2,1,0:T(8,128)(2,1)}, bf16[1,256,2048]{2,1,0:T(8,128)(2,1)}, u32[]{:S(2)}, u32[]{:S(2)}) collective-permute-start(bf16[1,256,2048]{2,1,0:T(8,128)(2,1)} %down0.1), channel_id=1, source_target_pairs={{0,1},{1,0},{2,3},{3,2},{4,5},{5,4},{6,7},{7,6},{8,9},{9,8},{10,11... | collective-permute-start | bytes 3145736 | tf_op jit(solution)/shard_map/ppermute | solution.py:573

commit v7 on v6

--- a/solution.py
+++ b/solution.py
@@ -40,22 +40,15 @@
     )(core, queries, key_rows, value_rows)
 
 
-def spread_kernel(core_ref, keep_ref, taken_ref, out_ref, held_ref, sems):
-    chips, depth, _ = held_ref.shape
-    heads = chips // 8
+def spread_kernel(core_ref, keep_ref, taken_ref, out_ref):
+    chips, depth, _ = out_ref.shape
     rows = depth - 8
-    copies = []
-    for head in range(heads):
+    for head in range(chips // 8):
         mine = head // 4 == core_ref[0]
         held = jnp.where(mine, keep_ref[head % 4], taken_ref[head % 4])
         for chip in range(8):
-            held_ref[8 * head + chip, :rows] = held[:rows]
-            held_ref[8 * head + chip, rows:] = held[rows + 8 * chip : rows + 8 * chip + 8]
-        span = pl.ds(8 * head, 8)
-        copies.append(pltpu.make_async_copy(held_ref.at[span], out_ref.at[span], sems.at[head]))
-        copies[-1].start()
-    for copy in copies:
-        copy.wait()
+            out_ref[8 * head + chip, :rows] = held[:rows]
+            out_ref[8 * head + chip, rows:] = held[rows + 8 * chip : rows + 8 * chip + 8]
 
 
 def spread(core, keep, taken):
@@ -63,10 +56,9 @@
     return pl.pallas_call(
         spread_kernel,
         in_specs=[pl.BlockSpec(memory_space=pltpu.SMEM)] + [pl.BlockSpec(memory_space=pltpu.VMEM)] * 2,
-        out_specs=pl.BlockSpec(memory_space=pl.ANY),
+        out_specs=pl.BlockSpec(memory_space=pltpu.VMEM),
         out_shape=jax.ShapeDtypeStruct(shape, jnp.bfloat16),
-        scratch_shapes=[pltpu.VMEM(shape, jnp.bfloat16), pltpu.SemaphoreType.DMA((8,))],
-        compiler_params=pltpu.CompilerParams(vmem_limit_bytes=VMEM_BYTES - 2**20),
+        compiler_params=pltpu.CompilerParams(vmem_limit_bytes=16 * 2**20),
         name="spread",
     )(core, keep, taken)
 
@@ -103,42 +95,40 @@
 GROUP = 4
 
 
-PIECES = 16
-
-
-def attention_kernel(meta_ref, mine, peer, out_ref, kv_ref, raw_ref, tri_ref, query_ref, acc_ref, sems):
+def attention_kernel(meta_ref, mine_ref, peer, out_ref, kv_ref, tri_ref, query_ref, acc_ref, sems):
     core, offset = meta_ref[0], meta_ref[1]
     side = tri_ref.shape[0]
     rows = side // 2
-    span = kv_ref.shape[0] // PIECES
     first_rows = pl.ds(pl.multiple_of(core * rows, rows), rows)
     other_rows = pl.ds(pl.multiple_of((1 - core) * rows, rows), rows)
-    loads = [pltpu.make_async_copy(mine.at[:, pl.ds(rows, 8)], raw_ref, sems.at[2 * PIECES])]
-    for piece in range(PIECES):
+    span = kv_ref.shape[0] // 4
+    loads = []
+    for piece in range(4):
         chips = pl.ds(piece * span, span)
-        for i, (source, place) in enumerate(((mine, first_rows), (peer, other_rows))):
-            loads.append(
-                pltpu.make_async_copy(
-                    source.at[chips, pl.ds(0, rows)], kv_ref.at[chips, place], sems.at[2 * piece + i]
-                )
-            )
-    for load in loads:
-        load.start()
+        loads.append(
+            pltpu.make_async_copy(peer.at[chips, pl.ds(0, rows)], kv_ref.at[chips, other_rows], sems.at[piece])
+        )
+        loads[-1].start()
     row = lax.broadcasted_iota(jnp.int32, (side, side), 0)
     col = lax.broadcasted_iota(jnp.int32, (side, side), 1)
     tri_ref[...] = (row > col).astype(jnp.float32)
-    loads[0].wait()
-    raw = raw_ref[...]
+    raw = mine_ref[:, rows:]
     none = jnp.zeros(raw.shape[:2] + (HEAD_DIM,), jnp.bfloat16)
     early = jnp.concatenate([raw[:, :, :HEAD_DIM], none], axis=2)
     late = jnp.concatenate([raw[:, :, HEAD_DIM:], none], axis=2)
     query_ref[...] = jnp.concatenate([early, late], axis=1).reshape(query_ref.shape)
-    for load in loads[1:]:
+
+    @pl.loop(0, kv_ref.shape[0] // 4)
+    def _(turn):
+        for i in range(4):
+            kv_ref[4 * turn + i, first_rows] = mine_ref[4 * turn + i, :rows]
+
+    for load in loads:
         load.wait()
 
-    def advance(tile, first, skip, diagonal):
+    def advance(tile, first, skip, diagonal, count=GROUP):
         query = query_ref[tile, skip:]
-        keys = [kv_ref[first + i] for i in range(GROUP)]
+        keys = [kv_ref[first + i] for i in range(count)]
         scores = [
             lax.dot_general(query, kv, (((1,), (1,)), ((), ())), preferred_element_type=jnp.float32)
             * (HEAD_DIM**-0.5 * LOG2E)
@@ -146,21 +136,27 @@
         ]
         costs = [jnp.maximum(s, 0.0) + jnp.log2(1.0 + jnp.exp2(-jnp.abs(s))) for s in scores]
         slacks = [s - c for s, c in zip(scores, costs)]
-        if diagonal is not None:
-            shape = scores[0].shape
-            place = skip + lax.broadcasted_iota(jnp.int32, shape, 0)
+        if diagonal:
+            edge = 16 * GROUP
+            shape = (edge, side)
+            place = lax.broadcasted_iota(jnp.int32, shape, 0)
             place = place // 16 * side + place % 16 + offset - lax.broadcasted_iota(jnp.int32, shape, 1)
-            live = [place > (diagonal + i) * side for i in range(GROUP)]
-            costs = [jnp.where(l, c, 0.0) for l, c in zip(live, costs)]
+            live = [place > i * side for i in range(count)]
+
+            def masked(i, value):
+                top = jnp.where(live[i], value[:edge], 0.0)
+                return top if value.shape[0] == edge else jnp.concatenate([top, value[edge:]], axis=0)
+
+            costs = [masked(i, c) for i, c in enumerate(costs)]
         tri = tri_ref[...]
         insides = [jnp.dot(c, tri, preferred_element_type=jnp.float32) for c in costs]
         acc = acc_ref[skip:]
-        for i in range(GROUP):
+        for i in range(count):
             weight = jnp.exp2(slacks[i] - insides[i])
-            if diagonal is not None:
-                weight = jnp.where(live[i], weight, 0.0)
+            if diagonal:
+                weight = masked(i, weight)
             part = jnp.dot(weight.astype(jnp.bfloat16), keys[i], preferred_element_type=jnp.float32)
-            acc = acc * jnp.exp2(-(insides[i][:, 0:1] + costs[i][:, 0:1])) + part
+            acc = acc * jnp.exp2(-jnp.sum(costs[i], axis=1, keepdims=True)) + part
         acc_ref[skip:] = acc
 
     blocks = query_ref.shape[1] // 16
@@ -170,12 +166,12 @@
     def _(tile):
         acc_ref[...] = jnp.zeros_like(acc_ref)
 
-        @pl.loop(0, steps * tile)
+        @pl.loop(0, steps * tile // 2)
         def _(step):
-            advance(tile, step * GROUP, 0, None)
+            advance(tile, step * 2 * GROUP, 0, False, 2 * GROUP)
 
         for step in range(steps):
-            advance(tile, blocks * tile + step * GROUP, step * GROUP * 16, step * GROUP)
+            advance(tile, blocks * tile + step * GROUP, step * GROUP * 16, True)
         done = acc_ref[:, HEAD_DIM:].reshape(blocks, 16, HEAD_DIM)
         done = jnp.concatenate([done[:, :8], done[:, 8:]], axis=2).astype(jnp.bfloat16)
         out_ref[pl.ds(tile * blocks, blocks)] = done
@@ -190,19 +186,18 @@
         out_shape=jax.ShapeDtypeStruct((chips, 8, LANES), jnp.bfloat16),
         in_specs=[
             pl.BlockSpec(memory_space=pltpu.SMEM),
-            pl.BlockSpec(memory_space=pl.ANY),
+            pl.BlockSpec(memory_space=pltpu.VMEM),
             pl.BlockSpec(memory_space=pl.ANY),
         ],
         out_specs=pl.BlockSpec(memory_space=pltpu.VMEM),
         scratch_shapes=[
             pltpu.VMEM((chips, side, LANES), jnp.bfloat16),
-            pltpu.VMEM((chips, 8, LANES), jnp.bfloat16),
             pltpu.VMEM((side, side), jnp.float32),
             pltpu.VMEM((2, 2 * side, LANES), jnp.bfloat16),
             pltpu.VMEM((2 * side, LANES), jnp.float32),
-            pltpu.SemaphoreType.DMA((2 * PIECES + 1,)),
-        ],
-        compiler_params=pltpu.CompilerParams(vmem_limit_bytes=VMEM_BYTES),
+            pltpu.SemaphoreType.DMA((4,)),
+        ],
+        compiler_params=pltpu.CompilerParams(vmem_limit_bytes=40 * 2**20),
         cost_estimate=pl.CostEstimate(
             flops=pairs * 2 * 768, bytes_accessed=6 * 2**20, transcendentals=pairs * 3
         ),
@@ -308,7 +303,7 @@
             jax.ShapeDtypeStruct((experts, 2 * (MAIN + TAIL), width // 2), jnp.bfloat16),
         ],
         scratch_shapes=[pltpu.VMEM((tokens, 8 * HEAD_DIM), jnp.bfloat16)],
-        compiler_params=pltpu.CompilerParams(vmem_limit_bytes=VMEM_BYTES),
+        compiler_params=pltpu.CompilerParams(vmem_limit_bytes=32 * 2**20),
         cost_estimate=pl.CostEstimate(flops=10**9, bytes_accessed=10**7, transcendentals=0),
         name="dispatch",
     )(attended, residual, out_weight, gain, ranks)

time: 272 us -> 259 us (0.952)
  Pallas kernels: 67.4 us -> 56.6 us
    pallas_call x1, Pallas kernels: 33.1 us -> 28 us  [attention(): pl.pallas_call(attention_kernel, out_shape=jax.ShapeDtypeStruct((chips, 8...]
    pallas_call x1, Pallas kernels: 6.5 us -> 3.04 us  [dispatch(): pl.pallas_call(dispatch_kernel, grid=(experts // step,), in_specs=[pl.Blo...]
  transfers between devices with their start and end apart: 5 -> 5, of which waited for: 2 -> 2; matrix products, arithmetic and copies ran while one was open for 0% -> 0% of each run, Pallas kernels for 13% -> 11%
where the time goes in v7:
time: 259 us; the launch traced here: 258 us
  blocking collectives  195 us (75%)
  Pallas kernels  56.6 us (22%)
  waiting for transfers between devices  4.58 us (2%)
    all_to_all x1, blocking collectives, local(): returned = lax.all_to_all(result, 'sp', 0, 0, tiled=True)  68.8 us
    all_to_all x1, blocking collectives, local(): incoming = lax.all_to_all(outgoing, 'sp', 0, 0, tiled=True)  68.1 us
    all_to_all x1, blocking collectives, local(): mine = lax.all_to_all(spread(cores, keep, taken), 'sp', 0, 0, tiled=True)  43.4 us
    pallas_call x1, Pallas kernels, attention(): pl.pallas_call(attention_kernel, out_shape=jax.ShapeDtypeStruct((chips, 8...  28 us
    pallas_call x1, Pallas kernels, expert(): pl.pallas_call(expert_kernel, in_specs=[pl.BlockSpec(memory_space=pl.ANY)...  15.8 us
    all_to_all x1, blocking collectives, local(): attended = lax.all_to_all(attended, 'sp', 0, 0, tiled=True)  15.2 us
    pallas_call x1, Pallas kernels, combine(): pl.pallas_call(combine_kernel, grid=(rows.shape[0] // step,), in_specs=[p...  6.1 us
  transfers between devices with their start and end apart: 5, of which 2 were waited for; matrix products, arithmetic and copies ran while one was open for 0% of the time, Pallas kernels for 11%

profile of v7, /device:TPU:0, one launch (start us, length us, event | category | flops | bytes accessed | tf_op | source)
XLA Modules:
  0.0 258.5 jit_solution(3962706075074445211)
XLA Ops:
  0.0 1.9 pack.1
  1.9 0.0 collective-permute-start
  1.9 1.6 collective-permute-done.taken_ref
  3.6 0.0 copy-start.1
  3.6 0.9 copy-done.1
  4.5 0.3 spread.1
  4.8 0.0 copy-start.7
  4.8 43.4 %all_to_all.20.mine_ref = bf16[64,136,128]{2,1,0:T(8,128)(2,1)S(1)} all-to-all(bf16[64,136,128]{2,1,0:T(8,128)(2,1)S(1)} %spread.1), channel_id=1, replica_groups=mesh['sp'=64,'tp'=2] {'sp'}, dimensions={0} | all-to-all | bytes 4456448 | tf_op jit(solution)/shard_map/all_to_all | solution.py:558
  48.3 0.0 collective-permute-start.1
  48.3 0.1 pad_add_fusion.meta_ref
  48.3 1.5 route.1.rank_ref.ranks_ref
  49.8 0.0 copy-start
  49.8 0.0 copy-start.2
  49.8 0.0 copy-start.3
  49.8 0.0 copy-start.4
  49.8 2.9 %collective-permute-done.1.peer = bf16[64,136,128]{2,1,0:T(8,128)(2,1)} collective-permute-done((bf16[64,136,128]{2,1,0:T(8,128)(2,1)S(1)}, bf16[64,136,128]{2,1,0:T(8,128)(2,1)}, u32[]{:S(2)}, u32[]{:S(2)}) %collective-permute-start.1) | collective-permute-done | bytes 2228256 | tf_op jit(solution)/shard_map/ppermute | solution.py:559
  52.7 0.0 copy-done.7
  52.7 0.1 collective-permute-start.2
  52.9 0.4 collective-permute-start.3
  53.2 0.1 collective-permute-start.4
  53.4 28.0 %attend.1 = bf16[64,8,128]{2,1,0:T(8,128)(2,1)S(1)} custom-call(s32[2]{0:T(128)S(1)} %pad_add_fusion.meta_ref, bf16[64,136,128]{2,1,0:T(8,128)(2,1)S(1)} %all_to_all.20.mine_ref, bf16[64,136,128]{2,1,0:T(8,128)(2,1)} %collective-permute-done.1.peer), custom_call_target="tpu_custom_call" | custom-call | flops 13690208256 | bytes 6291456 | tf_op jit(solution)/shard_map/attend/pallas_call | solution.py:184
  81.3 0.0 collective-permute-done.2.gate1
  81.4 0.0 copy-start.8
  81.4 0.0 collective-permute-done.3.up1
  81.4 0.0 copy-start.9
  81.4 0.0 collective-permute-done.4.down1
  81.4 0.0 copy-start.10
  81.4 15.2 %all_to_all.21.attended_ref = bf16[64,8,128]{2,1,0:T(8,128)(2,1)S(1)} all-to-all(bf16[64,8,128]{2,1,0:T(8,128)(2,1)S(1)} %attend.1), channel_id=1, replica_groups=mesh['sp'=64,'tp'=2] {'sp'}, dimensions={0} | all-to-all | bytes 262144 | tf_op jit(solution)/shard_map/all_to_all | solution.py:572
  96.6 0.0 copy-done
  96.6 0.0 copy-done.2
  96.6 0.0 copy-done.3
  96.6 0.0 copy-done.4
  96.6 3.0 %dispatch.1 = (bf16[128,2048]{1,0:T(8,128)(2,1)S(1)}, bf16[128,2048]{1,0:T(8,128)(2,1)S(1)}, bf16[64,40,1024]{2,1,0:T(8,128)(2,1)S(1)}) custom-call(bf16[64,8,128]{2,1,0:T(8,128)(2,1)S(1)} %all_to_all.21.attended_ref, bf16[128,2048]{1,0:T(8,128)(2,1)S(1)} %copy-done.3, bf16[512,2048]{1,0:T(8,128)(2,1)S(1)} %copy-done.2, f32[1,2048]{1,0:T(1,128)S(1)} %bitcast.5, ...), custom_call_target="tpu_custom_call" | custom-call | flops 1000000000 | bytes 10000000 | tf_op jit(solution)/shard_map/dispatch/pallas_call | solution.py:285
  99.6 0.0 copy-start.5
  99.7 0.0 copy-start.6
  99.7 68.1 %all_to_all.22.rows = bf16[64,40,1024]{2,1,0:T(8,128)(2,1)} all-to-all(bf16[64,40,1024]{2,1,0:T(8,128)(2,1)S(1)} %get-tuple-element.35), channel_id=1, replica_groups=mesh['sp'=64,'tp'=2] {'sp'}, dimensions={0} | all-to-all | bytes 10485760 | tf_op jit(solution)/shard_map/all_to_all | solution.py:577
  167.7 0.0 copy-done.8
  167.7 0.0 copy-done.9
  167.7 0.0 copy-done.10
  167.7 0.0 copy-done.5
  167.8 0.0 copy-done.6
  167.8 15.8 %expert.1 = (bf16[64,40,1024]{2,1,0:T(8,128)(2,1)}, f32[128,2048]{1,0:T(8,128)}) custom-call(bf16[64,40,1024]{2,1,0:T(8,128)(2,1)} %all_to_all.22.rows, bf16[1,2048,256]{2,1,0:T(8,128)(2,1)} %gate0.1, bf16[1,2048,256]{2,1,0:T(8,128)(2,1)} %up0.1, bf16[1,2048,256]{2,1,0:T(8,128)(2,1)} %copy-done.8, bf16[1,2048,256]{2,1,0:T(8,128)(2,1)} %copy-done.9, ...), custom_call_target="tpu_custom_call" | custom-call | flops 8000000000 | bytes 17000000 | tf_op jit(solution)/shard_map/expert/pallas_call | solution.py:451
  183.6 68.8 %all_to_all.23.rows_ref = bf16[64,40,1024]{2,1,0:T(8,128)(2,1)} all-to-all(bf16[64,40,1024]{2,1,0:T(8,128)(2,1)} %get-tuple-element.41), channel_id=1, replica_groups=mesh['sp'=64,'tp'=2] {'sp'}, dimensions={0} | all-to-all | bytes 10485760 | tf_op jit(solution)/shard_map/all_to_all | solution.py:594
  252.4 6.1 %combine.1 = bf16[128,2048]{1,0:T(8,128)(2,1)} custom-call(bf16[64,40,1024]{2,1,0:T(8,128)(2,1)} %all_to_all.23.rows_ref, bf16[192,128]{1,0:T(8,128)(2,1)} %route.1.rank_ref.ranks_ref, f32[128,2048]{1,0:T(8,128)} %get-tuple-element.42.base_ref), custom_call_target="tpu_custom_call" | custom-call | flops 1000000000 | bytes 10000000 | tf_op jit(solution)/shard_map/combine/pallas_call | solution.py:519
Async XLA Ops:
  1.9 1.7 collective-permute-start
  3.6 0.9 copy-start.1
  4.8 47.9 %copy-start.7 = (bf16[1,2048,256]{2,1,0:T(8,128)(2,1)S(1)}, bf16[1,2048,256]{2,1,0:T(8,128)(2,1)}, u32[]{:S(2)}) copy-start(bf16[1,2048,256]{2,1,0:T(8,128)(2,1)} %gate0.1) | copy-start | bytes 3145732
  48.3 4.5 %collective-permute-start.1 = (bf16[64,136,128]{2,1,0:T(8,128)(2,1)S(1)}, bf16[64,136,128]{2,1,0:T(8,128)(2,1)}, u32[]{:S(2)}, u32[]{:S(2)}) collective-permute-start(bf16[64,136,128]{2,1,0:T(8,128)(2,1)S(1)} %all_to_all.20.mine_ref), channel_id=1, source_target_pairs={{0,1},{1,0},{2,3},{3,2},{4,5},{5,4},{6,7},{7,6},{8,9},{9,8},{10,11... | collective-permute-start | bytes 6684680 | tf_op jit(solution)/shard_map/ppermute | solution.py:559
  49.8 46.8 %copy-start = (bf16[192,128]{1,0:T(8,128)(2,1)S(1)}, bf16[192,128]{1,0:T(8,128)(2,1)}, u32[]{:S(2)}) copy-start(bf16[192,128]{1,0:T(8,128)(2,1)} %route.1.rank_ref.ranks_ref) | copy-start | bytes 147460
  49.8 46.8 %copy-start.2 = (bf16[512,2048]{1,0:T(8,128)(2,1)S(1)}, bf16[512,2048]{1,0:T(8,128)(2,1)}, u32[]{:S(2)}) copy-start(bf16[512,2048]{1,0:T(8,128)(2,1)} %weight_ref.1) | copy-start | bytes 6291460
  49.8 46.8 %copy-start.3 = (bf16[128,2048]{1,0:T(8,128)(2,1)S(1)}, bf16[128,2048]{1,0:T(8,128)(2,1)}, u32[]{:S(2)}) copy-start(bf16[128,2048]{1,0:T(8,128)(2,1)} %residual_ref.1) | copy-start | bytes 1572868
  49.8 46.8 %copy-start.4 = (f32[2048]{0:T(1024)S(1)}, f32[2048]{0:T(1024)}, u32[]{:S(2)}) copy-start(f32[2048]{0:T(1024)} %param.19) | copy-start | bytes 24580
  52.7 28.6 %collective-permute-start.2 = (bf16[1,2048,256]{2,1,0:T(8,128)(2,1)S(1)}, bf16[1,2048,256]{2,1,0:T(8,128)(2,1)S(1)}, u32[]{:S(2)}, u32[]{:S(2)}) collective-permute-start(bf16[1,2048,256]{2,1,0:T(8,128)(2,1)S(1)} %copy-done.7), channel_id=1, source_target_pairs={{0,1},{1,0},{2,3},{3,2},{4,5},{5,4},{6,7},{7,6},{8,9},{9,8},{10,11... | collective-permute-start | bytes 3145736 | tf_op jit(solution)/shard_map/ppermute | solution.py:566
  52.9 28.5 %collective-permute-start.3 = (bf16[1,2048,256]{2,1,0:T(8,128)(2,1)}, bf16[1,2048,256]{2,1,0:T(8,128)(2,1)S(1)}, u32[]{:S(2)}, u32[]{:S(2)}) collective-permute-start(bf16[1,2048,256]{2,1,0:T(8,128)(2,1)} %up0.1), channel_id=1, source_target_pairs={{0,1},{1,0},{2,3},{3,2},{4,5},{5,4},{6,7},{7,6},{8,9},{9,8},{10,11... | collective-permute-start | bytes 3145736 | tf_op jit(solution)/shard_map/ppermute | solution.py:567
  53.2 28.1 %collective-permute-start.4 = (bf16[1,256,2048]{2,1,0:T(8,128)(2,1)}, bf16[1,256,2048]{2,1,0:T(8,128)(2,1)S(1)}, u32[]{:S(2)}, u32[]{:S(2)}) collective-permute-start(bf16[1,256,2048]{2,1,0:T(8,128)(2,1)} %down0.1), channel_id=1, source_target_pairs={{0,1},{1,0},{2,3},{3,2},{4,5},{5,4},{6,7},{7,6},{8,9},{9,8},{10,11... | collective-permute-start | bytes 3145736 | tf_op jit(solution)/shard_map/ppermute | solution.py:568
  81.4 86.4 %copy-start.8 = (bf16[1,2048,256]{2,1,0:T(8,128)(2,1)}, bf16[1,2048,256]{2,1,0:T(8,128)(2,1)S(1)}, u32[]{:S(2)}) copy-start(bf16[1,2048,256]{2,1,0:T(8,128)(2,1)S(1)} %collective-permute-done.2.gate1) | copy-start | bytes 3145732
  81.4 86.4 %copy-start.9 = (bf16[1,2048,256]{2,1,0:T(8,128)(2,1)}, bf16[1,2048,256]{2,1,0:T(8,128)(2,1)S(1)}, u32[]{:S(2)}) copy-start(bf16[1,2048,256]{2,1,0:T(8,128)(2,1)S(1)} %collective-permute-done.3.up1) | copy-start | bytes 3145732
  81.4 86.3 %copy-start.10 = (bf16[1,256,2048]{2,1,0:T(8,128)(2,1)}, bf16[1,256,2048]{2,1,0:T(8,128)(2,1)S(1)}, u32[]{:S(2)}) copy-start(bf16[1,256,2048]{2,1,0:T(8,128)(2,1)S(1)} %collective-permute-done.4.down1) | copy-start | bytes 3145732
  99.6 68.1 %copy-start.5 = (bf16[128,2048]{1,0:T(8,128)(2,1)}, bf16[128,2048]{1,0:T(8,128)(2,1)S(1)}, u32[]{:S(2)}) copy-start(bf16[128,2048]{1,0:T(8,128)(2,1)S(1)} %get-tuple-element.39.mixed) | copy-start | bytes 1572868
  99.7 68.1 %copy-start.6 = (bf16[128,2048]{1,0:T(8,128)(2,1)}, bf16[128,2048]{1,0:T(8,128)(2,1)S(1)}, u32[]{:S(2)}) copy-start(bf16[128,2048]{1,0:T(8,128)(2,1)S(1)} %get-tuple-element.40.normed) | copy-start | bytes 1572868

commit v8 on v7

--- a/solution.py
+++ b/solution.py
@@ -313,24 +313,7 @@
 
 
 def expert_kernel(
-    rows,
-    gate0,
-    up0,
-    gate1,
-    up1,
-    down0,
-    down1,
-    shared_gate,
-    shared_up,
-    shared_down,
-    mixed,
-    normed,
-    out,
-    base_ref,
-    spread_ref,
     rows_ref,
-    rows2_ref,
-    out_ref,
     gate0_ref,
     up0_ref,
     gate1_ref,
@@ -342,54 +325,13 @@
     shared_down_ref,
     mixed_ref,
     normed_ref,
-    row_sems,
-    sems,
-    out_sems,
+    out_ref,
+    base_ref,
+    spread_ref,
+    rows2_ref,
 ):
     total, _, half = rows_ref.shape
     tails, mains = PASS * TAIL, PASS * MAIN
-
-    def halves(source, target, at):
-        middle = source.shape[0] // 2
-        return [
-            pltpu.make_async_copy(source.at[part], target.at[part], sems.at[at + i])
-            for i, part in enumerate((pl.ds(0, middle), pl.ds(middle, middle)))
-        ]
-
-    loads = []
-    for source, target in (
-        (gate0, gate0_ref),
-        (up0, up0_ref),
-        (gate1, gate1_ref),
-        (up1, up1_ref),
-        (down0, down0_ref),
-        (down1, down1_ref),
-    ):
-        loads.append(halves(source.at[0], target.at[0], 2 * len(loads)))
-    for source, target in (
-        (shared_gate, shared_gate_ref),
-        (shared_up, shared_up_ref),
-        (shared_down, shared_down_ref),
-        (mixed, mixed_ref),
-        (normed, normed_ref),
-    ):
-        loads.append(halves(source, target, 2 * len(loads)))
-    row_loads = [copy_group(rows, rows_ref, row_sems, first, PASS, 4) for first in range(0, total, PASS)]
-
-    def start(groups):
-        for group in groups:
-            for copy in group:
-                copy.start()
-
-    def finish(groups):
-        for group in groups:
-            for copy in group:
-                copy.wait()
-
-    start(row_loads[:1])
-    start(loads[:6])
-    start(row_loads[1:])
-    start(loads[6:])
     row = lax.broadcasted_iota(jnp.int32, (2 * tails, 2 * tails), 0)
     col = lax.broadcasted_iota(jnp.int32, (2 * tails, 2 * tails), 1)
     slot = row % tails
@@ -401,10 +343,9 @@
         upward = jnp.dot(rows, up_matrix, preferred_element_type=jnp.float32)
         return (jax.nn.silu(gate) * upward).astype(jnp.bfloat16)
 
-    copies = []
-    for turn, first in enumerate(range(0, total, PASS)):
-        finish(row_loads[turn : turn + 1])
-        part = slice(first, first + PASS)
+    @pl.loop(0, total // PASS)
+    def _(turn):
+        part = pl.ds(turn * PASS, PASS)
         spread = spread_ref[...]
         rows2_ref[:mains, :half] = rows_ref[part, 0:MAIN, :].reshape(mains, half)
         rows2_ref[:mains, half:] = rows_ref[part, MAIN : 2 * MAIN, :].reshape(mains, half)
@@ -413,14 +354,8 @@
         ).astype(jnp.bfloat16)
         rows2_ref[mains:, :half] = ends[:tails]
         rows2_ref[mains:, half:] = ends[tails:]
-        if turn == 0:
-            finish(loads[0:2])
         act0 = hidden(rows2_ref[...], gate0_ref[0], up0_ref[0])
-        if turn == 0:
-            finish(loads[2:4])
         act1 = hidden(rows2_ref[...], gate1_ref[0], up1_ref[0])
-        if turn == 0:
-            finish(loads[4:6])
         ends = []
         for side in range(2):
             span = slice(side * half, (side + 1) * half)
@@ -434,100 +369,77 @@
             spread, jnp.concatenate(ends, axis=0), (((0,), (0,)), ((), ())), preferred_element_type=jnp.float32
         )
         out_ref[part, 2 * MAIN :, :] = ends.astype(jnp.bfloat16).reshape(PASS, 2 * TAIL, half)
-        group = copy_group(out_ref, out, out_sems, first, PASS, 4)
-        start([group])
-        copies.append(group)
-
-    finish(loads[6:])
+
     act = hidden(normed_ref[...], shared_gate_ref[...], shared_up_ref[...])
     base_ref[...] = mixed_ref[...].astype(jnp.float32) + jnp.dot(
         act, shared_down_ref[...], preferred_element_type=jnp.float32
     )
-    finish(copies)
 
 
 def expert(rows, weights, mixed, normed):
-    local_refs = list(weights) + [mixed, normed]
     return pl.pallas_call(
         expert_kernel,
-        in_specs=[pl.BlockSpec(memory_space=pl.ANY)] * (1 + len(local_refs)),
-        out_specs=[pl.BlockSpec(memory_space=pl.ANY), pl.BlockSpec(memory_space=pltpu.VMEM)],
+        in_specs=[pl.BlockSpec(memory_space=pltpu.VMEM)] * (3 + len(weights)),
+        out_specs=[pl.BlockSpec(memory_space=pltpu.VMEM)] * 2,
         out_shape=[
             jax.ShapeDtypeStruct(rows.shape, jnp.bfloat16),
             jax.ShapeDtypeStruct(mixed.shape, jnp.float32),
         ],
         scratch_shapes=[
             pltpu.VMEM((PASS * 2 * TAIL, PASS * 2 * TAIL), jnp.bfloat16),
-            pltpu.VMEM(rows.shape, jnp.bfloat16),
             pltpu.VMEM((PASS * (MAIN + TAIL), 2 * rows.shape[2]), jnp.bfloat16),
-            pltpu.VMEM(rows.shape, jnp.bfloat16),
-        ]
-        + [pltpu.VMEM(w.shape, w.dtype) for w in local_refs]
-        + [
-            pltpu.SemaphoreType.DMA((16,)),
-            pltpu.SemaphoreType.DMA((2 * len(local_refs),)),
-            pltpu.SemaphoreType.DMA((16,)),
-        ],
-        compiler_params=pltpu.CompilerParams(vmem_limit_bytes=VMEM_BYTES - 2**21),
+        ],
+        compiler_params=pltpu.CompilerParams(vmem_limit_bytes=24 * 2**20),
         cost_estimate=pl.CostEstimate(flops=8 * 10**9, bytes_accessed=17 * 10**6, transcendentals=10**6),
         name="expert",
-    )(rows, *local_refs)
+    )(rows, *weights, mixed, normed)
+
+
+HALF = 32
 
 
 def combine_kernel(rows_ref, ranks_ref, base_ref, out_ref, acc_ref):
-    count, _, half = rows_ref.shape
+    total, _, half = rows_ref.shape
     tokens = base_ref.shape[0]
     experts = ranks_ref.shape[0] // 3
-    at = pl.program_id(0)
-
-    @pl.when(at == 0)
-    def _():
-        acc_ref[...] = base_ref[...]
-
-    def weights(slots, wanted):
-        chosen = expand(count, slots, experts, at * count)
-        rank, high, low = [
-            jnp.dot(chosen, ranks_ref[i * experts : (i + 1) * experts], preferred_element_type=jnp.float32)
-            for i in range(3)
-        ]
-        slot = wanted(lax.broadcasted_iota(jnp.int32, rank.shape, 0) % slots).astype(jnp.float32)
-        here = rank == slot
-        parts = [jnp.where(here, part, 0.0) for part in (high, low)]
-        return jnp.concatenate(parts, axis=1).T.astype(jnp.bfloat16)
-
-    main = weights(MAIN, lambda slot: slot)
-    ends = rows_ref[:, 2 * MAIN :, :].reshape(count * 2 * TAIL, half)
-    for part in range(2):
-        tail = weights(
-            2 * TAIL, lambda slot: jnp.where(slot // TAIL == part, MAIN + slot % TAIL, -2)
-        )
-        rows = rows_ref[:, part * MAIN : (part + 1) * MAIN, :].reshape(count * MAIN, half)
-        total = jnp.dot(main, rows, preferred_element_type=jnp.float32) + jnp.dot(
-            tail, ends, preferred_element_type=jnp.float32
-        )
-        span = pl.ds(part * half, half)
-        acc_ref[:, span] += total[:tokens] + total[tokens:]
-
-    @pl.when(at == pl.num_programs(0) - 1)
-    def _():
-        out_ref[...] = acc_ref[...].astype(jnp.bfloat16)
+    acc_ref[...] = base_ref[...]
+
+    @pl.loop(0, total // HALF)
+    def _(turn):
+        def weights(slots, wanted):
+            chosen = expand(HALF, slots, experts, turn * HALF)
+            rank, high, low = [
+                jnp.dot(chosen, ranks_ref[i * experts : (i + 1) * experts], preferred_element_type=jnp.float32)
+                for i in range(3)
+            ]
+            slot = wanted(lax.broadcasted_iota(jnp.int32, rank.shape, 0) % slots).astype(jnp.float32)
+            here = rank == slot
+            parts = [jnp.where(here, part, 0.0) for part in (high, low)]
+            return jnp.concatenate(parts, axis=1).T.astype(jnp.bfloat16)
+
+        part = pl.ds(turn * HALF, HALF)
+        main = weights(MAIN, lambda slot: slot)
+        ends = rows_ref[part, 2 * MAIN :, :].reshape(HALF * 2 * TAIL, half)
+        for side in range(2):
+            tail = weights(2 * TAIL, lambda slot: jnp.where(slot // TAIL == side, MAIN + slot % TAIL, -2))
+            rows = rows_ref[part, side * MAIN : (side + 1) * MAIN, :].reshape(HALF * MAIN, half)
+            sums = jnp.dot(main, rows, preferred_element_type=jnp.float32) + jnp.dot(
+                tail, ends, preferred_element_type=jnp.float32
+            )
+            span = pl.ds(side * half, half)
+            acc_ref[:, span] += sums[:tokens] + sums[tokens:]
+
+    out_ref[...] = acc_ref[...].astype(jnp.bfloat16)
 
 
 def combine(rows, ranks, base):
-    step = 32
-    whole = lambda i: (0, 0)
     return pl.pallas_call(
         combine_kernel,
-        grid=(rows.shape[0] // step,),
-        in_specs=[
-            pl.BlockSpec((step,) + rows.shape[1:], lambda i: (i, 0, 0)),
-            pl.BlockSpec(ranks.shape, whole),
-            pl.BlockSpec(base.shape, whole),
-        ],
-        out_specs=pl.BlockSpec(base.shape, whole),
+        in_specs=[pl.BlockSpec(memory_space=pltpu.VMEM)] * 3,
+        out_specs=pl.BlockSpec(memory_space=pltpu.VMEM),
         out_shape=jax.ShapeDtypeStruct(base.shape, jnp.bfloat16),
         scratch_shapes=[pltpu.VMEM(base.shape, jnp.float32)],
-        compiler_params=pltpu.CompilerParams(vmem_limit_bytes=VMEM_BYTES),
+        compiler_params=pltpu.CompilerParams(vmem_limit_bytes=24 * 2**20),
         cost_estimate=pl.CostEstimate(flops=10**9, bytes_accessed=10**7, transcendentals=0),
         name="combine",
     )(rows, ranks, base)

time: 259 us -> 252 us (0.973)
  Pallas kernels: 56.6 us -> 49.8 us
    pallas_call x2, Pallas kernels: 21.9 us -> 15.1 us  [the longest x1 11.1 us: expert(): pl.pallas_call(expert_kernel, in_specs=[pl.BlockSpec(memory_space=pltpu.V...]
  transfers between devices with their start and end apart: 5 -> 5, of which waited for: 2 -> 2; matrix products, arithmetic and copies ran while one was open for 0% -> 0% of each run, Pallas kernels for 11% -> 12%
where the time goes in v8:
time: 252 us
  blocking collectives  195 us (77%)
  Pallas kernels  49.8 us (20%)
  waiting for transfers between devices  4.57 us (2%)
    all_to_all x1, blocking collectives, local(): returned = lax.all_to_all(result, 'sp', 0, 0, tiled=True)  68.5 us
    all_to_all x1, blocking collectives, local(): incoming = lax.all_to_all(outgoing, 'sp', 0, 0, tiled=True)  68.2 us
    all_to_all x1, blocking collectives, local(): mine = lax.all_to_all(spread(cores, keep, taken), 'sp', 0, 0, tiled=True)  43.4 us
    pallas_call x1, Pallas kernels, attention(): pl.pallas_call(attention_kernel, out_shape=jax.ShapeDtypeStruct((chips, 8...  28 us
    all_to_all x1, blocking collectives, local(): attended = lax.all_to_all(attended, 'sp', 0, 0, tiled=True)  15.2 us
    pallas_call x1, Pallas kernels, expert(): pl.pallas_call(expert_kernel, in_specs=[pl.BlockSpec(memory_space=pltpu.V...  11.1 us
  transfers between devices with their start and end apart: 5, of which 2 were waited for; matrix products, arithmetic and copies ran while one was open for 0% of the time, Pallas kernels for 12%

profile of v8, /device:TPU:0, one launch (start us, length us, event | category | flops | bytes accessed | tf_op | source)
XLA Modules:
  0.0 251.5 jit_solution(15243731031883294724)
XLA Ops:
  0.0 1.9 pack.1
  1.9 0.0 collective-permute-start
  1.9 1.6 collective-permute-done.taken_ref
  3.6 0.0 copy-start.1
  3.6 0.9 copy-done.1
  4.5 0.3 spread.1
  4.8 0.0 copy-start.6
  4.8 43.4 %all_to_all.20.mine_ref = bf16[64,136,128]{2,1,0:T(8,128)(2,1)S(1)} all-to-all(bf16[64,136,128]{2,1,0:T(8,128)(2,1)S(1)} %spread.1), channel_id=1, replica_groups=mesh['sp'=64,'tp'=2] {'sp'}, dimensions={0} | all-to-all | bytes 4456448 | tf_op jit(solution)/shard_map/all_to_all | solution.py:470
  48.3 0.0 collective-permute-start.1
  48.3 0.1 pad_add_fusion.meta_ref
  48.3 1.5 route.1.rank_ref.ranks_ref
  49.8 0.0 copy-start
  49.8 0.0 copy-start.2
  49.8 0.0 copy-start.9
  49.8 0.0 copy-start.10
  49.8 2.9 %collective-permute-done.1.peer = bf16[64,136,128]{2,1,0:T(8,128)(2,1)} collective-permute-done((bf16[64,136,128]{2,1,0:T(8,128)(2,1)S(1)}, bf16[64,136,128]{2,1,0:T(8,128)(2,1)}, u32[]{:S(2)}, u32[]{:S(2)}) %collective-permute-start.1) | collective-permute-done | bytes 2228256 | tf_op jit(solution)/shard_map/ppermute | solution.py:471
  52.7 0.0 copy-done.6
  52.7 0.1 collective-permute-start.2
  52.9 0.4 collective-permute-start.3
  53.2 0.1 collective-permute-start.4
  53.4 28.0 %attend.1 = bf16[64,8,128]{2,1,0:T(8,128)(2,1)S(1)} custom-call(s32[2]{0:T(128)S(1)} %pad_add_fusion.meta_ref, bf16[64,136,128]{2,1,0:T(8,128)(2,1)S(1)} %all_to_all.20.mine_ref, bf16[64,136,128]{2,1,0:T(8,128)(2,1)} %collective-permute-done.1.peer), custom_call_target="tpu_custom_call" | custom-call | flops 13690208256 | bytes 6291456 | tf_op jit(solution)/shard_map/attend/pallas_call | solution.py:184
  81.3 0.0 collective-permute-done.2.gate1_ref
  81.4 0.0 collective-permute-done.3.up1_ref
  81.4 0.0 collective-permute-done.4.down1_ref
  81.4 15.2 %all_to_all.21.attended_ref = bf16[64,8,128]{2,1,0:T(8,128)(2,1)S(1)} all-to-all(bf16[64,8,128]{2,1,0:T(8,128)(2,1)S(1)} %attend.1), channel_id=1, replica_groups=mesh['sp'=64,'tp'=2] {'sp'}, dimensions={0} | all-to-all | bytes 262144 | tf_op jit(solution)/shard_map/all_to_all | solution.py:484
  96.5 0.0 copy-done
  96.6 0.0 copy-done.2
  96.6 0.0 copy-done.9
  96.6 0.0 copy-done.10
  96.6 3.0 %dispatch.1 = (bf16[128,2048]{1,0:T(8,128)(2,1)S(1)}, bf16[128,2048]{1,0:T(8,128)(2,1)S(1)}, bf16[64,40,1024]{2,1,0:T(8,128)(2,1)S(1)}) custom-call(bf16[64,8,128]{2,1,0:T(8,128)(2,1)S(1)} %all_to_all.21.attended_ref, bf16[128,2048]{1,0:T(8,128)(2,1)S(1)} %copy-done.9, bf16[512,2048]{1,0:T(8,128)(2,1)S(1)} %copy-done.2, f32[1,2048]{1,0:T(1,128)S(1)} %bitcast.5, ...), custom_call_target="tpu_custom_call" | custom-call | flops 1000000000 | bytes 10000000 | tf_op jit(solution)/shard_map/dispatch/pallas_call | solution.py:285
  99.6 0.0 copy-start.3
  99.6 0.0 copy-start.4
  99.6 0.0 copy-start.5
  99.7 0.0 copy-start.7
  99.7 0.0 copy-start.8
  99.7 68.2 %all_to_all.22.rows_ref = bf16[64,40,1024]{2,1,0:T(8,128)(2,1)S(1)} all-to-all(bf16[64,40,1024]{2,1,0:T(8,128)(2,1)S(1)} %get-tuple-element.35), channel_id=1, replica_groups=mesh['sp'=64,'tp'=2] {'sp'}, dimensions={0} | all-to-all | bytes 10485760 | tf_op jit(solution)/shard_map/all_to_all | solution.py:489
  167.9 0.0 copy-done.3
  167.9 0.0 copy-done.4
  167.9 0.0 copy-done.5
  167.9 0.0 copy-done.7
  167.9 0.0 copy-done.8
  167.9 11.1 %expert.1 = (bf16[64,40,1024]{2,1,0:T(8,128)(2,1)S(1)}, f32[128,2048]{1,0:T(8,128)S(1)}) custom-call(bf16[64,40,1024]{2,1,0:T(8,128)(2,1)S(1)} %all_to_all.22.rows_ref, bf16[1,2048,256]{2,1,0:T(8,128)(2,1)S(1)} %copy-done.6, bf16[1,2048,256]{2,1,0:T(8,128)(2,1)S(1)} %copy-done.7, bf16[1,2048,256]{2,1,0:T(8,128)(2,1)S(1)} %collective-permute-done.2.gate1_ref, ...), custom_call_target="tpu_custom_call" | custom-call | flops 8000000000 | bytes 17000000 | tf_op jit(solution)/shard_map/expert/pallas_call | solution.py:380
  179.0 68.5 %all_to_all.23.rows_ref = bf16[64,40,1024]{2,1,0:T(8,128)(2,1)S(1)} all-to-all(bf16[64,40,1024]{2,1,0:T(8,128)(2,1)S(1)} %get-tuple-element.41), channel_id=1, replica_groups=mesh['sp'=64,'tp'=2] {'sp'}, dimensions={0} | all-to-all | bytes 10485760 | tf_op jit(solution)/shard_map/all_to_all | solution.py:506
  247.5 4.0 %combine.1 = bf16[128,2048]{1,0:T(8,128)(2,1)} custom-call(bf16[64,40,1024]{2,1,0:T(8,128)(2,1)S(1)} %all_to_all.23.rows_ref, bf16[192,128]{1,0:T(8,128)(2,1)S(1)} %copy-done, f32[128,2048]{1,0:T(8,128)S(1)} %get-tuple-element.42.base_ref), custom_call_target="tpu_custom_call" | custom-call | flops 1000000000 | bytes 10000000 | tf_op jit(solution)/shard_map/combine/pallas_call | solution.py:436
Async XLA Ops:
  1.9 1.7 collective-permute-start
  3.6 0.9 copy-start.1
  4.8 47.9 %copy-start.6 = (bf16[1,2048,256]{2,1,0:T(8,128)(2,1)S(1)}, bf16[1,2048,256]{2,1,0:T(8,128)(2,1)}, u32[]{:S(2)}) copy-start(bf16[1,2048,256]{2,1,0:T(8,128)(2,1)} %gate0_ref.1) | copy-start | bytes 3145732
  48.3 4.5 %collective-permute-start.1 = (bf16[64,136,128]{2,1,0:T(8,128)(2,1)S(1)}, bf16[64,136,128]{2,1,0:T(8,128)(2,1)}, u32[]{:S(2)}, u32[]{:S(2)}) collective-permute-start(bf16[64,136,128]{2,1,0:T(8,128)(2,1)S(1)} %all_to_all.20.mine_ref), channel_id=1, source_target_pairs={{0,1},{1,0},{2,3},{3,2},{4,5},{5,4},{6,7},{7,6},{8,9},{9,8},{10,11... | collective-permute-start | bytes 6684680 | tf_op jit(solution)/shard_map/ppermute | solution.py:471
  49.8 46.7 %copy-start = (bf16[192,128]{1,0:T(8,128)(2,1)S(1)}, bf16[192,128]{1,0:T(8,128)(2,1)}, u32[]{:S(2)}) copy-start(bf16[192,128]{1,0:T(8,128)(2,1)} %route.1.rank_ref.ranks_ref) | copy-start | bytes 147460
  49.8 46.7 %copy-start.2 = (bf16[512,2048]{1,0:T(8,128)(2,1)S(1)}, bf16[512,2048]{1,0:T(8,128)(2,1)}, u32[]{:S(2)}) copy-start(bf16[512,2048]{1,0:T(8,128)(2,1)} %weight_ref.1) | copy-start | bytes 6291460
  49.8 46.7 %copy-start.9 = (bf16[128,2048]{1,0:T(8,128)(2,1)S(1)}, bf16[128,2048]{1,0:T(8,128)(2,1)}, u32[]{:S(2)}) copy-start(bf16[128,2048]{1,0:T(8,128)(2,1)} %residual_ref.1) | copy-start | bytes 1572868
  49.8 46.7 %copy-start.10 = (f32[2048]{0:T(1024)S(1)}, f32[2048]{0:T(1024)}, u32[]{:S(2)}) copy-start(f32[2048]{0:T(1024)} %param.19) | copy-start | bytes 24580
  52.7 28.6 %collective-permute-start.2 = (bf16[1,2048,256]{2,1,0:T(8,128)(2,1)S(1)}, bf16[1,2048,256]{2,1,0:T(8,128)(2,1)S(1)}, u32[]{:S(2)}, u32[]{:S(2)}) collective-permute-start(bf16[1,2048,256]{2,1,0:T(8,128)(2,1)S(1)} %copy-done.6), channel_id=1, source_target_pairs={{0,1},{1,0},{2,3},{3,2},{4,5},{5,4},{6,7},{7,6},{8,9},{9,8},{10,11... | collective-permute-start | bytes 3145736 | tf_op jit(solution)/shard_map/ppermute | solution.py:478
  52.9 28.5 %collective-permute-start.3 = (bf16[1,2048,256]{2,1,0:T(8,128)(2,1)}, bf16[1,2048,256]{2,1,0:T(8,128)(2,1)S(1)}, u32[]{:S(2)}, u32[]{:S(2)}) collective-permute-start(bf16[1,2048,256]{2,1,0:T(8,128)(2,1)} %up0_ref.1), channel_id=1, source_target_pairs={{0,1},{1,0},{2,3},{3,2},{4,5},{5,4},{6,7},{7,6},{8,9},{9,8},{10,11... | collective-permute-start | bytes 3145736 | tf_op jit(solution)/shard_map/ppermute | solution.py:479
  53.2 28.1 %collective-permute-start.4 = (bf16[1,256,2048]{2,1,0:T(8,128)(2,1)}, bf16[1,256,2048]{2,1,0:T(8,128)(2,1)S(1)}, u32[]{:S(2)}, u32[]{:S(2)}) collective-permute-start(bf16[1,256,2048]{2,1,0:T(8,128)(2,1)} %down0_ref.1), channel_id=1, source_target_pairs={{0,1},{1,0},{2,3},{3,2},{4,5},{5,4},{6,7},{7,6},{8,9},{9,8},{10,11... | collective-permute-start | bytes 3145736 | tf_op jit(solution)/shard_map/ppermute | solution.py:480
  99.6 68.3 %copy-start.3 = (bf16[2048,512]{1,0:T(8,128)(2,1)S(1)}, bf16[2048,512]{1,0:T(8,128)(2,1)}, u32[]{:S(2)}) copy-start(bf16[2048,512]{1,0:T(8,128)(2,1)} %shared_gate_ref.1) | copy-start | bytes 6291460
  99.6 68.3 %copy-start.4 = (bf16[2048,512]{1,0:T(8,128)(2,1)S(1)}, bf16[2048,512]{1,0:T(8,128)(2,1)}, u32[]{:S(2)}) copy-start(bf16[2048,512]{1,0:T(8,128)(2,1)} %shared_up_ref.1) | copy-start | bytes 6291460
  99.6 68.3 %copy-start.5 = (bf16[512,2048]{1,0:T(8,128)(2,1)S(1)}, bf16[512,2048]{1,0:T(8,128)(2,1)}, u32[]{:S(2)}) copy-start(bf16[512,2048]{1,0:T(8,128)(2,1)} %shared_down_ref.1) | copy-start | bytes 6291460
  99.7 68.3 %copy-start.7 = (bf16[1,2048,256]{2,1,0:T(8,128)(2,1)S(1)}, bf16[1,2048,256]{2,1,0:T(8,128)(2,1)}, u32[]{:S(2)}) copy-start(bf16[1,2048,256]{2,1,0:T(8,128)(2,1)} %up0_ref.1) | copy-start | bytes 3145732
  99.7 68.3 %copy-start.8 = (bf16[1,256,2048]{2,1,0:T(8,128)(2,1)S(1)}, bf16[1,256,2048]{2,1,0:T(8,128)(2,1)}, u32[]{:S(2)}) copy-start(bf16[1,256,2048]{2,1,0:T(8,128)(2,1)} %down0_ref.1) | copy-start | bytes 3145732

commit v9 on v8

--- a/solution.py
+++ b/solution.py
@@ -36,6 +36,7 @@
         in_specs=[pl.BlockSpec(memory_space=pltpu.SMEM)] + [pl.BlockSpec(memory_space=pltpu.VMEM)] * 3,
         out_specs=[pl.BlockSpec(memory_space=pltpu.VMEM)] * 2,
         out_shape=[half, half],
+        compiler_params=pltpu.CompilerParams(vmem_limit_bytes=8 * 2**20),
         name="pack",
     )(core, queries, key_rows, value_rows)
 
@@ -92,7 +93,8 @@
     )(routes, route_weight)
 
 
-GROUP = 4
+GROUP = 2
+FULL = 8
 
 
 def attention_kernel(meta_ref, mine_ref, peer, out_ref, kv_ref, tri_ref, query_ref, acc_ref, sems):
@@ -126,18 +128,24 @@
     for load in loads:
         load.wait()
 
-    def advance(tile, first, skip, diagonal, count=GROUP):
-        query = query_ref[tile, skip:]
-        keys = [kv_ref[first + i] for i in range(count)]
+    tiles, depth = query_ref.shape[:2]
+    blocks = depth // 16
+
+    def advance(jobs, skip, diagonal, count):
+        chains = [(tile, first + i, i) for tile, first in jobs for i in range(count)]
+        queries = {tile: query_ref[tile, skip:] for tile, _ in jobs}
+        keys = [kv_ref[block] for _, block, _ in chains]
         scores = [
-            lax.dot_general(query, kv, (((1,), (1,)), ((), ())), preferred_element_type=jnp.float32)
+            lax.dot_general(
+                queries[tile], kv, (((1,), (1,)), ((), ())), preferred_element_type=jnp.float32
+            )
             * (HEAD_DIM**-0.5 * LOG2E)
-            for kv in keys
+            for (tile, _, _), kv in zip(chains, keys)
         ]
-        costs = [jnp.maximum(s, 0.0) + jnp.log2(1.0 + jnp.exp2(-jnp.abs(s))) for s in scores]
+        costs = [jnp.maximum(s, jnp.log2(1.0 + jnp.exp2(jnp.minimum(s, 126.0)))) for s in scores]
         slacks = [s - c for s, c in zip(scores, costs)]
         if diagonal:
-            edge = 16 * GROUP
+            edge = 16 * count
             shape = (edge, side)
             place = lax.broadcasted_iota(jnp.int32, shape, 0)
             place = place // 16 * side + place % 16 + offset - lax.broadcasted_iota(jnp.int32, shape, 1)
@@ -147,34 +155,29 @@
                 top = jnp.where(live[i], value[:edge], 0.0)
                 return top if value.shape[0] == edge else jnp.concatenate([top, value[edge:]], axis=0)
 
-            costs = [masked(i, c) for i, c in enumerate(costs)]
+            costs = [masked(i, c) for (_, _, i), c in zip(chains, costs)]
         tri = tri_ref[...]
         insides = [jnp.dot(c, tri, preferred_element_type=jnp.float32) for c in costs]
-        acc = acc_ref[skip:]
-        for i in range(count):
-            weight = jnp.exp2(slacks[i] - insides[i])
+        accs = {tile: acc_ref[tile, skip:] for tile, _ in jobs}
+        for (tile, _, i), kv, cost, slack, inside in zip(chains, keys, costs, slacks, insides):
+            weight = jnp.exp2(slack - inside)
             if diagonal:
                 weight = masked(i, weight)
-            part = jnp.dot(weight.astype(jnp.bfloat16), keys[i], preferred_element_type=jnp.float32)
-            acc = acc * jnp.exp2(-jnp.sum(costs[i], axis=1, keepdims=True)) + part
-        acc_ref[skip:] = acc
-
-    blocks = query_ref.shape[1] // 16
-    steps = blocks // GROUP
-
-    @pl.loop(0, query_ref.shape[0])
-    def _(tile):
-        acc_ref[...] = jnp.zeros_like(acc_ref)
-
-        @pl.loop(0, steps * tile // 2)
-        def _(step):
-            advance(tile, step * 2 * GROUP, 0, False, 2 * GROUP)
-
-        for step in range(steps):
-            advance(tile, blocks * tile + step * GROUP, step * GROUP * 16, True)
-        done = acc_ref[:, HEAD_DIM:].reshape(blocks, 16, HEAD_DIM)
-        done = jnp.concatenate([done[:, :8], done[:, 8:]], axis=2).astype(jnp.bfloat16)
-        out_ref[pl.ds(tile * blocks, blocks)] = done
+            part = jnp.dot(weight.astype(jnp.bfloat16), kv, preferred_element_type=jnp.float32)
+            accs[tile] = accs[tile] * jnp.exp2(-jnp.sum(cost, axis=1, keepdims=True)) + part
+        for tile, acc in accs.items():
+            acc_ref[tile, skip:] = acc
+
+    acc_ref[...] = jnp.zeros_like(acc_ref)
+
+    @pl.loop(0, blocks // FULL)
+    def _(step):
+        advance([(1, step * FULL)], 0, False, FULL)
+
+    for step in range(blocks // GROUP):
+        advance([(tile, blocks * tile + step * GROUP) for tile in range(tiles)], step * GROUP * 16, True, GROUP)
+    done = acc_ref[:, :, HEAD_DIM:].reshape(tiles * blocks, 16, HEAD_DIM)
+    out_ref[...] = jnp.concatenate([done[:, :8], done[:, 8:]], axis=2).astype(jnp.bfloat16)
 
 
 def attention(meta, mine, peer):
@@ -194,7 +197,7 @@
             pltpu.VMEM((chips, side, LANES), jnp.bfloat16),
             pltpu.VMEM((side, side), jnp.float32),
             pltpu.VMEM((2, 2 * side, LANES), jnp.bfloat16),
-            pltpu.VMEM((2 * side, LANES), jnp.float32),
+            pltpu.VMEM((2, 2 * side, LANES), jnp.float32),
             pltpu.SemaphoreType.DMA((4,)),
         ],
         compiler_params=pltpu.CompilerParams(vmem_limit_bytes=40 * 2**20),
@@ -309,7 +312,7 @@
     )(attended, residual, out_weight, gain, ranks)
 
 
-PASS = 16
+PASS = 32
 
 
 def expert_kernel(
@@ -395,7 +398,7 @@
     )(rows, *weights, mixed, normed)
 
 
-HALF = 32
+HALF = 64
 
 
 def combine_kernel(rows_ref, ranks_ref, base_ref, out_ref, acc_ref):

time: 252 us -> 249 us (0.988)
  Pallas kernels: 49.8 us -> 45.2 us
  transfers between devices with their start and end apart: 5 -> 5, of which waited for: 2 -> 2; matrix products, arithmetic and copies ran while one was open for 0% -> 0% of each run, Pallas kernels for 12% -> 11%
where the time goes in v9:
time: 249 us
  blocking collectives  195 us (78%)
  Pallas kernels  45.2 us (18%)
  waiting for transfers between devices  4.35 us (2%)
  local copies, waits for them, and re-layouts  2.76 us (1%)
    all_to_all x1, blocking collectives, local(): returned = lax.all_to_all(result, 'sp', 0, 0, tiled=True)  68.5 us
    all_to_all x1, blocking collectives, local(): incoming = lax.all_to_all(outgoing, 'sp', 0, 0, tiled=True)  68.2 us
    all_to_all x1, blocking collectives, local(): mine = lax.all_to_all(spread(cores, keep, taken), 'sp', 0, 0, tiled=True)  43.4 us
    pallas_call x1, Pallas kernels, attention(): pl.pallas_call(attention_kernel, out_shape=jax.ShapeDtypeStruct((chips, 8...  26.5 us
    all_to_all x1, blocking collectives, local(): attended = lax.all_to_all(attended, 'sp', 0, 0, tiled=True)  15.2 us
    pallas_call x1, Pallas kernels, expert(): pl.pallas_call(expert_kernel, in_specs=[pl.BlockSpec(memory_space=pltpu.V...  10.3 us
  transfers between devices with their start and end apart: 5, of which 2 were waited for; matrix products, arithmetic and copies ran while one was open for 0% of the time, Pallas kernels for 11%

profile of v9, /device:TPU:0, one launch (start us, length us, event | category | flops | bytes accessed | tf_op | source)
XLA Modules:
  0.0 248.7 jit_solution(7792527577505165899)
XLA Ops:
  0.0 0.0 copy-start.1
  0.0 0.9 copy-done.1
  0.9 0.0 copy-start.2
  0.9 0.9 copy-done.2
  1.8 0.0 copy-start.3
  1.8 0.9 copy-done.3
  2.7 0.2 pack.1
  2.9 0.1 collective-permute-start
  3.0 1.4 collective-permute-done.taken_ref
  4.4 0.3 spread.1
  4.7 0.0 copy-start.8
  4.7 43.4 %all_to_all.20.mine_ref = bf16[64,136,128]{2,1,0:T(8,128)(2,1)S(1)} all-to-all(bf16[64,136,128]{2,1,0:T(8,128)(2,1)S(1)} %spread.1), channel_id=1, replica_groups=mesh['sp'=64,'tp'=2] {'sp'}, dimensions={0} | all-to-all | bytes 4456448 | tf_op jit(solution)/shard_map/all_to_all | solution.py:473
  48.2 0.0 collective-permute-start.1
  48.2 0.1 pad_add_fusion.meta_ref
  48.3 1.5 route.1.rank_ref.ranks_ref
  49.7 0.0 copy-start
  49.8 0.0 copy-start.4
  49.8 0.0 copy-start.11
  49.8 0.0 copy-start.12
  49.8 2.9 %collective-permute-done.1.peer = bf16[64,136,128]{2,1,0:T(8,128)(2,1)} collective-permute-done((bf16[64,136,128]{2,1,0:T(8,128)(2,1)S(1)}, bf16[64,136,128]{2,1,0:T(8,128)(2,1)}, u32[]{:S(2)}, u32[]{:S(2)}) %collective-permute-start.1) | collective-permute-done | bytes 2228256 | tf_op jit(solution)/shard_map/ppermute | solution.py:474
  52.7 0.0 copy-done.8
  52.7 0.1 collective-permute-start.2
  52.8 0.4 collective-permute-start.3
  53.2 0.1 collective-permute-start.4
  53.3 26.5 %attend.1 = bf16[64,8,128]{2,1,0:T(8,128)(2,1)S(1)} custom-call(s32[2]{0:T(128)S(1)} %pad_add_fusion.meta_ref, bf16[64,136,128]{2,1,0:T(8,128)(2,1)S(1)} %all_to_all.20.mine_ref, bf16[64,136,128]{2,1,0:T(8,128)(2,1)} %collective-permute-done.1.peer), custom_call_target="tpu_custom_call" | custom-call | flops 13690208256 | bytes 6291456 | tf_op jit(solution)/shard_map/attend/pallas_call | solution.py:187
  79.8 0.0 collective-permute-done.2.gate1_ref
  79.8 0.0 collective-permute-done.3.up1_ref
  79.8 0.0 collective-permute-done.4.down1_ref
  79.8 15.2 %all_to_all.21.attended_ref = bf16[64,8,128]{2,1,0:T(8,128)(2,1)S(1)} all-to-all(bf16[64,8,128]{2,1,0:T(8,128)(2,1)S(1)} %attend.1), channel_id=1, replica_groups=mesh['sp'=64,'tp'=2] {'sp'}, dimensions={0} | all-to-all | bytes 262144 | tf_op jit(solution)/shard_map/all_to_all | solution.py:487
  95.0 0.0 copy-done
  95.0 0.0 copy-done.4
  95.0 0.0 copy-done.11
  95.0 0.0 copy-done.12
  95.1 3.0 %dispatch.1 = (bf16[128,2048]{1,0:T(8,128)(2,1)S(1)}, bf16[128,2048]{1,0:T(8,128)(2,1)S(1)}, bf16[64,40,1024]{2,1,0:T(8,128)(2,1)S(1)}) custom-call(bf16[64,8,128]{2,1,0:T(8,128)(2,1)S(1)} %all_to_all.21.attended_ref, bf16[128,2048]{1,0:T(8,128)(2,1)S(1)} %copy-done.11, bf16[512,2048]{1,0:T(8,128)(2,1)S(1)} %copy-done.4, f32[1,2048]{1,0:T(1,128)S(1)} %bitcast.5, ...), custom_call_target="tpu_custom_call" | custom-call | flops 1000000000 | bytes 10000000 | tf_op jit(solution)/shard_map/dispatch/pallas_call | solution.py:288
  98.1 0.0 copy-start.5
  98.1 0.0 copy-start.6
  98.1 0.0 copy-start.7
  98.1 0.0 copy-start.9
  98.1 0.0 copy-start.10
  98.2 68.2 %all_to_all.22.rows_ref = bf16[64,40,1024]{2,1,0:T(8,128)(2,1)S(1)} all-to-all(bf16[64,40,1024]{2,1,0:T(8,128)(2,1)S(1)} %get-tuple-element.35), channel_id=1, replica_groups=mesh['sp'=64,'tp'=2] {'sp'}, dimensions={0} | all-to-all | bytes 10485760 | tf_op jit(solution)/shard_map/all_to_all | solution.py:492
  166.4 0.0 copy-done.5
  166.4 0.0 copy-done.6
  166.4 0.0 copy-done.7
  166.4 0.0 copy-done.9
  166.4 0.0 copy-done.10
  166.4 10.3 %expert.1 = (bf16[64,40,1024]{2,1,0:T(8,128)(2,1)S(1)}, f32[128,2048]{1,0:T(8,128)S(1)}) custom-call(bf16[64,40,1024]{2,1,0:T(8,128)(2,1)S(1)} %all_to_all.22.rows_ref, bf16[1,2048,256]{2,1,0:T(8,128)(2,1)S(1)} %copy-done.8, bf16[1,2048,256]{2,1,0:T(8,128)(2,1)S(1)} %copy-done.9, bf16[1,2048,256]{2,1,0:T(8,128)(2,1)S(1)} %collective-permute-done.2.gate1_ref, ...), custom_call_target="tpu_custom_call" | custom-call | flops 8000000000 | bytes 17000000 | tf_op jit(solution)/shard_map/expert/pallas_call | solution.py:383
  176.7 68.5 %all_to_all.23.rows_ref = bf16[64,40,1024]{2,1,0:T(8,128)(2,1)S(1)} all-to-all(bf16[64,40,1024]{2,1,0:T(8,128)(2,1)S(1)} %get-tuple-element.41), channel_id=1, replica_groups=mesh['sp'=64,'tp'=2] {'sp'}, dimensions={0} | all-to-all | bytes 10485760 | tf_op jit(solution)/shard_map/all_to_all | solution.py:509
  245.2 3.5 %combine.1 = bf16[128,2048]{1,0:T(8,128)(2,1)} custom-call(bf16[64,40,1024]{2,1,0:T(8,128)(2,1)S(1)} %all_to_all.23.rows_ref, bf16[192,128]{1,0:T(8,128)(2,1)S(1)} %copy-done, f32[128,2048]{1,0:T(8,128)S(1)} %get-tuple-element.42.base_ref), custom_call_target="tpu_custom_call" | custom-call | flops 1000000000 | bytes 10000000 | tf_op jit(solution)/shard_map/combine/pallas_call | solution.py:439
Async XLA Ops:
  0.0 0.9 copy-start.1
  0.9 0.9 copy-start.2
  1.8 0.9 copy-start.3
  2.9 1.5 collective-permute-start
  4.7 47.9 %copy-start.8 = (bf16[1,2048,256]{2,1,0:T(8,128)(2,1)S(1)}, bf16[1,2048,256]{2,1,0:T(8,128)(2,1)}, u32[]{:S(2)}) copy-start(bf16[1,2048,256]{2,1,0:T(8,128)(2,1)} %gate0_ref.1) | copy-start | bytes 3145732
  48.2 4.5 %collective-permute-start.1 = (bf16[64,136,128]{2,1,0:T(8,128)(2,1)S(1)}, bf16[64,136,128]{2,1,0:T(8,128)(2,1)}, u32[]{:S(2)}, u32[]{:S(2)}) collective-permute-start(bf16[64,136,128]{2,1,0:T(8,128)(2,1)S(1)} %all_to_all.20.mine_ref), channel_id=1, source_target_pairs={{0,1},{1,0},{2,3},{3,2},{4,5},{5,4},{6,7},{7,6},{8,9},{9,8},{10,11... | collective-permute-start | bytes 6684680 | tf_op jit(solution)/shard_map/ppermute | solution.py:474
  49.7 45.3 %copy-start = (bf16[192,128]{1,0:T(8,128)(2,1)S(1)}, bf16[192,128]{1,0:T(8,128)(2,1)}, u32[]{:S(2)}) copy-start(bf16[192,128]{1,0:T(8,128)(2,1)} %route.1.rank_ref.ranks_ref) | copy-start | bytes 147460
  49.8 45.3 %copy-start.4 = (bf16[512,2048]{1,0:T(8,128)(2,1)S(1)}, bf16[512,2048]{1,0:T(8,128)(2,1)}, u32[]{:S(2)}) copy-start(bf16[512,2048]{1,0:T(8,128)(2,1)} %weight_ref.1) | copy-start | bytes 6291460
  49.8 45.3 %copy-start.11 = (bf16[128,2048]{1,0:T(8,128)(2,1)S(1)}, bf16[128,2048]{1,0:T(8,128)(2,1)}, u32[]{:S(2)}) copy-start(bf16[128,2048]{1,0:T(8,128)(2,1)} %residual_ref.1) | copy-start | bytes 1572868
  49.8 45.3 %copy-start.12 = (f32[2048]{0:T(1024)S(1)}, f32[2048]{0:T(1024)}, u32[]{:S(2)}) copy-start(f32[2048]{0:T(1024)} %param.19) | copy-start | bytes 24580
  52.7 27.1 %collective-permute-start.2 = (bf16[1,2048,256]{2,1,0:T(8,128)(2,1)S(1)}, bf16[1,2048,256]{2,1,0:T(8,128)(2,1)S(1)}, u32[]{:S(2)}, u32[]{:S(2)}) collective-permute-start(bf16[1,2048,256]{2,1,0:T(8,128)(2,1)S(1)} %copy-done.8), channel_id=1, source_target_pairs={{0,1},{1,0},{2,3},{3,2},{4,5},{5,4},{6,7},{7,6},{8,9},{9,8},{10,11... | collective-permute-start | bytes 3145736 | tf_op jit(solution)/shard_map/ppermute | solution.py:481
  52.8 27.0 %collective-permute-start.3 = (bf16[1,2048,256]{2,1,0:T(8,128)(2,1)}, bf16[1,2048,256]{2,1,0:T(8,128)(2,1)S(1)}, u32[]{:S(2)}, u32[]{:S(2)}) collective-permute-start(bf16[1,2048,256]{2,1,0:T(8,128)(2,1)} %up0_ref.1), channel_id=1, source_target_pairs={{0,1},{1,0},{2,3},{3,2},{4,5},{5,4},{6,7},{7,6},{8,9},{9,8},{10,11... | collective-permute-start | bytes 3145736 | tf_op jit(solution)/shard_map/ppermute | solution.py:482
  53.2 26.6 %collective-permute-start.4 = (bf16[1,256,2048]{2,1,0:T(8,128)(2,1)}, bf16[1,256,2048]{2,1,0:T(8,128)(2,1)S(1)}, u32[]{:S(2)}, u32[]{:S(2)}) collective-permute-start(bf16[1,256,2048]{2,1,0:T(8,128)(2,1)} %down0_ref.1), channel_id=1, source_target_pairs={{0,1},{1,0},{2,3},{3,2},{4,5},{5,4},{6,7},{7,6},{8,9},{9,8},{10,11... | collective-permute-start | bytes 3145736 | tf_op jit(solution)/shard_map/ppermute | solution.py:483
  98.1 68.3 %copy-start.5 = (bf16[2048,512]{1,0:T(8,128)(2,1)S(1)}, bf16[2048,512]{1,0:T(8,128)(2,1)}, u32[]{:S(2)}) copy-start(bf16[2048,512]{1,0:T(8,128)(2,1)} %shared_gate_ref.1) | copy-start | bytes 6291460
  98.1 68.3 %copy-start.6 = (bf16[2048,512]{1,0:T(8,128)(2,1)S(1)}, bf16[2048,512]{1,0:T(8,128)(2,1)}, u32[]{:S(2)}) copy-start(bf16[2048,512]{1,0:T(8,128)(2,1)} %shared_up_ref.1) | copy-start | bytes 6291460
  98.1 68.3 %copy-start.7 = (bf16[512,2048]{1,0:T(8,128)(2,1)S(1)}, bf16[512,2048]{1,0:T(8,128)(2,1)}, u32[]{:S(2)}) copy-start(bf16[512,2048]{1,0:T(8,128)(2,1)} %shared_down_ref.1) | copy-start | bytes 6291460
  98.1 68.3 %copy-start.9 = (bf16[1,2048,256]{2,1,0:T(8,128)(2,1)S(1)}, bf16[1,2048,256]{2,1,0:T(8,128)(2,1)}, u32[]{:S(2)}) copy-start(bf16[1,2048,256]{2,1,0:T(8,128)(2,1)} %up0_ref.1) | copy-start | bytes 3145732
  98.1 68.3 %copy-start.10 = (bf16[1,256,2048]{2,1,0:T(8,128)(2,1)S(1)}, bf16[1,256,2048]{2,1,0:T(8,128)(2,1)}, u32[]{:S(2)}) copy-start(bf16[1,256,2048]{2,1,0:T(8,128)(2,1)} %down0_ref.1) | copy-start | bytes 3145732

commit v10 on v9

--- a/solution.py
+++ b/solution.py
@@ -15,15 +15,15 @@
 VMEM_BYTES = 67043328
 
 
-def pack_kernel(core_ref, query_ref, key_ref, value_ref, keep_out, send_out):
-    heads, rows = keep_out.shape[0], query_ref.shape[0] // 2
+def pack_kernel(core_ref, rows_ref, keep_out, send_out):
+    heads, rows = keep_out.shape[0], rows_ref.shape[1] // 2
     core = core_ref[0]
-    for out, half in ((keep_out, core), (send_out, 1 - core)):
+    for out, half in ((send_out, 1 - core), (keep_out, core)):
         own = pl.ds(half * rows, rows)
         for head in range(heads):
             span = slice(head * HEAD_DIM, (head + 1) * HEAD_DIM)
-            out[head, :rows] = jnp.concatenate([key_ref[own, span], value_ref[own, span]], axis=1)
-            query = query_ref[own, span].reshape(rows // 16, 16, HEAD_DIM)
+            out[head, :rows] = jnp.concatenate([rows_ref[1, own, span], rows_ref[2, own, span]], axis=1)
+            query = rows_ref[0, own, span].reshape(rows // 16, 16, HEAD_DIM)
             query = jnp.concatenate([query[:, :8], query[:, 8:]], axis=2)
             out[head, rows:] = query.reshape(rows // 2, LANES)
 
@@ -33,12 +33,12 @@
     half = jax.ShapeDtypeStruct((width // HEAD_DIM, side // 2 + side // 4, LANES), jnp.bfloat16)
     return pl.pallas_call(
         pack_kernel,
-        in_specs=[pl.BlockSpec(memory_space=pltpu.SMEM)] + [pl.BlockSpec(memory_space=pltpu.VMEM)] * 3,
+        in_specs=[pl.BlockSpec(memory_space=pltpu.SMEM), pl.BlockSpec(memory_space=pltpu.VMEM)],
         out_specs=[pl.BlockSpec(memory_space=pltpu.VMEM)] * 2,
         out_shape=[half, half],
         compiler_params=pltpu.CompilerParams(vmem_limit_bytes=8 * 2**20),
         name="pack",
-    )(core, queries, key_rows, value_rows)
+    )(core, jnp.stack([queries, key_rows, value_rows]))
 
 
 def spread_kernel(core_ref, keep_ref, taken_ref, out_ref):

time: 249 us -> 247 us (level)
  local copies, waits for them, and re-layouts: 2.76 us -> 0.05 us
    unnamed x26 -> x20, local copies, waits for them, and re-layouts: 2.76 us -> 0.05 us
where the time goes in v10:
time: 247 us
  blocking collectives  195 us (79%)
  Pallas kernels  45.3 us (18%)
  waiting for transfers between devices  4.35 us (2%)
    all_to_all x1, blocking collectives, local(): returned = lax.all_to_all(result, 'sp', 0, 0, tiled=True)  68.5 us
    all_to_all x1, blocking collectives, local(): incoming = lax.all_to_all(outgoing, 'sp', 0, 0, tiled=True)  68.2 us
    all_to_all x1, blocking collectives, local(): mine = lax.all_to_all(spread(cores, keep, taken), 'sp', 0, 0, tiled=True)  43.4 us
    pallas_call x1, Pallas kernels, attention(): pl.pallas_call(attention_kernel, out_shape=jax.ShapeDtypeStruct((chips, 8...  26.5 us
    all_to_all x1, blocking collectives, local(): attended = lax.all_to_all(attended, 'sp', 0, 0, tiled=True)  15.2 us
    pallas_call x1, Pallas kernels, expert(): pl.pallas_call(expert_kernel, in_specs=[pl.BlockSpec(memory_space=pltpu.V...  10.3 us
  transfers between devices with their start and end apart: 5, of which 2 were waited for; matrix products, arithmetic and copies ran while one was open for 0% of the time, Pallas kernels for 11%

profile of v10, /device:TPU:0, one launch (start us, length us, event | category | flops | bytes accessed | tf_op | source)
XLA Modules:
  0.0 247.0 jit_solution(3057276229636074027)
XLA Ops:
  0.0 1.1 pad_maximum_fusion.rows_ref
  1.1 0.2 pack.1
  1.3 0.1 collective-permute-start
  1.4 1.4 collective-permute-done.taken_ref
  2.8 0.3 spread.1
  3.1 0.0 copy-start.5
  3.1 43.4 %all_to_all.20.mine_ref = bf16[64,136,128]{2,1,0:T(8,128)(2,1)S(1)} all-to-all(bf16[64,136,128]{2,1,0:T(8,128)(2,1)S(1)} %spread.1), channel_id=1, replica_groups=mesh['sp'=64,'tp'=2] {'sp'}, dimensions={0} | all-to-all | bytes 4456448 | tf_op jit(solution)/shard_map/all_to_all | solution.py:473
  46.6 0.0 collective-permute-start.1
  46.6 0.1 pad_add_fusion.meta_ref
  46.6 1.5 route.1.rank_ref.ranks_ref
  48.1 0.0 copy-start
  48.1 0.0 copy-start.1
  48.1 0.0 copy-start.8
  48.1 0.0 copy-start.9
  48.1 2.9 %collective-permute-done.1.peer = bf16[64,136,128]{2,1,0:T(8,128)(2,1)} collective-permute-done((bf16[64,136,128]{2,1,0:T(8,128)(2,1)S(1)}, bf16[64,136,128]{2,1,0:T(8,128)(2,1)}, u32[]{:S(2)}, u32[]{:S(2)}) %collective-permute-start.1) | collective-permute-done | bytes 2228256 | tf_op jit(solution)/shard_map/ppermute | solution.py:474
  51.0 0.0 copy-done.5
  51.0 0.1 collective-permute-start.2
  51.2 0.4 collective-permute-start.3
  51.6 0.1 collective-permute-start.4
  51.7 26.5 %attend.1 = bf16[64,8,128]{2,1,0:T(8,128)(2,1)S(1)} custom-call(s32[2]{0:T(128)S(1)} %pad_add_fusion.meta_ref, bf16[64,136,128]{2,1,0:T(8,128)(2,1)S(1)} %all_to_all.20.mine_ref, bf16[64,136,128]{2,1,0:T(8,128)(2,1)} %collective-permute-done.1.peer), custom_call_target="tpu_custom_call" | custom-call | flops 13690208256 | bytes 6291456 | tf_op jit(solution)/shard_map/attend/pallas_call | solution.py:187
  78.2 0.0 collective-permute-done.2.gate1_ref
  78.2 0.0 collective-permute-done.3.up1_ref
  78.2 0.0 collective-permute-done.4.down1_ref
  78.2 15.2 %all_to_all.21.attended_ref = bf16[64,8,128]{2,1,0:T(8,128)(2,1)S(1)} all-to-all(bf16[64,8,128]{2,1,0:T(8,128)(2,1)S(1)} %attend.1), channel_id=1, replica_groups=mesh['sp'=64,'tp'=2] {'sp'}, dimensions={0} | all-to-all | bytes 262144 | tf_op jit(solution)/shard_map/all_to_all | solution.py:487
  93.4 0.0 copy-done
  93.4 0.0 copy-done.1
  93.4 0.0 copy-done.8
  93.4 0.0 copy-done.9
  93.4 3.0 %dispatch.1 = (bf16[128,2048]{1,0:T(8,128)(2,1)S(1)}, bf16[128,2048]{1,0:T(8,128)(2,1)S(1)}, bf16[64,40,1024]{2,1,0:T(8,128)(2,1)S(1)}) custom-call(bf16[64,8,128]{2,1,0:T(8,128)(2,1)S(1)} %all_to_all.21.attended_ref, bf16[128,2048]{1,0:T(8,128)(2,1)S(1)} %copy-done.8, bf16[512,2048]{1,0:T(8,128)(2,1)S(1)} %copy-done.1, f32[1,2048]{1,0:T(1,128)S(1)} %bitcast.8, ...), custom_call_target="tpu_custom_call" | custom-call | flops 1000000000 | bytes 10000000 | tf_op jit(solution)/shard_map/dispatch/pallas_call | solution.py:288
  96.5 0.0 copy-start.2
  96.5 0.0 copy-start.3
  96.5 0.0 copy-start.4
  96.5 0.0 copy-start.6
  96.5 0.0 copy-start.7
  96.5 68.2 %all_to_all.22.rows_ref = bf16[64,40,1024]{2,1,0:T(8,128)(2,1)S(1)} all-to-all(bf16[64,40,1024]{2,1,0:T(8,128)(2,1)S(1)} %get-tuple-element.35), channel_id=1, replica_groups=mesh['sp'=64,'tp'=2] {'sp'}, dimensions={0} | all-to-all | bytes 10485760 | tf_op jit(solution)/shard_map/all_to_all | solution.py:492
  164.8 0.0 copy-done.2
  164.8 0.0 copy-done.3
  164.8 0.0 copy-done.4
  164.8 0.0 copy-done.6
  164.8 0.0 copy-done.7
  164.8 10.3 %expert.1 = (bf16[64,40,1024]{2,1,0:T(8,128)(2,1)S(1)}, f32[128,2048]{1,0:T(8,128)S(1)}) custom-call(bf16[64,40,1024]{2,1,0:T(8,128)(2,1)S(1)} %all_to_all.22.rows_ref, bf16[1,2048,256]{2,1,0:T(8,128)(2,1)S(1)} %copy-done.5, bf16[1,2048,256]{2,1,0:T(8,128)(2,1)S(1)} %copy-done.6, bf16[1,2048,256]{2,1,0:T(8,128)(2,1)S(1)} %collective-permute-done.2.gate1_ref, ...), custom_call_target="tpu_custom_call" | custom-call | flops 8000000000 | bytes 17000000 | tf_op jit(solution)/shard_map/expert/pallas_call | solution.py:383
  175.1 68.5 %all_to_all.23.rows_ref = bf16[64,40,1024]{2,1,0:T(8,128)(2,1)S(1)} all-to-all(bf16[64,40,1024]{2,1,0:T(8,128)(2,1)S(1)} %get-tuple-element.41), channel_id=1, replica_groups=mesh['sp'=64,'tp'=2] {'sp'}, dimensions={0} | all-to-all | bytes 10485760 | tf_op jit(solution)/shard_map/all_to_all | solution.py:509
  243.6 3.5 %combine.1 = bf16[128,2048]{1,0:T(8,128)(2,1)} custom-call(bf16[64,40,1024]{2,1,0:T(8,128)(2,1)S(1)} %all_to_all.23.rows_ref, bf16[192,128]{1,0:T(8,128)(2,1)S(1)} %copy-done, f32[128,2048]{1,0:T(8,128)S(1)} %get-tuple-element.42.base_ref), custom_call_target="tpu_custom_call" | custom-call | flops 1000000000 | bytes 10000000 | tf_op jit(solution)/shard_map/combine/pallas_call | solution.py:439
Async XLA Ops:
  1.3 1.5 collective-permute-start
  3.1 47.9 %copy-start.5 = (bf16[1,2048,256]{2,1,0:T(8,128)(2,1)S(1)}, bf16[1,2048,256]{2,1,0:T(8,128)(2,1)}, u32[]{:S(2)}) copy-start(bf16[1,2048,256]{2,1,0:T(8,128)(2,1)} %gate0_ref.1) | copy-start | bytes 3145732
  46.6 4.5 %collective-permute-start.1 = (bf16[64,136,128]{2,1,0:T(8,128)(2,1)S(1)}, bf16[64,136,128]{2,1,0:T(8,128)(2,1)}, u32[]{:S(2)}, u32[]{:S(2)}) collective-permute-start(bf16[64,136,128]{2,1,0:T(8,128)(2,1)S(1)} %all_to_all.20.mine_ref), channel_id=1, source_target_pairs={{0,1},{1,0},{2,3},{3,2},{4,5},{5,4},{6,7},{7,6},{8,9},{9,8},{10,11... | collective-permute-start | bytes 6684680 | tf_op jit(solution)/shard_map/ppermute | solution.py:474
  48.1 45.3 %copy-start = (bf16[192,128]{1,0:T(8,128)(2,1)S(1)}, bf16[192,128]{1,0:T(8,128)(2,1)}, u32[]{:S(2)}) copy-start(bf16[192,128]{1,0:T(8,128)(2,1)} %route.1.rank_ref.ranks_ref) | copy-start | bytes 147460
  48.1 45.3 %copy-start.1 = (bf16[512,2048]{1,0:T(8,128)(2,1)S(1)}, bf16[512,2048]{1,0:T(8,128)(2,1)}, u32[]{:S(2)}) copy-start(bf16[512,2048]{1,0:T(8,128)(2,1)} %weight_ref.1) | copy-start | bytes 6291460
  48.1 45.3 %copy-start.8 = (bf16[128,2048]{1,0:T(8,128)(2,1)S(1)}, bf16[128,2048]{1,0:T(8,128)(2,1)}, u32[]{:S(2)}) copy-start(bf16[128,2048]{1,0:T(8,128)(2,1)} %residual_ref.1) | copy-start | bytes 1572868
  48.1 45.3 %copy-start.9 = (f32[2048]{0:T(1024)S(1)}, f32[2048]{0:T(1024)}, u32[]{:S(2)}) copy-start(f32[2048]{0:T(1024)} %param.19) | copy-start | bytes 24580
  51.0 27.2 %collective-permute-start.2 = (bf16[1,2048,256]{2,1,0:T(8,128)(2,1)S(1)}, bf16[1,2048,256]{2,1,0:T(8,128)(2,1)S(1)}, u32[]{:S(2)}, u32[]{:S(2)}) collective-permute-start(bf16[1,2048,256]{2,1,0:T(8,128)(2,1)S(1)} %copy-done.5), channel_id=1, source_target_pairs={{0,1},{1,0},{2,3},{3,2},{4,5},{5,4},{6,7},{7,6},{8,9},{9,8},{10,11... | collective-permute-start | bytes 3145736 | tf_op jit(solution)/shard_map/ppermute | solution.py:481
  51.2 27.0 %collective-permute-start.3 = (bf16[1,2048,256]{2,1,0:T(8,128)(2,1)}, bf16[1,2048,256]{2,1,0:T(8,128)(2,1)S(1)}, u32[]{:S(2)}, u32[]{:S(2)}) collective-permute-start(bf16[1,2048,256]{2,1,0:T(8,128)(2,1)} %up0_ref.1), channel_id=1, source_target_pairs={{0,1},{1,0},{2,3},{3,2},{4,5},{5,4},{6,7},{7,6},{8,9},{9,8},{10,11... | collective-permute-start | bytes 3145736 | tf_op jit(solution)/shard_map/ppermute | solution.py:482
  51.6 26.7 %collective-permute-start.4 = (bf16[1,256,2048]{2,1,0:T(8,128)(2,1)}, bf16[1,256,2048]{2,1,0:T(8,128)(2,1)S(1)}, u32[]{:S(2)}, u32[]{:S(2)}) collective-permute-start(bf16[1,256,2048]{2,1,0:T(8,128)(2,1)} %down0_ref.1), channel_id=1, source_target_pairs={{0,1},{1,0},{2,3},{3,2},{4,5},{5,4},{6,7},{7,6},{8,9},{9,8},{10,11... | collective-permute-start | bytes 3145736 | tf_op jit(solution)/shard_map/ppermute | solution.py:483
  96.5 68.3 %copy-start.2 = (bf16[2048,512]{1,0:T(8,128)(2,1)S(1)}, bf16[2048,512]{1,0:T(8,128)(2,1)}, u32[]{:S(2)}) copy-start(bf16[2048,512]{1,0:T(8,128)(2,1)} %shared_gate_ref.1) | copy-start | bytes 6291460
  96.5 68.3 %copy-start.3 = (bf16[2048,512]{1,0:T(8,128)(2,1)S(1)}, bf16[2048,512]{1,0:T(8,128)(2,1)}, u32[]{:S(2)}) copy-start(bf16[2048,512]{1,0:T(8,128)(2,1)} %shared_up_ref.1) | copy-start | bytes 6291460
  96.5 68.3 %copy-start.4 = (bf16[512,2048]{1,0:T(8,128)(2,1)S(1)}, bf16[512,2048]{1,0:T(8,128)(2,1)}, u32[]{:S(2)}) copy-start(bf16[512,2048]{1,0:T(8,128)(2,1)} %shared_down_ref.1) | copy-start | bytes 6291460
  96.5 68.3 %copy-start.6 = (bf16[1,2048,256]{2,1,0:T(8,128)(2,1)S(1)}, bf16[1,2048,256]{2,1,0:T(8,128)(2,1)}, u32[]{:S(2)}) copy-start(bf16[1,2048,256]{2,1,0:T(8,128)(2,1)} %up0_ref.1) | copy-start | bytes 3145732
  96.5 68.3 %copy-start.7 = (bf16[1,256,2048]{2,1,0:T(8,128)(2,1)S(1)}, bf16[1,256,2048]{2,1,0:T(8,128)(2,1)}, u32[]{:S(2)}) copy-start(bf16[1,256,2048]{2,1,0:T(8,128)(2,1)} %down0_ref.1) | copy-start | bytes 3145732

commit v11 on v10

--- a/solution.py
+++ b/solution.py
@@ -158,15 +158,23 @@
             costs = [masked(i, c) for (_, _, i), c in zip(chains, costs)]
         tri = tri_ref[...]
         insides = [jnp.dot(c, tri, preferred_element_type=jnp.float32) for c in costs]
-        accs = {tile: acc_ref[tile, skip:] for tile, _ in jobs}
-        for (tile, _, i), kv, cost, slack, inside in zip(chains, keys, costs, slacks, insides):
-            weight = jnp.exp2(slack - inside)
-            if diagonal:
-                weight = masked(i, weight)
-            part = jnp.dot(weight.astype(jnp.bfloat16), kv, preferred_element_type=jnp.float32)
-            accs[tile] = accs[tile] * jnp.exp2(-jnp.sum(cost, axis=1, keepdims=True)) + part
-        for tile, acc in accs.items():
-            acc_ref[tile, skip:] = acc
+        for job, (tile, _) in enumerate(jobs):
+            weights, later = [None] * count, None
+            for i in reversed(range(count)):
+                chain = job * count + i
+                left = slacks[chain] if later is None else slacks[chain] - later
+                weight = jnp.exp2(left - insides[chain])
+                if diagonal:
+                    weight = masked(i, weight)
+                weights[i] = weight.astype(jnp.bfloat16)
+                total = jnp.sum(costs[chain], axis=1, keepdims=True)
+                later = total if later is None else later + total
+            part = jnp.dot(
+                jnp.concatenate(weights, axis=1),
+                jnp.concatenate(keys[job * count : (job + 1) * count], axis=0),
+                preferred_element_type=jnp.float32,
+            )
+            acc_ref[tile, skip:] = acc_ref[tile, skip:] * jnp.exp2(-later) + part
 
     acc_ref[...] = jnp.zeros_like(acc_ref)
 

time: 247 us -> 247 us (level)
  no operation moved by 1% of the time
where the time goes in v11:
time: 247 us
  blocking collectives  195 us (79%)
  Pallas kernels  45 us (18%)
  waiting for transfers between devices  4.35 us (2%)
    all_to_all x1, blocking collectives, local(): returned = lax.all_to_all(result, 'sp', 0, 0, tiled=True)  68.5 us
    all_to_all x1, blocking collectives, local(): incoming = lax.all_to_all(outgoing, 'sp', 0, 0, tiled=True)  68.2 us
    all_to_all x1, blocking collectives, local(): mine = lax.all_to_all(spread(cores, keep, taken), 'sp', 0, 0, tiled=True)  43.4 us
    pallas_call x1, Pallas kernels, attention(): pl.pallas_call(attention_kernel, out_shape=jax.ShapeDtypeStruct((chips, 8...  26.2 us
    all_to_all x1, blocking collectives, local(): attended = lax.all_to_all(attended, 'sp', 0, 0, tiled=True)  15.2 us
    pallas_call x1, Pallas kernels, expert(): pl.pallas_call(expert_kernel, in_specs=[pl.BlockSpec(memory_space=pltpu.V...  10.3 us
  transfers between devices with their start and end apart: 5, of which 2 were waited for; matrix products, arithmetic and copies ran while one was open for 0% of the time, Pallas kernels for 11%

profile of v11, /device:TPU:0, one launch (start us, length us, event | category | flops | bytes accessed | tf_op | source)
XLA Modules:
  0.0 246.7 jit_solution(18004518296029735379)
XLA Ops:
  0.0 1.1 pad_maximum_fusion.rows_ref
  1.1 0.2 pack.1
  1.3 0.1 collective-permute-start
  1.4 1.4 collective-permute-done.taken_ref
  2.8 0.3 spread.1
  3.1 0.0 copy-start.5
  3.1 43.4 %all_to_all.20.mine_ref = bf16[64,136,128]{2,1,0:T(8,128)(2,1)S(1)} all-to-all(bf16[64,136,128]{2,1,0:T(8,128)(2,1)S(1)} %spread.1), channel_id=1, replica_groups=mesh['sp'=64,'tp'=2] {'sp'}, dimensions={0} | all-to-all | bytes 4456448 | tf_op jit(solution)/shard_map/all_to_all | solution.py:481
  46.6 0.0 collective-permute-start.1
  46.6 0.1 pad_add_fusion.meta_ref
  46.6 1.5 route.1.rank_ref.ranks_ref
  48.1 0.0 copy-start
  48.1 0.0 copy-start.1
  48.1 0.0 copy-start.8
  48.1 0.0 copy-start.9
  48.1 2.9 %collective-permute-done.1.peer = bf16[64,136,128]{2,1,0:T(8,128)(2,1)} collective-permute-done((bf16[64,136,128]{2,1,0:T(8,128)(2,1)S(1)}, bf16[64,136,128]{2,1,0:T(8,128)(2,1)}, u32[]{:S(2)}, u32[]{:S(2)}) %collective-permute-start.1) | collective-permute-done | bytes 2228256 | tf_op jit(solution)/shard_map/ppermute | solution.py:482
  51.0 0.0 copy-done.5
  51.0 0.1 collective-permute-start.2
  51.2 0.4 collective-permute-start.3
  51.6 0.1 collective-permute-start.4
  51.7 26.2 %attend.1 = bf16[64,8,128]{2,1,0:T(8,128)(2,1)S(1)} custom-call(s32[2]{0:T(128)S(1)} %pad_add_fusion.meta_ref, bf16[64,136,128]{2,1,0:T(8,128)(2,1)S(1)} %all_to_all.20.mine_ref, bf16[64,136,128]{2,1,0:T(8,128)(2,1)} %collective-permute-done.1.peer), custom_call_target="tpu_custom_call" | custom-call | flops 13690208256 | bytes 6291456 | tf_op jit(solution)/shard_map/attend/pallas_call | solution.py:195
  77.9 0.0 collective-permute-done.2.gate1_ref
  77.9 0.0 collective-permute-done.3.up1_ref
  77.9 0.0 collective-permute-done.4.down1_ref
  77.9 15.2 %all_to_all.21.attended_ref = bf16[64,8,128]{2,1,0:T(8,128)(2,1)S(1)} all-to-all(bf16[64,8,128]{2,1,0:T(8,128)(2,1)S(1)} %attend.1), channel_id=1, replica_groups=mesh['sp'=64,'tp'=2] {'sp'}, dimensions={0} | all-to-all | bytes 262144 | tf_op jit(solution)/shard_map/all_to_all | solution.py:495
  93.1 0.0 copy-done
  93.1 0.0 copy-done.1
  93.1 0.0 copy-done.8
  93.1 0.0 copy-done.9
  93.1 3.0 %dispatch.1 = (bf16[128,2048]{1,0:T(8,128)(2,1)S(1)}, bf16[128,2048]{1,0:T(8,128)(2,1)S(1)}, bf16[64,40,1024]{2,1,0:T(8,128)(2,1)S(1)}) custom-call(bf16[64,8,128]{2,1,0:T(8,128)(2,1)S(1)} %all_to_all.21.attended_ref, bf16[128,2048]{1,0:T(8,128)(2,1)S(1)} %copy-done.8, bf16[512,2048]{1,0:T(8,128)(2,1)S(1)} %copy-done.1, f32[1,2048]{1,0:T(1,128)S(1)} %bitcast.8, ...), custom_call_target="tpu_custom_call" | custom-call | flops 1000000000 | bytes 10000000 | tf_op jit(solution)/shard_map/dispatch/pallas_call | solution.py:296
  96.1 0.0 copy-start.2
  96.2 0.0 copy-start.3
  96.2 0.0 copy-start.4
  96.2 0.0 copy-start.6
  96.2 0.0 copy-start.7
  96.2 68.2 %all_to_all.22.rows_ref = bf16[64,40,1024]{2,1,0:T(8,128)(2,1)S(1)} all-to-all(bf16[64,40,1024]{2,1,0:T(8,128)(2,1)S(1)} %get-tuple-element.35), channel_id=1, replica_groups=mesh['sp'=64,'tp'=2] {'sp'}, dimensions={0} | all-to-all | bytes 10485760 | tf_op jit(solution)/shard_map/all_to_all | solution.py:500
  164.4 0.0 copy-done.2
  164.4 0.0 copy-done.3
  164.4 0.0 copy-done.4
  164.4 0.0 copy-done.6
  164.5 0.0 copy-done.7
  164.5 10.3 %expert.1 = (bf16[64,40,1024]{2,1,0:T(8,128)(2,1)S(1)}, f32[128,2048]{1,0:T(8,128)S(1)}) custom-call(bf16[64,40,1024]{2,1,0:T(8,128)(2,1)S(1)} %all_to_all.22.rows_ref, bf16[1,2048,256]{2,1,0:T(8,128)(2,1)S(1)} %copy-done.5, bf16[1,2048,256]{2,1,0:T(8,128)(2,1)S(1)} %copy-done.6, bf16[1,2048,256]{2,1,0:T(8,128)(2,1)S(1)} %collective-permute-done.2.gate1_ref, ...), custom_call_target="tpu_custom_call" | custom-call | flops 8000000000 | bytes 17000000 | tf_op jit(solution)/shard_map/expert/pallas_call | solution.py:391
  174.8 68.5 %all_to_all.23.rows_ref = bf16[64,40,1024]{2,1,0:T(8,128)(2,1)S(1)} all-to-all(bf16[64,40,1024]{2,1,0:T(8,128)(2,1)S(1)} %get-tuple-element.41), channel_id=1, replica_groups=mesh['sp'=64,'tp'=2] {'sp'}, dimensions={0} | all-to-all | bytes 10485760 | tf_op jit(solution)/shard_map/all_to_all | solution.py:517
  243.2 3.5 %combine.1 = bf16[128,2048]{1,0:T(8,128)(2,1)} custom-call(bf16[64,40,1024]{2,1,0:T(8,128)(2,1)S(1)} %all_to_all.23.rows_ref, bf16[192,128]{1,0:T(8,128)(2,1)S(1)} %copy-done, f32[128,2048]{1,0:T(8,128)S(1)} %get-tuple-element.42.base_ref), custom_call_target="tpu_custom_call" | custom-call | flops 1000000000 | bytes 10000000 | tf_op jit(solution)/shard_map/combine/pallas_call | solution.py:447
Async XLA Ops:
  1.3 1.5 collective-permute-start
  3.1 47.9 %copy-start.5 = (bf16[1,2048,256]{2,1,0:T(8,128)(2,1)S(1)}, bf16[1,2048,256]{2,1,0:T(8,128)(2,1)}, u32[]{:S(2)}) copy-start(bf16[1,2048,256]{2,1,0:T(8,128)(2,1)} %gate0_ref.1) | copy-start | bytes 3145732
  46.6 4.5 %collective-permute-start.1 = (bf16[64,136,128]{2,1,0:T(8,128)(2,1)S(1)}, bf16[64,136,128]{2,1,0:T(8,128)(2,1)}, u32[]{:S(2)}, u32[]{:S(2)}) collective-permute-start(bf16[64,136,128]{2,1,0:T(8,128)(2,1)S(1)} %all_to_all.20.mine_ref), channel_id=1, source_target_pairs={{0,1},{1,0},{2,3},{3,2},{4,5},{5,4},{6,7},{7,6},{8,9},{9,8},{10,11... | collective-permute-start | bytes 6684680 | tf_op jit(solution)/shard_map/ppermute | solution.py:482
  48.1 45.0 %copy-start = (bf16[192,128]{1,0:T(8,128)(2,1)S(1)}, bf16[192,128]{1,0:T(8,128)(2,1)}, u32[]{:S(2)}) copy-start(bf16[192,128]{1,0:T(8,128)(2,1)} %route.1.rank_ref.ranks_ref) | copy-start | bytes 147460
  48.1 45.0 %copy-start.1 = (bf16[512,2048]{1,0:T(8,128)(2,1)S(1)}, bf16[512,2048]{1,0:T(8,128)(2,1)}, u32[]{:S(2)}) copy-start(bf16[512,2048]{1,0:T(8,128)(2,1)} %weight_ref.1) | copy-start | bytes 6291460
  48.1 45.0 %copy-start.8 = (bf16[128,2048]{1,0:T(8,128)(2,1)S(1)}, bf16[128,2048]{1,0:T(8,128)(2,1)}, u32[]{:S(2)}) copy-start(bf16[128,2048]{1,0:T(8,128)(2,1)} %residual_ref.1) | copy-start | bytes 1572868
  48.1 45.0 %copy-start.9 = (f32[2048]{0:T(1024)S(1)}, f32[2048]{0:T(1024)}, u32[]{:S(2)}) copy-start(f32[2048]{0:T(1024)} %param.19) | copy-start | bytes 24580
  51.0 26.8 %collective-permute-start.2 = (bf16[1,2048,256]{2,1,0:T(8,128)(2,1)S(1)}, bf16[1,2048,256]{2,1,0:T(8,128)(2,1)S(1)}, u32[]{:S(2)}, u32[]{:S(2)}) collective-permute-start(bf16[1,2048,256]{2,1,0:T(8,128)(2,1)S(1)} %copy-done.5), channel_id=1, source_target_pairs={{0,1},{1,0},{2,3},{3,2},{4,5},{5,4},{6,7},{7,6},{8,9},{9,8},{10,11... | collective-permute-start | bytes 3145736 | tf_op jit(solution)/shard_map/ppermute | solution.py:489
  51.2 26.7 %collective-permute-start.3 = (bf16[1,2048,256]{2,1,0:T(8,128)(2,1)}, bf16[1,2048,256]{2,1,0:T(8,128)(2,1)S(1)}, u32[]{:S(2)}, u32[]{:S(2)}) collective-permute-start(bf16[1,2048,256]{2,1,0:T(8,128)(2,1)} %up0_ref.1), channel_id=1, source_target_pairs={{0,1},{1,0},{2,3},{3,2},{4,5},{5,4},{6,7},{7,6},{8,9},{9,8},{10,11... | collective-permute-start | bytes 3145736 | tf_op jit(solution)/shard_map/ppermute | solution.py:490
  51.6 26.3 %collective-permute-start.4 = (bf16[1,256,2048]{2,1,0:T(8,128)(2,1)}, bf16[1,256,2048]{2,1,0:T(8,128)(2,1)S(1)}, u32[]{:S(2)}, u32[]{:S(2)}) collective-permute-start(bf16[1,256,2048]{2,1,0:T(8,128)(2,1)} %down0_ref.1), channel_id=1, source_target_pairs={{0,1},{1,0},{2,3},{3,2},{4,5},{5,4},{6,7},{7,6},{8,9},{9,8},{10,11... | collective-permute-start | bytes 3145736 | tf_op jit(solution)/shard_map/ppermute | solution.py:491
  96.1 68.3 %copy-start.2 = (bf16[2048,512]{1,0:T(8,128)(2,1)S(1)}, bf16[2048,512]{1,0:T(8,128)(2,1)}, u32[]{:S(2)}) copy-start(bf16[2048,512]{1,0:T(8,128)(2,1)} %shared_gate_ref.1) | copy-start | bytes 6291460
  96.2 68.3 %copy-start.3 = (bf16[2048,512]{1,0:T(8,128)(2,1)S(1)}, bf16[2048,512]{1,0:T(8,128)(2,1)}, u32[]{:S(2)}) copy-start(bf16[2048,512]{1,0:T(8,128)(2,1)} %shared_up_ref.1) | copy-start | bytes 6291460
  96.2 68.3 %copy-start.4 = (bf16[512,2048]{1,0:T(8,128)(2,1)S(1)}, bf16[512,2048]{1,0:T(8,128)(2,1)}, u32[]{:S(2)}) copy-start(bf16[512,2048]{1,0:T(8,128)(2,1)} %shared_down_ref.1) | copy-start | bytes 6291460
  96.2 68.3 %copy-start.6 = (bf16[1,2048,256]{2,1,0:T(8,128)(2,1)S(1)}, bf16[1,2048,256]{2,1,0:T(8,128)(2,1)}, u32[]{:S(2)}) copy-start(bf16[1,2048,256]{2,1,0:T(8,128)(2,1)} %up0_ref.1) | copy-start | bytes 3145732
  96.2 68.3 %copy-start.7 = (bf16[1,256,2048]{2,1,0:T(8,128)(2,1)S(1)}, bf16[1,256,2048]{2,1,0:T(8,128)(2,1)}, u32[]{:S(2)}) copy-start(bf16[1,256,2048]{2,1,0:T(8,128)(2,1)} %down0_ref.1) | copy-start | bytes 3145732
